TPU v7x, 256 devices: a whole 4x4x8 slice. The times are simulated.
256 devices in a mesh: rep: 2 (over z_hi), fs: 16 (over z_lo, x), tp: 8 (over y, core).
Axes of the slice: x: 4, y: 4, z: 8 (z_hi: 2, z_lo: 4; z = z_hi * 4 + z_lo), core: 2. Of those that a mesh axis runs over, the one named last changes fastest.
Arguments:
- tokens: bfloat16 [4096, 4096], P(('rep', 'fs'), 'tp'), may hold values from -6 to 6
- mixer_gain: float32 [4096], replicated, may hold values from 0.75 to 1.25
- gate_proj: bfloat16 [4096, 2048], P('fs', 'tp'), may hold values from -0.09375 to 0.09375
- value_proj: bfloat16 [4096, 2048], P('fs', 'tp'), may hold values from -0.09375 to 0.09375
- value_gain: float32 [16, 128], P('tp'), may hold values from 0.75 to 1.25
- spatial_mix: bfloat16 [16, 128, 128], P('tp', 'fs'), may hold values from -0.5 to 0.5
- spatial_bias: float32 [16, 128], P('tp'), may hold values from 0.5 to 1.5
- head_gain: float32 [16, 128], P('tp'), may hold values from 0.75 to 1.25
- merge_proj: bfloat16 [2048, 4096], P('tp', 'fs'), may hold values from -0.125 to 0.125
- ffn_gain: float32 [4096], replicated, may hold values from 0.25 to 1.75
- gate_up: bfloat16 [4096, 11008], P('fs', 'tp'), may hold values from -0.09375 to 0.09375
- value_up: bfloat16 [4096, 11008], P('fs', 'tp'), may hold values from -0.09375 to 0.09375
- gate_kernel: float32 [3, 11008], P(None, 'tp'), may hold values from -3.5 to 3.5
- value_kernel: float32 [3, 11008], P(None, 'tp'), may hold values from -3.5 to 3.5
- gate_offset: float32 [11008], P('tp'), may hold values from -0.6 to 0.6
- value_offset: float32 [11008], P('tp'), may hold values from -1.8 to 1.8
- down_proj: bfloat16 [11008, 4096], P('tp', 'fs'), may hold values from -0.0546875 to 0.0546875
Outputs:
- layer_out: bfloat16 [4096, 4096], P(('rep', 'fs'), 'tp')
All inputs are finite; a program needn't handle non-finite values.
Results may differ from a plain program's by a relative error of at most 0.02.
Values may be sent and summed in bfloat16 or wider, within the bound.
No kernel may reach another device: no remote copies, remote signals or barrier semaphores. Data moves between devices by JAX's collectives and lax.ppermute only.
A program may use at most 128 MiB of HBM per device.

v0:
```python
import jax
import jax.numpy as jnp
from jax import lax
from jax.experimental import pallas as pl
from jax.experimental.pallas import tpu as pltpu
from jax.sharding import Mesh
from jax.sharding import PartitionSpec as P


REP, ZLO, X, Y, CORE = "rep", "fs_0", "fs_1", "tp_0", "tp_1"
TP = (Y, CORE)
FS = (ZLO, X)
REP_FS = (REP, ZLO, X)
RING = 4
BF16 = jnp.bfloat16
F32 = jnp.float32
LANES = 128

epsilon = 1e-06


def shift(value, axes, size, by):
    return lax.ppermute(value, axes, [(i, (i + by) % size) for i in range(size)])


def shift_x(value, by):
    return shift(value, X, RING, by)


def shift_y(value, by):
    return shift(value, Y, RING, by)


def swap_core(value):
    return shift(value, CORE, 2, 1)


def shift_apart(value, axes, size, by):
    pairs = [(2 * i + c, 2 * ((i + by * (1 - 2 * c)) % size) + c) for i in range(size) for c in range(2)]
    return lax.ppermute(value, (*axes, CORE), pairs)


def gather_ring(value, axes, size):
    first = shift_apart(value, axes, size, 1)
    second = shift_apart(value, axes, size, -1)
    return [value, first, second, shift_apart(first, axes, size, 1)]


def gather_z(block):
    return gather_ring(block, (REP, ZLO), 2 * RING)


def order_before(core):
    return 0, 1 + 2 * core, RING - 1 - 2 * core, 2


def order_z(core):
    return 0, RING - 1 - 2 * core, 1 + 2 * core, 2


def trade(value, flip):
    pairs = [
        (2 * i + c, 2 * (2 * c + (i % 2 if not flip else 1 - i % 2)) + i // 2)
        for i in range(RING)
        for c in range(2)
    ]
    return lax.ppermute(value, (X, CORE), pairs)


def kernel_call(body, outs, flops=0, scratch=(), hbm_in=(), hbm_out=(), limit=16):
    def run(*args):
        def spec(at, where):
            return pl.BlockSpec(memory_space=pltpu.HBM if at in where else pltpu.VMEM)

        return pl.pallas_call(
            body,
            out_shape=[jax.ShapeDtypeStruct(*out) for out in outs],
            in_specs=[spec(i, hbm_in) for i in range(len(args))],
            out_specs=[spec(i, hbm_out) for i in range(len(outs))],
            scratch_shapes=list(scratch),
            cost_estimate=pl.CostEstimate(flops=flops, bytes_accessed=0, transcendentals=0),
            compiler_params=pltpu.CompilerParams(vmem_limit_bytes=limit << 20),
        )(*args)

    return run


def place():
    return tuple(lax.axis_index(axis) for axis in (ZLO, X, Y, CORE))


def aligned(start, size):
    return pl.ds(pl.multiple_of(start, size), size)


def dot(left, right):
    return jnp.dot(left, right, preferred_element_type=F32)


def dot_t(left, right):
    return lax.dot_general(left, right, (((1,), (1,)), ((), ())), preferred_element_type=F32)


def two_parts(values):
    high = values.astype(BF16)
    return high, (values - high.astype(F32)).astype(BF16)


def gelu_exact(values):
    return 0.5 * values * (1.0 + lax.erf(values * (0.5**0.5)))


def rms(values, gain):
    return values * lax.rsqrt(jnp.mean(values * values, axis=-1, keepdims=True) + epsilon) * gain


def body(
    tokens,
    mixer_gain,
    gate_proj,
    value_proj,
    value_gain,
    spatial_mix,
    spatial_bias,
    head_gain,
    merge_proj,
    ffn_gain,
    gate_up,
    value_up,
    gate_kernel,
    value_kernel,
    gate_offset,
    value_offset,
    down_proj,
):
    length, features = tokens.shape
    heads, rows, _ = spatial_mix.shape
    part, width = gate_proj.shape
    inner = gate_up.shape[1]
    full = mixer_gain.shape[0]
    half = length // 2
    span = RING * part
    all_rows = RING * length
    own_rows = 2 * length
    padded = -(-inner // LANES) * LANES
    extra_rows = heads * rows
    pack_rows = 3 * part + extra_rows

    def turn(x, xs):
        return (x - xs) % RING

    gains = jnp.stack([mixer_gain, ffn_gain]).reshape(-1, part)

    def move(*moves):
        *pairs, sems = moves
        copies = [pltpu.make_async_copy(a, b, sems.at[i]) for i, (a, b) in enumerate(pairs)]
        for copy in copies:
            copy.start()
        for copy in copies:
            copy.wait()

    def entry_body(tokens, gate, value, merge, spatial, near, far, pack, sems):
        x = place()[1]
        move(
            (tokens.at[:, aligned(part * (x % 2), part)], near),
            (tokens.at[:, aligned(part * (1 - x % 2), part)], far),
            (gate, pack.at[0:part]),
            (value, pack.at[part : 2 * part]),
            (merge, pack.at[2 * part : 3 * part]),
            (spatial, pack.at[3 * part : pack_rows, 0:LANES]),
            sems,
        )

    piece = ((length, part), BF16)
    near, far, pack = kernel_call(
        entry_body,
        [piece, piece, ((pack_rows, part), BF16)],
        scratch=[pltpu.SemaphoreType.DMA((6,))],
        hbm_in=range(5),
        limit=62,
    )(tokens, gate_proj, value_proj, merge_proj, spatial_mix.reshape(extra_rows, length))
    near, far = trade(near, False), trade(far, True)

    packs = gather_z(pack)

    def join_body(gate, value, out, both, sems):
        move((gate, both.at[0:inner]), (value, both.at[inner : 2 * inner]), sems)
        move((both, out), sems)

    (up,) = kernel_call(
        join_body,
        [((2 * inner, part), BF16)],
        scratch=[pltpu.VMEM((2 * inner, part), BF16), pltpu.SemaphoreType.DMA((2,))],
        hbm_in=range(2),
        hbm_out=range(1),
        limit=62,
    )(gate_up.T, value_up.T)
    ups = gather_z(up)
    downs = gather_z(down_proj)

    def column_body(near, far, out):
        out[0:length] = near[...]
        out[length:] = far[...]

    (column,) = kernel_call(column_body, [((own_rows, part), BF16)])(near, far)
    columns = gather_ring(column, (Y,), RING)

    def stack_body(*refs):
        for k in range(RING):
            refs[RING][k] = refs[k][...]

    (own,) = kernel_call(stack_body, [((RING, own_rows, part), BF16)])(*columns)
    other = swap_core(own)

    def project_body(*refs):
        own, other, weights = refs[0], refs[1], refs[2:6]
        gain, raw, pays = refs[6], refs[7], refs[8:12]
        z, x, y, core = place()
        for side, blocks in ((core, own), (1 - core, other)):
            for n, k in enumerate(order_before(side)):
                j = (y - z - k) % RING
                for i in range(2):
                    xs = 2 * side + (x + i) % 2
                    raw[j, aligned(length * turn(x, xs), length), :] = blocks[
                        n, i * length : (i + 1) * length
                    ]
        squares = jnp.zeros((all_rows, 1), F32)
        gate = jnp.zeros((all_rows, width), F32)
        value = jnp.zeros((all_rows, width), F32)
        for j, weight in zip(order_z(core), weights):
            block = raw[j].astype(F32)
            squares = squares + jnp.sum(block * block, axis=1, keepdims=True)
            at = RING * ((z + j) % RING) + x
            scaled = (block * gain[pl.ds(at, 1), :]).astype(BF16)
            gate = gate + dot(scaled, weight[0:part])
            value = value + dot(scaled, weight[part : 2 * part])
        for t in range(RING):
            at = slice(t * length, (t + 1) * length)
            pays[t][:, :width] = gate[at].astype(BF16)
            pays[t][:, width : 2 * width] = value[at].astype(BF16)
            for j in range(RING):
                pays[t][extra_rows * j : extra_rows * (j + 1), 2 * width :] = weights[j][
                    3 * part :, :LANES
                ]
            row = jnp.broadcast_to(squares[at], (length, length)).T
            high, low = two_parts(row)
            base = RING * extra_rows
            pays[t][base : base + 16, 2 * width :] = high[:16]
            pays[t][base + 16 : base + 32, 2 * width :] = low[:16]
            pays[t][base + 32 :, 2 * width :] = jnp.zeros((length - base - 32, LANES), BF16)

    pay_shape = ((length, 2 * width + LANES), BF16)
    raw, *pays = kernel_call(
        project_body,
        [((RING, all_rows, part), BF16)] + [pay_shape] * RING,
        flops=2 * all_rows * span * 2 * width,
    )(own, other, *packs, gains)
    pays = [pays[0]] + [shift_x(pays[t], -t) for t in range(1, RING)]

    def mix_body(*refs):
        pays, (value_gain, bias, head_gain), out, matrix = refs[0:4], refs[4:7], refs[7], refs[8]
        z, x, _, core = place()
        base = RING * extra_rows
        squares = jnp.zeros((1, length), F32)
        total = jnp.zeros((length, 2 * width), F32)
        for t in range(RING):
            total = total + pays[t][:, : 2 * width].astype(F32)
            squares = squares + pays[t][base : base + 16, 2 * width :].astype(F32)[0:1]
            squares = squares + pays[t][base + 16 : base + 32, 2 * width :].astype(F32)[0:1]
            for i, j in enumerate(order_z(core)):
                block = pays[t][extra_rows * i : extra_rows * (i + 1), 2 * width :].astype(F32)
                at = rows * (RING * ((z + j) % RING) + (x + t) % RING)
                for h in range(heads):
                    matrix[h, aligned(at, rows), :] = block[h * rows : (h + 1) * rows]
        scale = jnp.broadcast_to(lax.rsqrt(squares / full + epsilon), (length, length)).T
        for h in range(heads):
            at = slice(h * length, (h + 1) * length)
            gated = gelu_exact((total[:, at] * scale).astype(BF16).astype(F32))
            at = slice(width + h * length, width + (h + 1) * length)
            spread = gelu_exact((total[:, at] * scale).astype(BF16).astype(F32))
            spread = rms(spread, value_gain[h : h + 1, :]).astype(BF16)
            mixed = dot(matrix[h].astype(BF16), spread)
            mixed = mixed + jnp.broadcast_to(bias[h : h + 1, :], (length, length)).T
            joined = rms(gated * mixed, head_gain[h : h + 1, :])
            out[:, h * length : (h + 1) * length] = joined.astype(BF16)

    (merged,) = kernel_call(
        mix_body,
        [((length, width), BF16)],
        flops=1 << 22,
        scratch=[pltpu.VMEM((heads, length, length), F32)],
    )(*pays, value_gain, spatial_bias, head_gain)
    merges = gather_ring(merged, (X,), RING)

    def side_of(blocks, scratch, x, core, side):
        for t, block in zip(order_before(core), blocks):
            scratch[t] = block[...]
        return jnp.concatenate([scratch[turn(x, 2 * side + i)] for i in range(2)], 0)

    def merge_other_body(*refs):
        merges, weights, out, blocks = refs[0:4], refs[4:8], refs[8], refs[9]
        _, x, _, core = place()
        left = side_of(merges, blocks, x, core, 1 - core)
        for j, weight in zip(order_z(core), weights):
            out[:, aligned(j * part, part)] = dot(left, weight[2 * part : 3 * part]).astype(BF16)

    merge_flops = 2 * own_rows * width * span
    merge_scratch = pltpu.VMEM((RING, length, width), BF16)
    (other,) = kernel_call(
        merge_other_body, [((own_rows, span), BF16)], flops=merge_flops, scratch=[merge_scratch]
    )(*merges, *packs)
    received = swap_core(other)

    def merge_own_body(*refs):
        merges, weights, received, raw = refs[0:4], refs[4:8], refs[8], refs[9]
        keep, sends, total, blocks = refs[10], refs[11:14], refs[14], refs[15]
        _, x, y, core = place()
        left = side_of(merges, blocks, x, core, core)
        for j, weight in zip(order_z(core), weights):
            at = aligned(j * part, part)
            total[:, at] = dot(left, weight[2 * part : 3 * part]) + received[:, at].astype(F32)
        mine = aligned(half * y, half)
        tokens = aligned(length * turn(x, 2 * core + y // 2) + half * (y % 2), half)
        for j in range(RING):
            at = slice(j * part, (j + 1) * part)
            keep[:, at] = total[mine, at] + raw[j, tokens, :].astype(F32)
        for k in range(1, RING):
            sends[k - 1][...] = total[aligned(half * ((y + k) % RING), half), :].astype(BF16)

    keep, *sends = kernel_call(
        merge_own_body,
        [((half, span), F32)] + [((half, span), BF16)] * 3,
        flops=merge_flops,
        scratch=[pltpu.VMEM((own_rows, span), F32), merge_scratch],
    )(*merges, *packs, received, raw)
    sums = [shift_y(sends[k - 1], k) for k in range(1, RING)]

    def hidden_body(keep, first, second, third, out):
        total = keep[...] + first[...].astype(F32) + second[...].astype(F32)
        out[...] = (total + third[...].astype(F32)).astype(BF16)

    (hidden,) = kernel_call(hidden_body, [((half, span), BF16)])(keep, *sums)

    mine = gather_ring(hidden, (Y,), RING)
    (mine,) = kernel_call(stack_body, [((RING, half, span), BF16)])(*mine)
    theirs = swap_core(mine)

    spare = padded - inner

    def over_tiles(run):
        def step(n, carry):
            start = pl.multiple_of(n * part, part)
            run(pl.ds(start, part), pl.ds(pl.multiple_of(inner + start, 32), part))
            return carry

        lax.fori_loop(0, inner // part, step, 0)
        rest = inner // part * part
        run(slice(rest, inner), slice(inner + rest, 2 * inner))

    def up_dot(left, weights, last, at):
        split = (RING - 1) * part
        return dot_t(left[:, :split], weights[at]) + dot_t(left[:, split:], last[at])

    def load_body(gate, value, first, second, out, sems):
        move(
            (gate, out.at[0:inner, 0:part]),
            (value, out.at[inner : 2 * inner, 0:part]),
            (first, out.at[:, part : 2 * part]),
            (second, out.at[:, 2 * part : 3 * part]),
            sems,
        )

    load_sems = pltpu.SemaphoreType.DMA((RING,))
    (weights,) = kernel_call(
        load_body, [((2 * inner, 3 * part), BF16)], scratch=[load_sems], hbm_in=range(4)
    )(gate_up.T, value_up.T, ups[1], ups[2])

    def up_far_body(*refs):
        mine, theirs, gain, weights, last_in = refs[0:5]
        gate_out, value_out, scaled, parts, last, sem = refs[5:11]
        z, x, y, core = place()
        copy = pltpu.make_async_copy(last_in, last, sem.at[0])
        copy.start()
        lane = lax.broadcasted_iota(jnp.int32, (half, LANES), 1)
        for side, block in ((core, mine), (1 - core, theirs)):
            for n, k in enumerate(order_before(side)):
                ys = (y - k) % RING
                at = aligned(half * (ys % 2), half)
                t = turn(x, 2 * side + ys // 2)
                slot = jnp.where(t == 0, 3, jnp.where(t == 2, 0, (t + 1) // 2))
                squares = jnp.zeros((half, 1), F32)
                for i, j in enumerate(order_z(core)):
                    piece = block[n, :, aligned(j * part, part)].astype(F32)
                    squares = squares + jnp.sum(piece * piece, axis=1, keepdims=True)
                    row = gain[pl.ds(RING * (RING + (z + j) % RING) + x, 1), :]
                    scaled[slot, at, i * part : (i + 1) * part] = (piece * row).astype(BF16)
                high, low = two_parts(squares)
                high = jnp.broadcast_to(high.astype(F32), (half, LANES))
                low = jnp.broadcast_to(low.astype(F32), (half, LANES))
                parts[slot, at] = jnp.where(lane == 0, high, jnp.where(lane == 1, low, 0.0))
        copy.wait()

        def run(at, value_at):
            gate_out[:, at] = up_dot(scaled[0], weights, last, at).astype(BF16)
            value_out[:, at] = up_dot(scaled[0], weights, last, value_at).astype(BF16)

        over_tiles(run)
        gate_out[:, inner:] = parts[0, :, :spare].astype(BF16)

    up_flops = 2 * length * span * inner
    gate_shape, value_shape = (length, padded), (length, inner)
    gate_two, value_two, scaled, parts, last = kernel_call(
        up_far_body,
        [
            (gate_shape, BF16),
            (value_shape, BF16),
            ((RING, length, span), BF16),
            ((RING, length, LANES), F32),
            ((2 * inner, part), BF16),
        ],
        flops=2 * up_flops,
        scratch=[pltpu.SemaphoreType.DMA((1,))],
        hbm_in=range(4, 5),
        limit=24,
    )(mine, theirs, gains, weights, ups[3])
    gate_two = shift_x(gate_two, 1)
    value_two = shift_x(value_two, -1)

    def up_near_body(scaled, parts, weights, last, *outs):
        gate_out, value_out, gate_add, value_add, gate_own, value_own = outs
        left = scaled[1:RING].reshape((RING - 1) * length, span)

        def run(at, value_at):
            piece = up_dot(left, weights, last, at)
            gate_out[:, at] = piece[:length].astype(BF16)
            gate_add[:, at] = piece[length : 2 * length]
            gate_own[:, at] = piece[2 * length :]
            piece = up_dot(left, weights, last, value_at)
            value_add[:, at] = piece[:length]
            value_out[:, at] = piece[length : 2 * length].astype(BF16)
            value_own[:, at] = piece[2 * length :]

        over_tiles(run)
        gate_out[:, inner:] = parts[1, :, :spare].astype(BF16)
        gate_add[:, inner:] = parts[2, :, :spare]
        gate_own[:, inner:] = parts[3, :, :spare]

    gate_near, value_near, gate_add, value_add, gate_own, value_own = kernel_call(
        up_near_body,
        [(gate_shape, BF16), (value_shape, BF16)] + [(gate_shape, F32), (value_shape, F32)] * 2,
        flops=6 * up_flops,
        limit=24,
    )(scaled, parts, weights, last)
    gate_near = shift_x(gate_near, -1)
    value_near = shift_x(value_near, 1)

    def up_join_body(gate_two, value_two, gate_add, value_add, gate_out, value_out):
        def step(n, carry):
            at = aligned(n * 16, 16)
            gate_out[at] = (gate_two[at].astype(F32) + gate_add[at]).astype(BF16)
            value_out[at] = (value_two[at].astype(F32) + value_add[at]).astype(BF16)
            return carry

        lax.fori_loop(0, length // 16, step, 0)
        total = gate_two[:, inner:].astype(F32) + gate_add[:, inner:]
        high, low = two_parts(total[:, 0:1] + total[:, 1:2])
        gate_out[:, inner : inner + 1] = high
        gate_out[:, inner + 1 : inner + 2] = low

    gate_join, value_join = kernel_call(
        up_join_body, [(gate_shape, BF16), (value_shape, BF16)]
    )(gate_two, value_two, gate_add, value_add)
    gate_join = shift_x(gate_join, 1)
    value_join = shift_x(value_join, -1)

    def active_body(
        gate_own, gate_near, gate_join, value_own, value_near, value_join,
        gate_kernel, value_kernel, gate_offset, value_offset, out,
    ):
        gates, values = (gate_own, gate_near, gate_join), (value_own, value_near, value_join)
        squares = jnp.zeros((length, 1), F32)
        for ref in gates:
            squares = squares + ref[:, inner : inner + 1].astype(F32)
            squares = squares + ref[:, inner + 1 : inner + 2].astype(F32)
        scale = lax.rsqrt(squares / full + epsilon)

        def run(at, size):
            position = lax.broadcasted_iota(jnp.int32, (length, size), 0)

            def convolve(refs, kernel, offset):
                total = refs[0][:, at] + refs[1][:, at].astype(F32) + refs[2][:, at].astype(F32)
                pre = (total * scale).astype(BF16).astype(F32)
                before = jnp.where(position == 0, 0.0, pltpu.roll(pre, 1, 0))
                after = jnp.where(position == length - 1, 0.0, pltpu.roll(pre, length - 1, 0))
                taps = before * kernel[0:1, at] + pre * kernel[1:2, at] + after * kernel[2:3, at]
                return offset[:, at] + taps

            gate = convolve(gates, gate_kernel, gate_offset)
            value = convolve(values, value_kernel, value_offset)
            out[:, at] = (gelu_exact(gate) * value).astype(BF16)

        def step(n, carry):
            run(aligned(n * LANES, LANES), LANES)
            return carry

        lax.fori_loop(0, inner // LANES, step, 0)
        rest = inner // LANES * LANES
        run(slice(rest, inner), inner - rest)

    (active,) = kernel_call(active_body, [((length, inner), BF16)], flops=1 << 24)(
        gate_own, gate_near, gate_join, value_own, value_near, value_join,
        gate_kernel, value_kernel, gate_offset[None], value_offset[None],
    )
    actives = gather_ring(active, (X,), RING)

    def down_load_body(*refs):
        order = order_z(place()[3])
        move(*((refs[i], refs[RING].at[j]) for i, j in enumerate(order)), refs[RING + 1])

    (weights,) = kernel_call(
        down_load_body, [((RING, inner, part), BF16)], scratch=[load_sems], hbm_in=range(4)
    )(*downs)


    def down_body(side_is_own):
        def run(*refs):
            actives, weights, out, blocks, left = refs[0:4], refs[4], refs[5], refs[6], refs[7]
            _, x, _, core = place()
            left[...] = side_of(actives, blocks, x, core, core if side_is_own else 1 - core)

            def step(j, carry):
                out[j] = dot(left[...], weights[j]).astype(out.dtype)
                return carry

            lax.fori_loop(0, RING, step, 0, unroll=2)

        return kernel_call(
            run,
            [((RING, own_rows, part), F32 if side_is_own else BF16)],
            flops=2 * own_rows * inner * span,
            scratch=[pltpu.VMEM((RING, length, inner), BF16), pltpu.VMEM((own_rows, inner), BF16)],
        )

    (other,) = down_body(False)(*actives, weights)
    received = swap_core(other)
    (own,) = down_body(True)(*actives, weights)

    def down_add_body(*refs):
        own, received, mine, keep, sends = refs[0], refs[1], refs[2], refs[3], refs[4:7]
        z, _, y, core = place()
        at = (y - z) % RING
        for k in range(1, RING):
            j = (at + k) % RING
            sends[k - 1][...] = (own[j] + received[j].astype(F32)).astype(BF16)
        keep[...] = own[at] + received[at].astype(F32)
        for n, k in enumerate(order_before(core)):
            place_rows = aligned(half * ((y - k) % RING), half)
            for j in range(RING):

                @pl.when(at == j)
                def _():
                    piece = mine[n, :, j * part : (j + 1) * part].astype(F32)
                    keep[place_rows, :] = keep[place_rows, :] + piece

    block = (own_rows, part)
    keep, *sends = kernel_call(
        down_add_body, [(block, F32)] + [(block, BF16)] * 3, flops=1 << 20
    )(own, received, mine)
    sums = [shift_y(sends[k - 1], k) for k in range(1, RING)]

    def result_body(keep, first, second, third, near, far, total):
        x = place()[1]
        added = keep[...] + first[...].astype(F32) + second[...].astype(F32)
        total[...] = added + third[...].astype(F32)
        near[...] = total[aligned(length * (x % 2), length), :].astype(BF16)
        far[...] = total[aligned(length * (1 - x % 2), length), :].astype(BF16)

    near, far = kernel_call(
        result_body, [piece, piece], scratch=[pltpu.VMEM(block, F32)]
    )(keep, *sums)

    near, far = trade(near, False), trade(far, True)

    def exit_body(near, far, out, sems):
        x = place()[1]
        move(
            (near, out.at[:, aligned(part * (x % 2), part)]),
            (far, out.at[:, aligned(part * (1 - x % 2), part)]),
            sems,
        )

    (out,) = kernel_call(
        exit_body,
        [((length, features), BF16)],
        scratch=[pltpu.SemaphoreType.DMA((2,))],
        hbm_in=range(2),
        hbm_out=range(1),
    )(near, far)
    return out


def solution(mesh):
    finer = Mesh(
        mesh.devices.reshape(mesh.shape["rep"], RING, RING, RING, 2), (REP, ZLO, X, Y, CORE)
    )

    return jax.shard_map(
        body,
        mesh=finer,
        in_specs=(
            P(REP_FS, TP),
            P(),
            P(FS, TP),
            P(FS, TP),
            P(TP, None),
            P(TP, FS, None),
            P(TP, None),
            P(TP, None),
            P(TP, FS),
            P(),
            P(FS, TP),
            P(FS, TP),
            P(None, TP),
            P(None, TP),
            P(TP),
            P(TP),
            P(TP, FS),
        ),
        out_specs=P(REP_FS, TP),
        check_vma=False,
    )
```

profile of v0, /device:TPU:4, one launch (start us, length us, event | category | flops | bytes accessed | tf_op | source)
XLA Modules:
  0.0 178.9 jit_solution(3296913331606927805)
XLA Ops:
  0.0 2.4 %shard_map.172 = bf16[2752,256]{1,0:T(8,128)(2,1)} custom-call(bf16[1376,256]{1,0:T(8,128)(2,1)} %bitcast.5, bf16[1376,256]{1,0:T(8,128)(2,1)} %bitcast.7), custom_call_target="tpu_custom_call" | custom-call | tf_op jit(solution)/shard_map/pallas_call | solution.py:75
  2.5 2.0 %collective-permute-start.23 = (bf16[2752,256]{1,0:T(8,128)(2,1)}, bf16[2752,256]{1,0:T(8,128)(2,1)S(1)}, u32[]{:S(2)}, u32[]{:S(2)}) collective-permute-start(bf16[2752,256]{1,0:T(8,128)(2,1)} %shard_map.172), channel_id=1, source_target_pairs={{0,32},{1,225},{32,64},{33,1},{64,96},{65,33},{96,128},{97,65},{12... | collective-permute-start | bytes 4227080 | tf_op jit(solution)/shard_map/ppermute | solution.py:40
  4.4 2.0 %shard_map.163 = (bf16[128,256]{1,0:T(8,128)(2,1)}, bf16[128,256]{1,0:T(8,128)(2,1)}, bf16[784,256]{1,0:T(8,128)(2,1)}) custom-call(bf16[128,512]{1,0:T(8,128)(2,1)} %tokens.1, bf16[256,256]{1,0:T(8,128)(2,1)} %gate.1, bf16[256,256]{1,0:T(8,128)(2,1)} %value.1, bf16[256,256]{1,0:T(8,128)(2,1)} %merge.1, bf16[16,128]{1,0:T(8,128)(2,1)} %bitcast.11), custom_call_target="tpu_custom_call" | custom-call | tf_op jit(solution)/shard_map/pallas_call | solution.py:75
  6.4 5.6 %collective-permute-start = (bf16[128,256]{1,0:T(8,128)(2,1)}, bf16[128,256]{1,0:T(8,128)(2,1)S(1)}, u32[]{:S(2)}, u32[]{:S(2)}) collective-permute-start(bf16[128,256]{1,0:T(8,128)(2,1)} %get-tuple-element.36), channel_id=1, source_target_pairs={{0,0},{1,16},{8,8},{9,24},{16,1},{17,17},{24,9},{25,25},{2,2},{3,1... | collective-permute-start | bytes 196616 | tf_op jit(solution)/shard_map/ppermute | solution.py:67
  12.9 1.7 collective-permute-done.near
  14.6 1.5 collective-permute-done.1.far
  16.1 1.7 collective-permute-start.2
  17.7 1.7 collective-permute-start.3
  19.4 3.5 %collective-permute-done.2.refs_1_ = bf16[256,256]{1,0:T(8,128)(2,1)S(1)} collective-permute-done((bf16[256,256]{1,0:T(8,128)(2,1)S(1)}, bf16[256,256]{1,0:T(8,128)(2,1)S(1)}, u32[]{:S(2)}, u32[]{:S(2)}) %collective-permute-start.2) | collective-permute-done | bytes 131104 | tf_op jit(solution)/shard_map/ppermute | solution.py:40
  23.7 5.4 %collective-permute-done.4.refs_3_ = bf16[256,256]{1,0:T(8,128)(2,1)S(1)} collective-permute-done((bf16[256,256]{1,0:T(8,128)(2,1)S(1)}, bf16[256,256]{1,0:T(8,128)(2,1)S(1)}, u32[]{:S(2)}, u32[]{:S(2)}) %collective-permute-start.4) | collective-permute-done | bytes 131104 | tf_op jit(solution)/shard_map/ppermute | solution.py:40
  29.2 2.6 %collective-permute-start.7 = (bf16[784,256]{1,0:T(8,128)(2,1)}, bf16[784,256]{1,0:T(8,128)(2,1)S(1)}, u32[]{:S(2)}, u32[]{:S(2)}) collective-permute-start(bf16[784,256]{1,0:T(8,128)(2,1)} %get-tuple-element.38.refs_2_.refs_4_), channel_id=1, source_target_pairs={{0,224},{1,33},{32,0},{33,65},{64,32},{65,97},{96,64},{97,129},{12... | collective-permute-start | bytes 1204232 | tf_op jit(solution)/shard_map/ppermute | solution.py:40
  31.8 1.4 pad_maximum_fusion
  34.6 6.8 %collective-permute-done.7.refs_4_.refs_6_ = bf16[784,256]{1,0:T(8,128)(2,1)S(1)} collective-permute-done((bf16[784,256]{1,0:T(8,128)(2,1)}, bf16[784,256]{1,0:T(8,128)(2,1)S(1)}, u32[]{:S(2)}, u32[]{:S(2)}) %collective-permute-start.7) | collective-permute-done | bytes 401440 | tf_op jit(solution)/shard_map/ppermute | solution.py:40
  43.1 1.9 %shard_map.166 = (bf16[4,512,256]{2,1,0:T(8,128)(2,1)S(1)}, bf16[128,640]{1,0:T(8,128)(2,1)S(1)}, bf16[128,640]{1,0:T(8,128)(2,1)S(1)}, bf16[128,640]{1,0:T(8,128)(2,1)S(1)}, bf16[128,640]{1,0:T(8,128)(2,1)S(1)}) custom-call(bf16[4,256,256]{2,1,0:T(8,128)(2,1)S(1)} %shard_map.165.refs_0_, bf16[4,256,256]{2,1,0:T(8,128)(2,1)} %collective-permute-done.5.refs_1_, ...), custom_call_target="tpu_custom_call" | custom-call | flops 536870912 | tf_op jit(solution)/shard_map/pallas_call | solution.py:75
  45.0 3.4 %collective-permute-start.11 = (bf16[128,640]{1,0:T(8,128)(2,1)S(1)}, bf16[128,640]{1,0:T(8,128)(2,1)S(1)}, u32[]{:S(2)}, u32[]{:S(2)}) collective-permute-start(bf16[128,640]{1,0:T(8,128)(2,1)S(1)} %get-tuple-element.42), channel_id=1, source_target_pairs={{0,8},{8,16},{16,24},{24,0},{1,9},{9,17},{17,25},{25,1},{2,10},{10... | collective-permute-start | bytes 491528 | tf_op jit(solution)/shard_map/ppermute | solution.py:23
  49.9 3.5 %collective-permute-done.10.refs_2_ = bf16[128,640]{1,0:T(8,128)(2,1)S(1)} collective-permute-done((bf16[128,640]{1,0:T(8,128)(2,1)S(1)}, bf16[128,640]{1,0:T(8,128)(2,1)S(1)}, u32[]{:S(2)}, u32[]{:S(2)}) %collective-permute-start.10) | collective-permute-done | bytes 163872 | tf_op jit(solution)/shard_map/ppermute | solution.py:23
  53.3 1.7 collective-permute-done.11.refs_3_
  55.6 3.3 %collective-permute-start.12 = (bf16[128,256]{1,0:T(8,128)(2,1)S(1)}, bf16[128,256]{1,0:T(8,128)(2,1)S(1)}, u32[]{:S(2)}, u32[]{:S(2)}) collective-permute-start(bf16[128,256]{1,0:T(8,128)(2,1)S(1)} %shard_map.167.refs_0_), channel_id=1, source_target_pairs={{0,8},{1,25},{8,16},{9,1},{16,24},{17,9},{24,0},{25,17},{2,10},{3,... | collective-permute-start | bytes 196616 | tf_op jit(solution)/shard_map/ppermute | solution.py:40
  58.9 1.9 %collective-permute-done.12.refs_1_ = bf16[128,256]{1,0:T(8,128)(2,1)S(1)} collective-permute-done((bf16[128,256]{1,0:T(8,128)(2,1)S(1)}, bf16[128,256]{1,0:T(8,128)(2,1)S(1)}, u32[]{:S(2)}, u32[]{:S(2)}) %collective-permute-start.12) | collective-permute-done | bytes 65568 | tf_op jit(solution)/shard_map/ppermute | solution.py:40
  60.8 2.4 %collective-permute-start.14 = (bf16[128,256]{1,0:T(8,128)(2,1)S(1)}, bf16[128,256]{1,0:T(8,128)(2,1)S(1)}, u32[]{:S(2)}, u32[]{:S(2)}) collective-permute-start(bf16[128,256]{1,0:T(8,128)(2,1)S(1)} %collective-permute-done.12.refs_1_), channel_id=1, source_target_pairs={{0,8},{1,25},{8,16},{9,1},{16,24},{17,9},{24,0},{25,17},{2,10},{3,... | collective-permute-start | bytes 196616 | tf_op jit(solution)/shard_map/ppermute | solution.py:40
  63.2 1.9 %collective-permute-done.14.refs_3_ = bf16[128,256]{1,0:T(8,128)(2,1)S(1)} collective-permute-done((bf16[128,256]{1,0:T(8,128)(2,1)S(1)}, bf16[128,256]{1,0:T(8,128)(2,1)S(1)}, u32[]{:S(2)}, u32[]{:S(2)}) %collective-permute-start.14) | collective-permute-done | bytes 65568 | tf_op jit(solution)/shard_map/ppermute | solution.py:40
  65.5 2.9 %collective-permute-start.24 = (bf16[2752,256]{1,0:T(8,128)(2,1)S(1)}, bf16[2752,256]{1,0:T(8,128)(2,1)S(1)}, u32[]{:S(2)}, u32[]{:S(2)}) collective-permute-start(bf16[2752,256]{1,0:T(8,128)(2,1)S(1)} %copy-done.11), channel_id=1, source_target_pairs={{0,224},{1,33},{32,0},{33,65},{64,32},{65,97},{96,64},{97,129},{12... | collective-permute-start | bytes 4227080 | tf_op jit(solution)/shard_map/ppermute | solution.py:40
  68.9 2.3 %collective-permute-start.17 = (bf16[64,1024]{1,0:T(8,128)(2,1)S(1)}, bf16[64,1024]{1,0:T(8,128)(2,1)S(1)}, u32[]{:S(2)}, u32[]{:S(2)}) collective-permute-start(bf16[64,1024]{1,0:T(8,128)(2,1)S(1)} %get-tuple-element.46), channel_id=1, source_target_pairs={{0,4},{2,6},{4,0},{6,2},{1,5},{3,7},{5,1},{7,3},{8,12},{10,14},{12... | collective-permute-start | bytes 393224 | tf_op jit(solution)/shard_map/ppermute | solution.py:23
  72.1 6.5 %collective-permute-done.16.first = bf16[64,1024]{1,0:T(8,128)(2,1)S(1)} collective-permute-done((bf16[64,1024]{1,0:T(8,128)(2,1)S(1)}, bf16[64,1024]{1,0:T(8,128)(2,1)S(1)}, u32[]{:S(2)}, u32[]{:S(2)}) %collective-permute-start.16) | collective-permute-done | bytes 131104 | tf_op jit(solution)/shard_map/ppermute | solution.py:23
  79.6 3.0 %collective-permute-start.20 = (bf16[64,1024]{1,0:T(8,128)(2,1)S(1)}, bf16[64,1024]{1,0:T(8,128)(2,1)S(1)}, u32[]{:S(2)}, u32[]{:S(2)}) collective-permute-start(bf16[64,1024]{1,0:T(8,128)(2,1)S(1)} %shard_map.170.refs_0_), channel_id=1, source_target_pairs={{0,6},{1,3},{2,0},{3,5},{4,2},{5,7},{6,4},{7,1},{8,14},{9,11},{10,... | collective-permute-start | bytes 393224 | tf_op jit(solution)/shard_map/ppermute | solution.py:40
  82.6 3.5 %collective-permute-done.19.refs_1_ = bf16[64,1024]{1,0:T(8,128)(2,1)S(1)} collective-permute-done((bf16[64,1024]{1,0:T(8,128)(2,1)S(1)}, bf16[64,1024]{1,0:T(8,128)(2,1)S(1)}, u32[]{:S(2)}, u32[]{:S(2)}) %collective-permute-start.19) | collective-permute-done | bytes 131104 | tf_op jit(solution)/shard_map/ppermute | solution.py:40
  86.1 6.2 %collective-permute-done.21.refs_3_ = bf16[64,1024]{1,0:T(8,128)(2,1)S(1)} collective-permute-done((bf16[64,1024]{1,0:T(8,128)(2,1)S(1)}, bf16[64,1024]{1,0:T(8,128)(2,1)S(1)}, u32[]{:S(2)}, u32[]{:S(2)}) %collective-permute-start.21) | collective-permute-done | bytes 131104 | tf_op jit(solution)/shard_map/ppermute | solution.py:40
  92.4 6.8 %collective-permute-done.24.second = bf16[2752,256]{1,0:T(8,128)(2,1)S(1)} collective-permute-done((bf16[2752,256]{1,0:T(8,128)(2,1)S(1)}, bf16[2752,256]{1,0:T(8,128)(2,1)S(1)}, u32[]{:S(2)}, u32[]{:S(2)}) %collective-permute-start.24) | collective-permute-done | bytes 1409056 | tf_op jit(solution)/shard_map/ppermute | solution.py:40
  100.0 3.4 %shard_map.174 = (bf16[128,1408]{1,0:T(8,128)(2,1)S(1)}, bf16[128,1376]{1,0:T(8,128)(2,1)S(1)}, bf16[4,128,1024]{2,1,0:T(8,128)(2,1)S(1)}, f32[4,128,128]{2,1,0:T(8,128)S(1)}, bf16[2752,256]{1,0:T(8,128)(2,1)S(1)}) custom-call(bf16[4,64,1024]{2,1,0:T(8,128)(2,1)S(1)} %shard_map.171.refs_0_.refs_2_, bf16[4,64,1024]{2,1,0:T(8,128)(2,1)S(1)} %collective-permute-done.22.refs_1_, ...), custom_call_target="tpu_custom_call" | custom-call | flops 721420288 | tf_op jit(solution)/shard_map/pallas_call | solution.py:75
  103.3 2.4 %collective-permute-start.27 = (bf16[128,1408]{1,0:T(8,128)(2,1)S(1)}, bf16[128,1408]{1,0:T(8,128)(2,1)S(1)}, u32[]{:S(2)}, u32[]{:S(2)}) collective-permute-start(bf16[128,1408]{1,0:T(8,128)(2,1)S(1)} %get-tuple-element.53), channel_id=1, source_target_pairs={{0,8},{8,16},{16,24},{24,0},{1,9},{9,17},{17,25},{25,1},{2,10},{10... | collective-permute-start | bytes 1081352 | tf_op jit(solution)/shard_map/ppermute | solution.py:23
  105.8 3.7 %shard_map.175 = (bf16[128,1408]{1,0:T(8,128)(2,1)S(1)}, bf16[128,1376]{1,0:T(8,128)(2,1)S(1)}, f32[128,1408]{1,0:T(8,128)S(1)}, f32[128,1376]{1,0:T(8,128)S(1)}...) custom-call(bf16[4,128,1024]{2,1,0:T(8,128)(2,1)S(1)} %get-tuple-element.48.scaled, ...), custom_call_target="tpu_custom_call" | custom-call | flops 2164260864 | tf_op jit(solution)/shard_map/pallas_call | solution.py:75
  109.6 2.9 %collective-permute-start.26 = (bf16[128,1408]{1,0:T(8,128)(2,1)S(1)}, bf16[128,1408]{1,0:T(8,128)(2,1)S(1)}, u32[]{:S(2)}, u32[]{:S(2)}) collective-permute-start(bf16[128,1408]{1,0:T(8,128)(2,1)S(1)} %get-tuple-element.52), channel_id=1, source_target_pairs={{0,24},{8,0},{16,8},{24,16},{1,25},{9,1},{17,9},{25,17},{2,26},{10... | collective-permute-start | bytes 1081352 | tf_op jit(solution)/shard_map/ppermute | solution.py:23
  112.5 4.3 %collective-permute-done.28.value_two = bf16[128,1376]{1,0:T(8,128)(2,1)S(1)} collective-permute-done((bf16[128,1376]{1,0:T(8,128)(2,1)S(1)}, bf16[128,1376]{1,0:T(8,128)(2,1)S(1)}, u32[]{:S(2)}, u32[]{:S(2)}) %collective-permute-start.28) | collective-permute-done | bytes 352288 | tf_op jit(solution)/shard_map/ppermute | solution.py:23
  117.1 3.0 %collective-permute-start.29 = (bf16[128,1408]{1,0:T(8,128)(2,1)S(1)}, bf16[128,1408]{1,0:T(8,128)(2,1)S(1)}, u32[]{:S(2)}, u32[]{:S(2)}) collective-permute-start(bf16[128,1408]{1,0:T(8,128)(2,1)S(1)} %get-tuple-element.57), channel_id=1, source_target_pairs={{0,8},{8,16},{16,24},{24,0},{1,9},{9,17},{17,25},{25,1},{2,10},{10... | collective-permute-start | bytes 1081352 | tf_op jit(solution)/shard_map/ppermute | solution.py:23
  120.2 1.9 %collective-permute-start.31 = (bf16[128,1376]{1,0:T(8,128)(2,1)S(1)}, bf16[128,1376]{1,0:T(8,128)(2,1)S(1)}, u32[]{:S(2)}, u32[]{:S(2)}) collective-permute-start(bf16[128,1376]{1,0:T(8,128)(2,1)S(1)} %get-tuple-element.60), channel_id=1, source_target_pairs={{0,24},{8,0},{16,8},{24,16},{1,25},{9,1},{17,9},{25,17},{2,26},{10... | collective-permute-start | bytes 1056776 | tf_op jit(solution)/shard_map/ppermute | solution.py:23
  122.2 5.1 %collective-permute-start.36 = (bf16[1376,256]{1,0:T(8,128)(2,1)S(1)}, bf16[1376,256]{1,0:T(8,128)(2,1)S(1)}, u32[]{:S(2)}, u32[]{:S(2)}) collective-permute-start(bf16[1376,256]{1,0:T(8,128)(2,1)S(1)} %copy-done.3), channel_id=1, source_target_pairs={{0,224},{1,33},{32,0},{33,65},{64,32},{65,97},{96,64},{97,129},{12... | collective-permute-start | bytes 2113544 | tf_op jit(solution)/shard_map/ppermute | solution.py:40
  127.3 6.9 %collective-permute-done.30.value_near = bf16[128,1376]{1,0:T(8,128)(2,1)S(1)} collective-permute-done((bf16[128,1376]{1,0:T(8,128)(2,1)S(1)}, bf16[128,1376]{1,0:T(8,128)(2,1)S(1)}, u32[]{:S(2)}, u32[]{:S(2)}) %collective-permute-start.30) | collective-permute-done | bytes 352288 | tf_op jit(solution)/shard_map/ppermute | solution.py:23
  134.3 1.7 shard_map.177.refs_0_
  136.0 2.0 %collective-permute-start.32 = (bf16[128,1376]{1,0:T(8,128)(2,1)S(1)}, bf16[128,1376]{1,0:T(8,128)(2,1)S(1)}, u32[]{:S(2)}, u32[]{:S(2)}) collective-permute-start(bf16[128,1376]{1,0:T(8,128)(2,1)S(1)} %shard_map.177.refs_0_), channel_id=1, source_target_pairs={{0,8},{1,25},{8,16},{9,1},{16,24},{17,9},{24,0},{25,17},{2,10},{3,... | collective-permute-start | bytes 1056776 | tf_op jit(solution)/shard_map/ppermute | solution.py:40
  138.1 8.7 %collective-permute-done.32.refs_1_ = bf16[128,1376]{1,0:T(8,128)(2,1)S(1)} collective-permute-done((bf16[128,1376]{1,0:T(8,128)(2,1)S(1)}, bf16[128,1376]{1,0:T(8,128)(2,1)S(1)}, u32[]{:S(2)}, u32[]{:S(2)}) %collective-permute-start.32) | collective-permute-done | bytes 352288 | tf_op jit(solution)/shard_map/ppermute | solution.py:40
  146.8 1.9 %collective-permute-start.34 = (bf16[128,1376]{1,0:T(8,128)(2,1)S(1)}, bf16[128,1376]{1,0:T(8,128)(2,1)S(1)}, u32[]{:S(2)}, u32[]{:S(2)}) collective-permute-start(bf16[128,1376]{1,0:T(8,128)(2,1)S(1)} %collective-permute-done.32.refs_1_), channel_id=1, source_target_pairs={{0,8},{1,25},{8,16},{9,1},{16,24},{17,9},{24,0},{25,17},{2,10},{3,... | collective-permute-start | bytes 1056776 | tf_op jit(solution)/shard_map/ppermute | solution.py:40
  149.8 4.4 %collective-permute-done.34.refs_3_ = bf16[128,1376]{1,0:T(8,128)(2,1)S(1)} collective-permute-done((bf16[128,1376]{1,0:T(8,128)(2,1)S(1)}, bf16[128,1376]{1,0:T(8,128)(2,1)S(1)}, u32[]{:S(2)}, u32[]{:S(2)}) %collective-permute-start.34) | collective-permute-done | bytes 352288 | tf_op jit(solution)/shard_map/ppermute | solution.py:40
  157.9 3.2 %collective-permute-start.40 = (bf16[256,256]{1,0:T(8,128)(2,1)S(1)}, bf16[256,256]{1,0:T(8,128)(2,1)S(1)}, u32[]{:S(2)}, u32[]{:S(2)}) collective-permute-start(bf16[256,256]{1,0:T(8,128)(2,1)S(1)} %get-tuple-element.63), channel_id=1, source_target_pairs={{0,4},{2,6},{4,0},{6,2},{1,5},{3,7},{5,1},{7,3},{8,12},{10,14},{12... | collective-permute-start | bytes 393224 | tf_op jit(solution)/shard_map/ppermute | solution.py:23
  161.1 4.3 %collective-permute-done.39.first = bf16[256,256]{1,0:T(8,128)(2,1)S(1)} collective-permute-done((bf16[256,256]{1,0:T(8,128)(2,1)S(1)}, bf16[256,256]{1,0:T(8,128)(2,1)S(1)}, u32[]{:S(2)}, u32[]{:S(2)}) %collective-permute-start.39) | collective-permute-done | bytes 131104 | tf_op jit(solution)/shard_map/ppermute | solution.py:23
  165.4 2.0 %collective-permute-done.40.second = bf16[256,256]{1,0:T(8,128)(2,1)S(1)} collective-permute-done((bf16[256,256]{1,0:T(8,128)(2,1)S(1)}, bf16[256,256]{1,0:T(8,128)(2,1)S(1)}, u32[]{:S(2)}, u32[]{:S(2)}) %collective-permute-start.40) | collective-permute-done | bytes 131104 | tf_op jit(solution)/shard_map/ppermute | solution.py:23
  168.1 6.1 %collective-permute-start.42 = (bf16[128,256]{1,0:T(8,128)(2,1)S(1)}, bf16[128,256]{1,0:T(8,128)(2,1)S(1)}, u32[]{:S(2)}, u32[]{:S(2)}) collective-permute-start(bf16[128,256]{1,0:T(8,128)(2,1)S(1)} %get-tuple-element.65), channel_id=1, source_target_pairs={{0,0},{1,16},{8,8},{9,24},{16,1},{17,17},{24,9},{25,25},{2,2},{3,1... | collective-permute-start | bytes 196616 | tf_op jit(solution)/shard_map/ppermute | solution.py:67
  174.4 2.0 %collective-permute-done.42.near = bf16[128,256]{1,0:T(8,128)(2,1)S(1)} collective-permute-done((bf16[128,256]{1,0:T(8,128)(2,1)S(1)}, bf16[128,256]{1,0:T(8,128)(2,1)S(1)}, u32[]{:S(2)}, u32[]{:S(2)}) %collective-permute-start.42) | collective-permute-done | bytes 65568 | tf_op jit(solution)/shard_map/ppermute | solution.py:67
  176.4 1.7 collective-permute-done.43.far
  (93 shorter events, 17.3 us)
Async XLA Ops:
  2.5 65.9 %collective-permute-start.23 = (bf16[2752,256]{1,0:T(8,128)(2,1)}, bf16[2752,256]{1,0:T(8,128)(2,1)S(1)}, u32[]{:S(2)}, u32[]{:S(2)}) collective-permute-start(bf16[2752,256]{1,0:T(8,128)(2,1)} %shard_map.172), channel_id=1, source_target_pairs={{0,32},{1,225},{32,64},{33,1},{64,96},{65,33},{96,128},{97,65},{12... | collective-permute-start | bytes 4227080 | tf_op jit(solution)/shard_map/ppermute | solution.py:40
  6.4 35.9 %copy-start = (bf16[784,256]{1,0:T(8,128)(2,1)S(1)}, bf16[784,256]{1,0:T(8,128)(2,1)}, u32[]{:S(2)}) copy-start(bf16[784,256]{1,0:T(8,128)(2,1)} %get-tuple-element.38.refs_2_.refs_4_) | copy-start | bytes 1204228
  6.4 8.2 %collective-permute-start = (bf16[128,256]{1,0:T(8,128)(2,1)}, bf16[128,256]{1,0:T(8,128)(2,1)S(1)}, u32[]{:S(2)}, u32[]{:S(2)}) collective-permute-start(bf16[128,256]{1,0:T(8,128)(2,1)} %get-tuple-element.36), channel_id=1, source_target_pairs={{0,0},{1,16},{8,8},{9,24},{16,1},{17,17},{24,9},{25,25},{2,2},{3,1... | collective-permute-start | bytes 196616 | tf_op jit(solution)/shard_map/ppermute | solution.py:67
  12.1 4.0 %collective-permute-start.1 = (bf16[128,256]{1,0:T(8,128)(2,1)}, bf16[128,256]{1,0:T(8,128)(2,1)S(1)}, u32[]{:S(2)}, u32[]{:S(2)}) collective-permute-start(bf16[128,256]{1,0:T(8,128)(2,1)} %get-tuple-element.37), channel_id=1, source_target_pairs={{0,8},{1,24},{8,0},{9,16},{16,9},{17,25},{24,1},{25,17},{2,10},{3,... | collective-permute-start | bytes 196616 | tf_op jit(solution)/shard_map/ppermute | solution.py:67
  12.2 19.6 %collective-permute-start.6 = (bf16[784,256]{1,0:T(8,128)(2,1)}, bf16[784,256]{1,0:T(8,128)(2,1)S(1)}, u32[]{:S(2)}, u32[]{:S(2)}) collective-permute-start(bf16[784,256]{1,0:T(8,128)(2,1)} %get-tuple-element.38.refs_2_.refs_4_), channel_id=1, source_target_pairs={{0,32},{1,225},{32,64},{33,1},{64,96},{65,33},{96,128},{97,65},{12... | collective-permute-start | bytes 1204232 | tf_op jit(solution)/shard_map/ppermute | solution.py:40
  16.1 6.8 %collective-permute-start.2 = (bf16[256,256]{1,0:T(8,128)(2,1)S(1)}, bf16[256,256]{1,0:T(8,128)(2,1)S(1)}, u32[]{:S(2)}, u32[]{:S(2)}) collective-permute-start(bf16[256,256]{1,0:T(8,128)(2,1)S(1)} %shard_map.164.refs_0_), channel_id=1, source_target_pairs={{0,2},{1,7},{2,4},{3,1},{4,6},{5,3},{6,0},{7,5},{8,10},{9,15},{10,... | collective-permute-start | bytes 393224 | tf_op jit(solution)/shard_map/ppermute | solution.py:40
  17.7 6.0 %collective-permute-start.3 = (bf16[256,256]{1,0:T(8,128)(2,1)S(1)}, bf16[256,256]{1,0:T(8,128)(2,1)S(1)}, u32[]{:S(2)}, u32[]{:S(2)}) collective-permute-start(bf16[256,256]{1,0:T(8,128)(2,1)S(1)} %shard_map.164.refs_0_), channel_id=1, source_target_pairs={{0,6},{1,3},{2,0},{3,5},{4,2},{5,7},{6,4},{7,1},{8,14},{9,11},{10,... | collective-permute-start | bytes 393224 | tf_op jit(solution)/shard_map/ppermute | solution.py:40
  22.9 6.2 %collective-permute-start.4 = (bf16[256,256]{1,0:T(8,128)(2,1)S(1)}, bf16[256,256]{1,0:T(8,128)(2,1)S(1)}, u32[]{:S(2)}, u32[]{:S(2)}) collective-permute-start(bf16[256,256]{1,0:T(8,128)(2,1)S(1)} %collective-permute-done.2.refs_1_), channel_id=1, source_target_pairs={{0,2},{1,7},{2,4},{3,1},{4,6},{5,3},{6,0},{7,5},{8,10},{9,15},{10,... | collective-permute-start | bytes 393224 | tf_op jit(solution)/shard_map/ppermute | solution.py:40
  29.1 13.2 %collective-permute-start.5 = (bf16[4,256,256]{2,1,0:T(8,128)(2,1)S(1)}, bf16[4,256,256]{2,1,0:T(8,128)(2,1)}, u32[]{:S(2)}, u32[]{:S(2)}) collective-permute-start(bf16[4,256,256]{2,1,0:T(8,128)(2,1)S(1)} %shard_map.165.refs_0_), channel_id=1, source_target_pairs={{0,1},{1,0},{2,3},{3,2},{4,5},{5,4},{6,7},{7,6},{8,9},{9,8},{10,11... | collective-permute-start | bytes 1572872 | tf_op jit(solution)/shard_map/ppermute | solution.py:23
  29.2 12.3 %collective-permute-start.7 = (bf16[784,256]{1,0:T(8,128)(2,1)}, bf16[784,256]{1,0:T(8,128)(2,1)S(1)}, u32[]{:S(2)}, u32[]{:S(2)}) collective-permute-start(bf16[784,256]{1,0:T(8,128)(2,1)} %get-tuple-element.38.refs_2_.refs_4_), channel_id=1, source_target_pairs={{0,224},{1,33},{32,0},{33,65},{64,32},{65,97},{96,64},{97,129},{12... | collective-permute-start | bytes 1204232 | tf_op jit(solution)/shard_map/ppermute | solution.py:40
  31.8 10.5 %collective-permute-start.8 = (bf16[784,256]{1,0:T(8,128)(2,1)S(1)}, bf16[784,256]{1,0:T(8,128)(2,1)S(1)}, u32[]{:S(2)}, u32[]{:S(2)}) collective-permute-start(bf16[784,256]{1,0:T(8,128)(2,1)S(1)} %collective-permute-done.6.refs_3_.refs_5_), channel_id=1, source_target_pairs={{0,32},{1,225},{32,64},{33,1},{64,96},{65,33},{96,128},{97,65},{12... | collective-permute-start | bytes 1204232 | tf_op jit(solution)/shard_map/ppermute | solution.py:40
  44.9 8.4 %collective-permute-start.10 = (bf16[128,640]{1,0:T(8,128)(2,1)S(1)}, bf16[128,640]{1,0:T(8,128)(2,1)S(1)}, u32[]{:S(2)}, u32[]{:S(2)}) collective-permute-start(bf16[128,640]{1,0:T(8,128)(2,1)S(1)} %get-tuple-element.41), channel_id=1, source_target_pairs={{0,16},{8,24},{16,0},{24,8},{1,17},{9,25},{17,1},{25,9},{2,18},{10... | collective-permute-start | bytes 491528 | tf_op jit(solution)/shard_map/ppermute | solution.py:23
  45.0 10.0 %collective-permute-start.11 = (bf16[128,640]{1,0:T(8,128)(2,1)S(1)}, bf16[128,640]{1,0:T(8,128)(2,1)S(1)}, u32[]{:S(2)}, u32[]{:S(2)}) collective-permute-start(bf16[128,640]{1,0:T(8,128)(2,1)S(1)} %get-tuple-element.42), channel_id=1, source_target_pairs={{0,8},{8,16},{16,24},{24,0},{1,9},{9,17},{17,25},{25,1},{2,10},{10... | collective-permute-start | bytes 491528 | tf_op jit(solution)/shard_map/ppermute | solution.py:23
  48.5 6.5 %collective-permute-start.9 = (bf16[128,640]{1,0:T(8,128)(2,1)S(1)}, bf16[128,640]{1,0:T(8,128)(2,1)S(1)}, u32[]{:S(2)}, u32[]{:S(2)}) collective-permute-start(bf16[128,640]{1,0:T(8,128)(2,1)S(1)} %get-tuple-element.40), channel_id=1, source_target_pairs={{0,24},{8,0},{16,8},{24,16},{1,25},{9,1},{17,9},{25,17},{2,26},{10... | collective-permute-start | bytes 491528 | tf_op jit(solution)/shard_map/ppermute | solution.py:23
  55.6 5.2 %collective-permute-start.12 = (bf16[128,256]{1,0:T(8,128)(2,1)S(1)}, bf16[128,256]{1,0:T(8,128)(2,1)S(1)}, u32[]{:S(2)}, u32[]{:S(2)}) collective-permute-start(bf16[128,256]{1,0:T(8,128)(2,1)S(1)} %shard_map.167.refs_0_), channel_id=1, source_target_pairs={{0,8},{1,25},{8,16},{9,1},{16,24},{17,9},{24,0},{25,17},{2,10},{3,... | collective-permute-start | bytes 196616 | tf_op jit(solution)/shard_map/ppermute | solution.py:40
  58.9 4.3 %collective-permute-start.13 = (bf16[128,256]{1,0:T(8,128)(2,1)S(1)}, bf16[128,256]{1,0:T(8,128)(2,1)S(1)}, u32[]{:S(2)}, u32[]{:S(2)}) collective-permute-start(bf16[128,256]{1,0:T(8,128)(2,1)S(1)} %shard_map.167.refs_0_), channel_id=1, source_target_pairs={{0,24},{1,9},{8,0},{9,17},{16,8},{17,25},{24,16},{25,1},{2,26},{3,... | collective-permute-start | bytes 196616 | tf_op jit(solution)/shard_map/ppermute | solution.py:40
  60.8 4.3 %collective-permute-start.14 = (bf16[128,256]{1,0:T(8,128)(2,1)S(1)}, bf16[128,256]{1,0:T(8,128)(2,1)S(1)}, u32[]{:S(2)}, u32[]{:S(2)}) collective-permute-start(bf16[128,256]{1,0:T(8,128)(2,1)S(1)} %collective-permute-done.12.refs_1_), channel_id=1, source_target_pairs={{0,8},{1,25},{8,16},{9,1},{16,24},{17,9},{24,0},{25,17},{2,10},{3,... | collective-permute-start | bytes 196616 | tf_op jit(solution)/shard_map/ppermute | solution.py:40
  65.4 3.0 %collective-permute-start.15 = (bf16[256,1024]{1,0:T(8,128)(2,1)S(1)}, bf16[256,1024]{1,0:T(8,128)(2,1)S(1)}, u32[]{:S(2)}, u32[]{:S(2)}) collective-permute-start(bf16[256,1024]{1,0:T(8,128)(2,1)S(1)} %shard_map.168), channel_id=1, source_target_pairs={{0,1},{1,0},{2,3},{3,2},{4,5},{5,4},{6,7},{7,6},{8,9},{9,8},{10,11... | collective-permute-start | bytes 1572872 | tf_op jit(solution)/shard_map/ppermute | solution.py:23
  65.5 33.8 %collective-permute-start.24 = (bf16[2752,256]{1,0:T(8,128)(2,1)S(1)}, bf16[2752,256]{1,0:T(8,128)(2,1)S(1)}, u32[]{:S(2)}, u32[]{:S(2)}) collective-permute-start(bf16[2752,256]{1,0:T(8,128)(2,1)S(1)} %copy-done.11), channel_id=1, source_target_pairs={{0,224},{1,33},{32,0},{33,65},{64,32},{65,97},{96,64},{97,129},{12... | collective-permute-start | bytes 4227080 | tf_op jit(solution)/shard_map/ppermute | solution.py:40
  68.3 31.6 %collective-permute-start.25 = (bf16[2752,256]{1,0:T(8,128)(2,1)S(1)}, bf16[2752,256]{1,0:T(8,128)(2,1)S(1)}, u32[]{:S(2)}, u32[]{:S(2)}) collective-permute-start(bf16[2752,256]{1,0:T(8,128)(2,1)S(1)} %collective-permute-done.23.first), channel_id=1, source_target_pairs={{0,32},{1,225},{32,64},{33,1},{64,96},{65,33},{96,128},{97,65},{12... | collective-permute-start | bytes 4227080 | tf_op jit(solution)/shard_map/ppermute | solution.py:40
  68.8 30.5 %copy-start.1 = (bf16[256,1376]{0,1:T(8,128)(2,1)S(1)}, bf16[256,1376]{0,1:T(8,128)(2,1)}, u32[]{:S(2)}) copy-start(bf16[256,1376]{0,1:T(8,128)(2,1)} %param.27) | copy-start | bytes 2113540
  68.8 30.5 %copy-start.2 = (bf16[256,1376]{0,1:T(8,128)(2,1)S(1)}, bf16[256,1376]{0,1:T(8,128)(2,1)}, u32[]{:S(2)}) copy-start(bf16[256,1376]{0,1:T(8,128)(2,1)} %param.28) | copy-start | bytes 2113540
  68.8 9.8 %collective-permute-start.16 = (bf16[64,1024]{1,0:T(8,128)(2,1)S(1)}, bf16[64,1024]{1,0:T(8,128)(2,1)S(1)}, u32[]{:S(2)}, u32[]{:S(2)}) collective-permute-start(bf16[64,1024]{1,0:T(8,128)(2,1)S(1)} %get-tuple-element.45), channel_id=1, source_target_pairs={{0,2},{2,4},{4,6},{6,0},{1,3},{3,5},{5,7},{7,1},{8,10},{10,12},{12... | collective-permute-start | bytes 393224 | tf_op jit(solution)/shard_map/ppermute | solution.py:23
  68.9 9.7 %collective-permute-start.17 = (bf16[64,1024]{1,0:T(8,128)(2,1)S(1)}, bf16[64,1024]{1,0:T(8,128)(2,1)S(1)}, u32[]{:S(2)}, u32[]{:S(2)}) collective-permute-start(bf16[64,1024]{1,0:T(8,128)(2,1)S(1)} %get-tuple-element.46), channel_id=1, source_target_pairs={{0,4},{2,6},{4,0},{6,2},{1,5},{3,7},{5,1},{7,3},{8,12},{10,14},{12... | collective-permute-start | bytes 393224 | tf_op jit(solution)/shard_map/ppermute | solution.py:23
  71.1 8.1 %collective-permute-start.18 = (bf16[64,1024]{1,0:T(8,128)(2,1)S(1)}, bf16[64,1024]{1,0:T(8,128)(2,1)S(1)}, u32[]{:S(2)}, u32[]{:S(2)}) collective-permute-start(bf16[64,1024]{1,0:T(8,128)(2,1)S(1)} %get-tuple-element.47), channel_id=1, source_target_pairs={{0,6},{2,0},{4,2},{6,4},{1,7},{3,1},{5,3},{7,5},{8,14},{10,8},{12,... | collective-permute-start | bytes 393224 | tf_op jit(solution)/shard_map/ppermute | solution.py:23
  79.3 6.8 %collective-permute-start.19 = (bf16[64,1024]{1,0:T(8,128)(2,1)S(1)}, bf16[64,1024]{1,0:T(8,128)(2,1)S(1)}, u32[]{:S(2)}, u32[]{:S(2)}) collective-permute-start(bf16[64,1024]{1,0:T(8,128)(2,1)S(1)} %shard_map.170.refs_0_), channel_id=1, source_target_pairs={{0,2},{1,7},{2,4},{3,1},{4,6},{5,3},{6,0},{7,5},{8,10},{9,15},{10,... | collective-permute-start | bytes 393224 | tf_op jit(solution)/shard_map/ppermute | solution.py:40
  79.6 6.5 %collective-permute-start.20 = (bf16[64,1024]{1,0:T(8,128)(2,1)S(1)}, bf16[64,1024]{1,0:T(8,128)(2,1)S(1)}, u32[]{:S(2)}, u32[]{:S(2)}) collective-permute-start(bf16[64,1024]{1,0:T(8,128)(2,1)S(1)} %shard_map.170.refs_0_), channel_id=1, source_target_pairs={{0,6},{1,3},{2,0},{3,5},{4,2},{5,7},{6,4},{7,1},{8,14},{9,11},{10,... | collective-permute-start | bytes 393224 | tf_op jit(solution)/shard_map/ppermute | solution.py:40
  86.1 6.2 %collective-permute-start.21 = (bf16[64,1024]{1,0:T(8,128)(2,1)S(1)}, bf16[64,1024]{1,0:T(8,128)(2,1)S(1)}, u32[]{:S(2)}, u32[]{:S(2)}) collective-permute-start(bf16[64,1024]{1,0:T(8,128)(2,1)S(1)} %collective-permute-done.19.refs_1_), channel_id=1, source_target_pairs={{0,2},{1,7},{2,4},{3,1},{4,6},{5,3},{6,0},{7,5},{8,10},{9,15},{10,... | collective-permute-start | bytes 393224 | tf_op jit(solution)/shard_map/ppermute | solution.py:40
  92.3 7.2 %collective-permute-start.22 = (bf16[4,64,1024]{2,1,0:T(8,128)(2,1)S(1)}, bf16[4,64,1024]{2,1,0:T(8,128)(2,1)S(1)}, u32[]{:S(2)}, u32[]{:S(2)}) collective-permute-start(bf16[4,64,1024]{2,1,0:T(8,128)(2,1)S(1)} %shard_map.171.refs_0_.refs_2_), channel_id=1, source_target_pairs={{0,1},{1,0},{2,3},{3,2},{4,5},{5,4},{6,7},{7,6},{8,9},{9,8},{10,11... | collective-permute-start | bytes 1572872 | tf_op jit(solution)/shard_map/ppermute | solution.py:23
  103.3 13.4 %collective-permute-start.27 = (bf16[128,1408]{1,0:T(8,128)(2,1)S(1)}, bf16[128,1408]{1,0:T(8,128)(2,1)S(1)}, u32[]{:S(2)}, u32[]{:S(2)}) collective-permute-start(bf16[128,1408]{1,0:T(8,128)(2,1)S(1)} %get-tuple-element.53), channel_id=1, source_target_pairs={{0,8},{8,16},{16,24},{24,0},{1,9},{9,17},{17,25},{25,1},{2,10},{10... | collective-permute-start | bytes 1081352 | tf_op jit(solution)/shard_map/ppermute | solution.py:23
  105.8 11.0 %collective-permute-start.28 = (bf16[128,1376]{1,0:T(8,128)(2,1)S(1)}, bf16[128,1376]{1,0:T(8,128)(2,1)S(1)}, u32[]{:S(2)}, u32[]{:S(2)}) collective-permute-start(bf16[128,1376]{1,0:T(8,128)(2,1)S(1)} %get-tuple-element.54), channel_id=1, source_target_pairs={{0,24},{8,0},{16,8},{24,16},{1,25},{9,1},{17,9},{25,17},{2,26},{10... | collective-permute-start | bytes 1056776 | tf_op jit(solution)/shard_map/ppermute | solution.py:23
  105.8 16.4 %collective-permute-start.35 = (bf16[1376,256]{1,0:T(8,128)(2,1)S(1)}, bf16[1376,256]{1,0:T(8,128)(2,1)S(1)}, u32[]{:S(2)}, u32[]{:S(2)}) collective-permute-start(bf16[1376,256]{1,0:T(8,128)(2,1)S(1)} %copy-done.3), channel_id=1, source_target_pairs={{0,32},{1,225},{32,64},{33,1},{64,96},{65,33},{96,128},{97,65},{12... | collective-permute-start | bytes 2113544 | tf_op jit(solution)/shard_map/ppermute | solution.py:40
  109.6 24.7 %copy-start.6 = (f32[3,1376]{1,0:T(4,128)S(1)}, f32[3,1376]{1,0:T(4,128)}, u32[]{:S(2)}) copy-start(f32[3,1376]{1,0:T(4,128)} %gate_kernel.1) | copy-start | bytes 49540
  109.6 24.6 %collective-permute-start.26 = (bf16[128,1408]{1,0:T(8,128)(2,1)S(1)}, bf16[128,1408]{1,0:T(8,128)(2,1)S(1)}, u32[]{:S(2)}, u32[]{:S(2)}) collective-permute-start(bf16[128,1408]{1,0:T(8,128)(2,1)S(1)} %get-tuple-element.52), channel_id=1, source_target_pairs={{0,24},{8,0},{16,8},{24,16},{1,25},{9,1},{17,9},{25,17},{2,26},{10... | collective-permute-start | bytes 1081352 | tf_op jit(solution)/shard_map/ppermute | solution.py:23
  117.1 17.1 %collective-permute-start.29 = (bf16[128,1408]{1,0:T(8,128)(2,1)S(1)}, bf16[128,1408]{1,0:T(8,128)(2,1)S(1)}, u32[]{:S(2)}, u32[]{:S(2)}) collective-permute-start(bf16[128,1408]{1,0:T(8,128)(2,1)S(1)} %get-tuple-element.57), channel_id=1, source_target_pairs={{0,8},{8,16},{16,24},{24,0},{1,9},{9,17},{17,25},{25,1},{2,10},{10... | collective-permute-start | bytes 1081352 | tf_op jit(solution)/shard_map/ppermute | solution.py:23
  120.1 14.1 %collective-permute-start.30 = (bf16[128,1376]{1,0:T(8,128)(2,1)S(1)}, bf16[128,1376]{1,0:T(8,128)(2,1)S(1)}, u32[]{:S(2)}, u32[]{:S(2)}) collective-permute-start(bf16[128,1376]{1,0:T(8,128)(2,1)S(1)} %get-tuple-element.59), channel_id=1, source_target_pairs={{0,8},{8,16},{16,24},{24,0},{1,9},{9,17},{17,25},{25,1},{2,10},{10... | collective-permute-start | bytes 1056776 | tf_op jit(solution)/shard_map/ppermute | solution.py:23
  120.2 14.0 %collective-permute-start.31 = (bf16[128,1376]{1,0:T(8,128)(2,1)S(1)}, bf16[128,1376]{1,0:T(8,128)(2,1)S(1)}, u32[]{:S(2)}, u32[]{:S(2)}) collective-permute-start(bf16[128,1376]{1,0:T(8,128)(2,1)S(1)} %get-tuple-element.60), channel_id=1, source_target_pairs={{0,24},{8,0},{16,8},{24,16},{1,25},{9,1},{17,9},{25,17},{2,26},{10... | collective-permute-start | bytes 1056776 | tf_op jit(solution)/shard_map/ppermute | solution.py:23
  122.2 26.5 %collective-permute-start.36 = (bf16[1376,256]{1,0:T(8,128)(2,1)S(1)}, bf16[1376,256]{1,0:T(8,128)(2,1)S(1)}, u32[]{:S(2)}, u32[]{:S(2)}) collective-permute-start(bf16[1376,256]{1,0:T(8,128)(2,1)S(1)} %copy-done.3), channel_id=1, source_target_pairs={{0,224},{1,33},{32,0},{33,65},{64,32},{65,97},{96,64},{97,129},{12... | collective-permute-start | bytes 2113544 | tf_op jit(solution)/shard_map/ppermute | solution.py:40
  134.2 14.5 %collective-permute-start.37 = (bf16[1376,256]{1,0:T(8,128)(2,1)S(1)}, bf16[1376,256]{1,0:T(8,128)(2,1)S(1)}, u32[]{:S(2)}, u32[]{:S(2)}) collective-permute-start(bf16[1376,256]{1,0:T(8,128)(2,1)S(1)} %collective-permute-done.35.refs_1_), channel_id=1, source_target_pairs={{0,32},{1,225},{32,64},{33,1},{64,96},{65,33},{96,128},{97,65},{12... | collective-permute-start | bytes 2113544 | tf_op jit(solution)/shard_map/ppermute | solution.py:40
  136.0 10.8 %collective-permute-start.32 = (bf16[128,1376]{1,0:T(8,128)(2,1)S(1)}, bf16[128,1376]{1,0:T(8,128)(2,1)S(1)}, u32[]{:S(2)}, u32[]{:S(2)}) collective-permute-start(bf16[128,1376]{1,0:T(8,128)(2,1)S(1)} %shard_map.177.refs_0_), channel_id=1, source_target_pairs={{0,8},{1,25},{8,16},{9,1},{16,24},{17,9},{24,0},{25,17},{2,10},{3,... | collective-permute-start | bytes 1056776 | tf_op jit(solution)/shard_map/ppermute | solution.py:40
  138.0 11.8 %collective-permute-start.33 = (bf16[128,1376]{1,0:T(8,128)(2,1)S(1)}, bf16[128,1376]{1,0:T(8,128)(2,1)S(1)}, u32[]{:S(2)}, u32[]{:S(2)}) collective-permute-start(bf16[128,1376]{1,0:T(8,128)(2,1)S(1)} %shard_map.177.refs_0_), channel_id=1, source_target_pairs={{0,24},{1,9},{8,0},{9,17},{16,8},{17,25},{24,16},{25,1},{2,26},{3,... | collective-permute-start | bytes 1056776 | tf_op jit(solution)/shard_map/ppermute | solution.py:40
  146.8 7.4 %collective-permute-start.34 = (bf16[128,1376]{1,0:T(8,128)(2,1)S(1)}, bf16[128,1376]{1,0:T(8,128)(2,1)S(1)}, u32[]{:S(2)}, u32[]{:S(2)}) collective-permute-start(bf16[128,1376]{1,0:T(8,128)(2,1)S(1)} %collective-permute-done.32.refs_1_), channel_id=1, source_target_pairs={{0,8},{1,25},{8,16},{9,1},{16,24},{17,9},{24,0},{25,17},{2,10},{3,... | collective-permute-start | bytes 1056776 | tf_op jit(solution)/shard_map/ppermute | solution.py:40
  155.6 2.0 %collective-permute-start.38 = (bf16[4,256,256]{2,1,0:T(8,128)(2,1)S(1)}, bf16[4,256,256]{2,1,0:T(8,128)(2,1)S(1)}, u32[]{:S(2)}, u32[]{:S(2)}) collective-permute-start(bf16[4,256,256]{2,1,0:T(8,128)(2,1)S(1)} %shard_map.180), channel_id=1, source_target_pairs={{0,1},{1,0},{2,3},{3,2},{4,5},{5,4},{6,7},{7,6},{8,9},{9,8},{10,11... | collective-permute-start | bytes 1572872 | tf_op jit(solution)/shard_map/ppermute | solution.py:23
  157.8 7.7 %collective-permute-start.39 = (bf16[256,256]{1,0:T(8,128)(2,1)S(1)}, bf16[256,256]{1,0:T(8,128)(2,1)S(1)}, u32[]{:S(2)}, u32[]{:S(2)}) collective-permute-start(bf16[256,256]{1,0:T(8,128)(2,1)S(1)} %get-tuple-element.62), channel_id=1, source_target_pairs={{0,2},{2,4},{4,6},{6,0},{1,3},{3,5},{5,7},{7,1},{8,10},{10,12},{12... | collective-permute-start | bytes 393224 | tf_op jit(solution)/shard_map/ppermute | solution.py:23
  157.9 9.5 %collective-permute-start.40 = (bf16[256,256]{1,0:T(8,128)(2,1)S(1)}, bf16[256,256]{1,0:T(8,128)(2,1)S(1)}, u32[]{:S(2)}, u32[]{:S(2)}) collective-permute-start(bf16[256,256]{1,0:T(8,128)(2,1)S(1)} %get-tuple-element.63), channel_id=1, source_target_pairs={{0,4},{2,6},{4,0},{6,2},{1,5},{3,7},{5,1},{7,3},{8,12},{10,14},{12... | collective-permute-start | bytes 393224 | tf_op jit(solution)/shard_map/ppermute | solution.py:23
  161.0 7.0 %collective-permute-start.41 = (bf16[256,256]{1,0:T(8,128)(2,1)S(1)}, bf16[256,256]{1,0:T(8,128)(2,1)S(1)}, u32[]{:S(2)}, u32[]{:S(2)}) collective-permute-start(bf16[256,256]{1,0:T(8,128)(2,1)S(1)} %get-tuple-element.64), channel_id=1, source_target_pairs={{0,6},{2,0},{4,2},{6,4},{1,7},{3,1},{5,3},{7,5},{8,14},{10,8},{12,... | collective-permute-start | bytes 393224 | tf_op jit(solution)/shard_map/ppermute | solution.py:23
  168.1 8.3 %collective-permute-start.42 = (bf16[128,256]{1,0:T(8,128)(2,1)S(1)}, bf16[128,256]{1,0:T(8,128)(2,1)S(1)}, u32[]{:S(2)}, u32[]{:S(2)}) collective-permute-start(bf16[128,256]{1,0:T(8,128)(2,1)S(1)} %get-tuple-element.65), channel_id=1, source_target_pairs={{0,0},{1,16},{8,8},{9,24},{16,1},{17,17},{24,9},{25,25},{2,2},{3,1... | collective-permute-start | bytes 196616 | tf_op jit(solution)/shard_map/ppermute | solution.py:67
  174.3 3.8 %collective-permute-start.43 = (bf16[128,256]{1,0:T(8,128)(2,1)S(1)}, bf16[128,256]{1,0:T(8,128)(2,1)S(1)}, u32[]{:S(2)}, u32[]{:S(2)}) collective-permute-start(bf16[128,256]{1,0:T(8,128)(2,1)S(1)} %get-tuple-element.66), channel_id=1, source_target_pairs={{0,8},{1,24},{8,0},{9,16},{16,9},{17,25},{24,1},{25,17},{2,10},{3,... | collective-permute-start | bytes 196616 | tf_op jit(solution)/shard_map/ppermute | solution.py:67
  (10 other events, 144.7 us)
where the time goes:
time: 182 us; the launch traced here: 179 us
  waiting for transfers between devices  88.4 us (49%)
  starting transfers between devices  64.5 us (35%)
  Pallas kernels  21.7 us (12%)
  local copies, waits for them, and re-layouts  2.23 us (1%)
    ppermute x21, waiting for transfers between devices, shift_apart(): return lax.ppermute(value, (*axes, CORE), pairs)  50.4 us
    ppermute x19, waiting for transfers between devices, shift(): lax.ppermute(value, axes, [(i, (i + by) % size) for i in range(size)])  31.1 us
    ppermute x21, starting transfers between devices, shift_apart(): return lax.ppermute(value, (*axes, CORE), pairs)  30.3 us
    ppermute x19, starting transfers between devices, shift(): lax.ppermute(value, axes, [(i, (i + by) % size) for i in range(size)])  22.3 us
    pallas_call x21, Pallas kernels, run(): pl.pallas_call(body, out_shape=[jax.ShapeDtypeStruct(*out) for out in out...  21.7 us
    ppermute x4, starting transfers between devices, trade(): return lax.ppermute(value, (X, CORE), pairs)  12 us
    ppermute x4, waiting for transfers between devices, trade(): return lax.ppermute(value, (X, CORE), pairs)  6.88 us
  transfers between devices with their start and end apart: 44, of which 26 were waited for; matrix products, arithmetic and copies ran while one was open for 2% of the time, Pallas kernels for 8%

commit v1 on v0

--- a/solution.py
+++ b/solution.py
@@ -203,7 +203,7 @@
         out[length:] = far[...]
 
     (column,) = kernel_call(column_body, [((own_rows, part), BF16)])(near, far)
-    columns = gather_ring(column, (Y,), RING)
+    columns = [column] + [shift_y(column, k) for k in range(1, RING)]
 
     def stack_body(*refs):
         for k in range(RING):
@@ -217,12 +217,12 @@
         gain, raw, pays = refs[6], refs[7], refs[8:12]
         z, x, y, core = place()
         for side, blocks in ((core, own), (1 - core, other)):
-            for n, k in enumerate(order_before(side)):
+            for k in range(RING):
                 j = (y - z - k) % RING
                 for i in range(2):
                     xs = 2 * side + (x + i) % 2
                     raw[j, aligned(length * turn(x, xs), length), :] = blocks[
-                        n, i * length : (i + 1) * length
+                        k, i * length : (i + 1) * length
                     ]
         squares = jnp.zeros((all_rows, 1), F32)
         gate = jnp.zeros((all_rows, width), F32)
@@ -290,17 +290,17 @@
         flops=1 << 22,
         scratch=[pltpu.VMEM((heads, length, length), F32)],
     )(*pays, value_gain, spatial_bias, head_gain)
-    merges = gather_ring(merged, (X,), RING)
-
-    def side_of(blocks, scratch, x, core, side):
-        for t, block in zip(order_before(core), blocks):
+    merges = [merged] + [shift_x(merged, k) for k in range(1, RING)]
+
+    def side_of(blocks, order, scratch, x, side):
+        for t, block in zip(order, blocks):
             scratch[t] = block[...]
         return jnp.concatenate([scratch[turn(x, 2 * side + i)] for i in range(2)], 0)
 
     def merge_other_body(*refs):
         merges, weights, out, blocks = refs[0:4], refs[4:8], refs[8], refs[9]
         _, x, _, core = place()
-        left = side_of(merges, blocks, x, core, 1 - core)
+        left = side_of(merges, range(RING), blocks, x, 1 - core)
         for j, weight in zip(order_z(core), weights):
             out[:, aligned(j * part, part)] = dot(left, weight[2 * part : 3 * part]).astype(BF16)
 
@@ -315,7 +315,7 @@
         merges, weights, received, raw = refs[0:4], refs[4:8], refs[8], refs[9]
         keep, sends, total, blocks = refs[10], refs[11:14], refs[14], refs[15]
         _, x, y, core = place()
-        left = side_of(merges, blocks, x, core, core)
+        left = side_of(merges, range(RING), blocks, x, core)
         for j, weight in zip(order_z(core), weights):
             at = aligned(j * part, part)
             total[:, at] = dot(left, weight[2 * part : 3 * part]) + received[:, at].astype(F32)
@@ -341,7 +341,7 @@
 
     (hidden,) = kernel_call(hidden_body, [((half, span), BF16)])(keep, *sums)
 
-    mine = gather_ring(hidden, (Y,), RING)
+    mine = [hidden] + [shift_y(hidden, k) for k in range(1, RING)]
     (mine,) = kernel_call(stack_body, [((RING, half, span), BF16)])(*mine)
     theirs = swap_core(mine)
 
@@ -383,14 +383,14 @@
         copy.start()
         lane = lax.broadcasted_iota(jnp.int32, (half, LANES), 1)
         for side, block in ((core, mine), (1 - core, theirs)):
-            for n, k in enumerate(order_before(side)):
+            for k in range(RING):
                 ys = (y - k) % RING
                 at = aligned(half * (ys % 2), half)
                 t = turn(x, 2 * side + ys // 2)
                 slot = jnp.where(t == 0, 3, jnp.where(t == 2, 0, (t + 1) // 2))
                 squares = jnp.zeros((half, 1), F32)
                 for i, j in enumerate(order_z(core)):
-                    piece = block[n, :, aligned(j * part, part)].astype(F32)
+                    piece = block[k, :, aligned(j * part, part)].astype(F32)
                     squares = squares + jnp.sum(piece * piece, axis=1, keepdims=True)
                     row = gain[pl.ds(RING * (RING + (z + j) % RING) + x, 1), :]
                     scaled[slot, at, i * part : (i + 1) * part] = (piece * row).astype(BF16)
@@ -526,7 +526,8 @@
         def run(*refs):
             actives, weights, out, blocks, left = refs[0:4], refs[4], refs[5], refs[6], refs[7]
             _, x, _, core = place()
-            left[...] = side_of(actives, blocks, x, core, core if side_is_own else 1 - core)
+            side = core if side_is_own else 1 - core
+            left[...] = side_of(actives, order_before(core), blocks, x, side)
 
             def step(j, carry):
                 out[j] = dot(left[...], weights[j]).astype(out.dtype)
@@ -547,19 +548,19 @@
 
     def down_add_body(*refs):
         own, received, mine, keep, sends = refs[0], refs[1], refs[2], refs[3], refs[4:7]
-        z, _, y, core = place()
+        z, _, y, _ = place()
         at = (y - z) % RING
         for k in range(1, RING):
             j = (at + k) % RING
             sends[k - 1][...] = (own[j] + received[j].astype(F32)).astype(BF16)
         keep[...] = own[at] + received[at].astype(F32)
-        for n, k in enumerate(order_before(core)):
+        for k in range(RING):
             place_rows = aligned(half * ((y - k) % RING), half)
             for j in range(RING):
 
                 @pl.when(at == j)
                 def _():
-                    piece = mine[n, :, j * part : (j + 1) * part].astype(F32)
+                    piece = mine[k, :, j * part : (j + 1) * part].astype(F32)
                     keep[place_rows, :] = keep[place_rows, :] + piece
 
     block = (own_rows, part)

time: 182 us -> 168 us (0.923)
  waiting for transfers between devices: 88.4 us -> 77.4 us
  starting transfers between devices: 64.5 us -> 61.6 us
    ppermute x21 -> x12, waiting for transfers between devices: 50.4 us -> 22.5 us  [shift_apart(): return lax.ppermute(value, (*axes, CORE), pairs)]
    ppermute x19 -> x28, waiting for transfers between devices: 31.1 us -> 47.4 us  [shift(): lax.ppermute(value, axes, [(i, (i + by) % size) for i in range(size)])]
    ppermute x21 -> x12, starting transfers between devices: 30.3 us -> 14.5 us  [shift_apart(): return lax.ppermute(value, (*axes, CORE), pairs)]
    ppermute x19 -> x28, starting transfers between devices: 22.3 us -> 37.5 us  [shift(): lax.ppermute(value, axes, [(i, (i + by) % size) for i in range(size)])]
    ppermute x4, starting transfers between devices: 12 us -> 9.65 us  [trade(): return lax.ppermute(value, (X, CORE), pairs)]
  transfers between devices with their start and end apart: 44 -> 44, of which waited for: 26 -> 27; matrix products, arithmetic and copies ran while one was open for 2% -> 2% of each run, Pallas kernels for 8% -> 8%
where the time goes in v1:
time: 168 us; the launch traced here: 165 us
  waiting for transfers between devices  77.4 us (46%)
  starting transfers between devices  61.6 us (37%)
  Pallas kernels  21.8 us (13%)
  local copies, waits for them, and re-layouts  2.23 us (1%)
    ppermute x28, waiting for transfers between devices, shift(): lax.ppermute(value, axes, [(i, (i + by) % size) for i in range(size)])  47.4 us
    ppermute x28, starting transfers between devices, shift(): lax.ppermute(value, axes, [(i, (i + by) % size) for i in range(size)])  37.5 us
    ppermute x12, waiting for transfers between devices, shift_apart(): return lax.ppermute(value, (*axes, CORE), pairs)  22.5 us
    pallas_call x21, Pallas kernels, run(): pl.pallas_call(body, out_shape=[jax.ShapeDtypeStruct(*out) for out in out...  21.8 us
    ppermute x12, starting transfers between devices, shift_apart(): return lax.ppermute(value, (*axes, CORE), pairs)  14.5 us
    ppermute x4, starting transfers between devices, trade(): return lax.ppermute(value, (X, CORE), pairs)  9.65 us
    ppermute x4, waiting for transfers between devices, trade(): return lax.ppermute(value, (X, CORE), pairs)  7.54 us
  transfers between devices with their start and end apart: 44, of which 27 were waited for; matrix products, arithmetic and copies ran while one was open for 2% of the time, Pallas kernels for 8%

profile of v1, /device:TPU:4, one launch (start us, length us, event | category | flops | bytes accessed | tf_op | source)
XLA Modules:
  0.0 165.1 jit_solution(1722848324710456283)
XLA Ops:
  0.0 2.4 %shard_map.172 = bf16[2752,256]{1,0:T(8,128)(2,1)} custom-call(bf16[1376,256]{1,0:T(8,128)(2,1)} %bitcast.5, bf16[1376,256]{1,0:T(8,128)(2,1)} %bitcast.7), custom_call_target="tpu_custom_call" | custom-call | tf_op jit(solution)/shard_map/pallas_call | solution.py:75
  2.5 2.0 %collective-permute-start.23 = (bf16[2752,256]{1,0:T(8,128)(2,1)}, bf16[2752,256]{1,0:T(8,128)(2,1)S(1)}, u32[]{:S(2)}, u32[]{:S(2)}) collective-permute-start(bf16[2752,256]{1,0:T(8,128)(2,1)} %shard_map.172), channel_id=1, source_target_pairs={{0,32},{1,225},{32,64},{33,1},{64,96},{65,33},{96,128},{97,65},{12... | collective-permute-start | bytes 4227080 | tf_op jit(solution)/shard_map/ppermute | solution.py:40
  4.4 2.0 %shard_map.163 = (bf16[128,256]{1,0:T(8,128)(2,1)}, bf16[128,256]{1,0:T(8,128)(2,1)}, bf16[784,256]{1,0:T(8,128)(2,1)}) custom-call(bf16[128,512]{1,0:T(8,128)(2,1)} %tokens.1, bf16[256,256]{1,0:T(8,128)(2,1)} %gate.1, bf16[256,256]{1,0:T(8,128)(2,1)} %value.1, bf16[256,256]{1,0:T(8,128)(2,1)} %merge.1, bf16[16,128]{1,0:T(8,128)(2,1)} %bitcast.11), custom_call_target="tpu_custom_call" | custom-call | tf_op jit(solution)/shard_map/pallas_call | solution.py:75
  6.4 2.0 %collective-permute-start.6 = (bf16[784,256]{1,0:T(8,128)(2,1)}, bf16[784,256]{1,0:T(8,128)(2,1)S(1)}, u32[]{:S(2)}, u32[]{:S(2)}) collective-permute-start(bf16[784,256]{1,0:T(8,128)(2,1)} %get-tuple-element.38.refs_2_.refs_4_), channel_id=1, source_target_pairs={{0,32},{1,225},{32,64},{33,1},{64,96},{65,33},{96,128},{97,65},{12... | collective-permute-start | bytes 1204232 | tf_op jit(solution)/shard_map/ppermute | solution.py:40
  8.4 4.3 %collective-permute-start = (bf16[128,256]{1,0:T(8,128)(2,1)}, bf16[128,256]{1,0:T(8,128)(2,1)S(1)}, u32[]{:S(2)}, u32[]{:S(2)}) collective-permute-start(bf16[128,256]{1,0:T(8,128)(2,1)} %get-tuple-element.36), channel_id=1, source_target_pairs={{0,0},{1,16},{8,8},{9,24},{16,1},{17,17},{24,9},{25,25},{2,2},{3,1... | collective-permute-start | bytes 196616 | tf_op jit(solution)/shard_map/ppermute | solution.py:67
  12.9 2.8 %collective-permute-done.near = bf16[128,256]{1,0:T(8,128)(2,1)S(1)} collective-permute-done((bf16[128,256]{1,0:T(8,128)(2,1)}, bf16[128,256]{1,0:T(8,128)(2,1)S(1)}, u32[]{:S(2)}, u32[]{:S(2)}) %collective-permute-start) | collective-permute-done | bytes 65568 | tf_op jit(solution)/shard_map/ppermute | solution.py:67
  16.8 1.7 %collective-permute-start.2 = (bf16[256,256]{1,0:T(8,128)(2,1)S(1)}, bf16[256,256]{1,0:T(8,128)(2,1)S(1)}, u32[]{:S(2)}, u32[]{:S(2)}) collective-permute-start(bf16[256,256]{1,0:T(8,128)(2,1)S(1)} %shard_map.164.refs_0_), channel_id=1, source_target_pairs={{0,2},{2,4},{4,6},{6,0},{1,3},{3,5},{5,7},{7,1},{8,10},{10,12},{12... | collective-permute-start | bytes 393224 | tf_op jit(solution)/shard_map/ppermute | solution.py:23
  18.4 2.9 %collective-permute-start.3 = (bf16[256,256]{1,0:T(8,128)(2,1)S(1)}, bf16[256,256]{1,0:T(8,128)(2,1)S(1)}, u32[]{:S(2)}, u32[]{:S(2)}) collective-permute-start(bf16[256,256]{1,0:T(8,128)(2,1)S(1)} %shard_map.164.refs_0_), channel_id=1, source_target_pairs={{0,4},{2,6},{4,0},{6,2},{1,5},{3,7},{5,1},{7,3},{8,12},{10,14},{12... | collective-permute-start | bytes 393224 | tf_op jit(solution)/shard_map/ppermute | solution.py:23
  22.7 1.4 collective-permute-done.2.refs_1_
  24.1 2.5 %collective-permute-done.3.refs_2_ = bf16[256,256]{1,0:T(8,128)(2,1)S(1)} collective-permute-done((bf16[256,256]{1,0:T(8,128)(2,1)S(1)}, bf16[256,256]{1,0:T(8,128)(2,1)S(1)}, u32[]{:S(2)}, u32[]{:S(2)}) %collective-permute-start.3) | collective-permute-done | bytes 131104 | tf_op jit(solution)/shard_map/ppermute | solution.py:23
  29.6 1.4 pad_maximum_fusion
  32.4 6.0 %collective-permute-done.7.refs_4_.refs_6_ = bf16[784,256]{1,0:T(8,128)(2,1)S(1)} collective-permute-done((bf16[784,256]{1,0:T(8,128)(2,1)}, bf16[784,256]{1,0:T(8,128)(2,1)S(1)}, u32[]{:S(2)}, u32[]{:S(2)}) %collective-permute-start.7) | collective-permute-done | bytes 401440 | tf_op jit(solution)/shard_map/ppermute | solution.py:40
  38.4 1.5 collective-permute-done.8.refs_5_.refs_7_
  40.7 2.0 %shard_map.166 = (bf16[4,512,256]{2,1,0:T(8,128)(2,1)S(1)}, bf16[128,640]{1,0:T(8,128)(2,1)S(1)}, bf16[128,640]{1,0:T(8,128)(2,1)S(1)}, bf16[128,640]{1,0:T(8,128)(2,1)S(1)}, bf16[128,640]{1,0:T(8,128)(2,1)S(1)}) custom-call(bf16[4,256,256]{2,1,0:T(8,128)(2,1)S(1)} %shard_map.165.refs_0_, bf16[4,256,256]{2,1,0:T(8,128)(2,1)} %collective-permute-done.5.refs_1_, ...), custom_call_target="tpu_custom_call" | custom-call | flops 536870912 | tf_op jit(solution)/shard_map/pallas_call | solution.py:75
  43.7 2.1 %collective-permute-start.11 = (bf16[128,640]{1,0:T(8,128)(2,1)S(1)}, bf16[128,640]{1,0:T(8,128)(2,1)S(1)}, u32[]{:S(2)}, u32[]{:S(2)}) collective-permute-start(bf16[128,640]{1,0:T(8,128)(2,1)S(1)} %get-tuple-element.42), channel_id=1, source_target_pairs={{0,8},{8,16},{16,24},{24,0},{1,9},{9,17},{17,25},{25,1},{2,10},{10... | collective-permute-start | bytes 491528 | tf_op jit(solution)/shard_map/ppermute | solution.py:23
  47.5 1.7 %collective-permute-start.25 = (bf16[2752,256]{1,0:T(8,128)(2,1)S(1)}, bf16[2752,256]{1,0:T(8,128)(2,1)S(1)}, u32[]{:S(2)}, u32[]{:S(2)}) collective-permute-start(bf16[2752,256]{1,0:T(8,128)(2,1)S(1)} %collective-permute-done.23.first), channel_id=1, source_target_pairs={{0,32},{1,225},{32,64},{33,1},{64,96},{65,33},{96,128},{97,65},{12... | collective-permute-start | bytes 4227080 | tf_op jit(solution)/shard_map/ppermute | solution.py:40
  49.2 2.2 %collective-permute-done.10.refs_2_ = bf16[128,640]{1,0:T(8,128)(2,1)S(1)} collective-permute-done((bf16[128,640]{1,0:T(8,128)(2,1)S(1)}, bf16[128,640]{1,0:T(8,128)(2,1)S(1)}, u32[]{:S(2)}, u32[]{:S(2)}) %collective-permute-start.10) | collective-permute-done | bytes 163872 | tf_op jit(solution)/shard_map/ppermute | solution.py:23
  51.3 2.0 %collective-permute-done.11.refs_3_ = bf16[128,640]{1,0:T(8,128)(2,1)S(1)} collective-permute-done((bf16[128,640]{1,0:T(8,128)(2,1)S(1)}, bf16[128,640]{1,0:T(8,128)(2,1)S(1)}, u32[]{:S(2)}, u32[]{:S(2)}) %collective-permute-start.11) | collective-permute-done | bytes 163872 | tf_op jit(solution)/shard_map/ppermute | solution.py:23
  53.9 2.9 %collective-permute-start.12 = (bf16[128,256]{1,0:T(8,128)(2,1)S(1)}, bf16[128,256]{1,0:T(8,128)(2,1)S(1)}, u32[]{:S(2)}, u32[]{:S(2)}) collective-permute-start(bf16[128,256]{1,0:T(8,128)(2,1)S(1)} %shard_map.167.refs_0_), channel_id=1, source_target_pairs={{0,8},{8,16},{16,24},{24,0},{1,9},{9,17},{17,25},{25,1},{2,10},{10... | collective-permute-start | bytes 196616 | tf_op jit(solution)/shard_map/ppermute | solution.py:23
  56.8 2.0 %collective-permute-start.14 = (bf16[128,256]{1,0:T(8,128)(2,1)S(1)}, bf16[128,256]{1,0:T(8,128)(2,1)S(1)}, u32[]{:S(2)}, u32[]{:S(2)}) collective-permute-start(bf16[128,256]{1,0:T(8,128)(2,1)S(1)} %shard_map.167.refs_0_), channel_id=1, source_target_pairs={{0,24},{8,0},{16,8},{24,16},{1,25},{9,1},{17,9},{25,17},{2,26},{10... | collective-permute-start | bytes 196616 | tf_op jit(solution)/shard_map/ppermute | solution.py:23
  58.8 3.7 %collective-permute-done.13.refs_2_ = bf16[128,256]{1,0:T(8,128)(2,1)S(1)} collective-permute-done((bf16[128,256]{1,0:T(8,128)(2,1)S(1)}, bf16[128,256]{1,0:T(8,128)(2,1)S(1)}, u32[]{:S(2)}, u32[]{:S(2)}) %collective-permute-start.13) | collective-permute-done | bytes 65568 | tf_op jit(solution)/shard_map/ppermute | solution.py:23
  63.0 1.9 %collective-permute-done.15.refs_8_ = bf16[256,1024]{1,0:T(8,128)(2,1)S(1)} collective-permute-done((bf16[256,1024]{1,0:T(8,128)(2,1)S(1)}, bf16[256,1024]{1,0:T(8,128)(2,1)S(1)}, u32[]{:S(2)}, u32[]{:S(2)}) %collective-permute-start.15) | collective-permute-done | bytes 524320 | tf_op jit(solution)/shard_map/ppermute | solution.py:23
  66.4 3.0 %collective-permute-start.17 = (bf16[64,1024]{1,0:T(8,128)(2,1)S(1)}, bf16[64,1024]{1,0:T(8,128)(2,1)S(1)}, u32[]{:S(2)}, u32[]{:S(2)}) collective-permute-start(bf16[64,1024]{1,0:T(8,128)(2,1)S(1)} %get-tuple-element.46), channel_id=1, source_target_pairs={{0,4},{2,6},{4,0},{6,2},{1,5},{3,7},{5,1},{7,3},{8,12},{10,14},{12... | collective-permute-start | bytes 393224 | tf_op jit(solution)/shard_map/ppermute | solution.py:23
  70.3 1.9 %collective-permute-done.16.first = bf16[64,1024]{1,0:T(8,128)(2,1)S(1)} collective-permute-done((bf16[64,1024]{1,0:T(8,128)(2,1)S(1)}, bf16[64,1024]{1,0:T(8,128)(2,1)S(1)}, u32[]{:S(2)}, u32[]{:S(2)}) %collective-permute-start.16) | collective-permute-done | bytes 131104 | tf_op jit(solution)/shard_map/ppermute | solution.py:23
  72.2 3.5 %collective-permute-done.17.second = bf16[64,1024]{1,0:T(8,128)(2,1)S(1)} collective-permute-done((bf16[64,1024]{1,0:T(8,128)(2,1)S(1)}, bf16[64,1024]{1,0:T(8,128)(2,1)S(1)}, u32[]{:S(2)}, u32[]{:S(2)}) %collective-permute-start.17) | collective-permute-done | bytes 131104 | tf_op jit(solution)/shard_map/ppermute | solution.py:23
  75.8 1.5 collective-permute-start.19
  77.3 2.5 %collective-permute-start.20 = (bf16[64,1024]{1,0:T(8,128)(2,1)S(1)}, bf16[64,1024]{1,0:T(8,128)(2,1)S(1)}, u32[]{:S(2)}, u32[]{:S(2)}) collective-permute-start(bf16[64,1024]{1,0:T(8,128)(2,1)S(1)} %shard_map.170.refs_0_), channel_id=1, source_target_pairs={{0,4},{2,6},{4,0},{6,2},{1,5},{3,7},{5,1},{7,3},{8,12},{10,14},{12... | collective-permute-start | bytes 393224 | tf_op jit(solution)/shard_map/ppermute | solution.py:23
  80.6 1.9 %collective-permute-done.19.refs_1_ = bf16[64,1024]{1,0:T(8,128)(2,1)S(1)} collective-permute-done((bf16[64,1024]{1,0:T(8,128)(2,1)S(1)}, bf16[64,1024]{1,0:T(8,128)(2,1)S(1)}, u32[]{:S(2)}, u32[]{:S(2)}) %collective-permute-start.19) | collective-permute-done | bytes 131104 | tf_op jit(solution)/shard_map/ppermute | solution.py:23
  82.4 3.3 %collective-permute-done.20.refs_2_ = bf16[64,1024]{1,0:T(8,128)(2,1)S(1)} collective-permute-done((bf16[64,1024]{1,0:T(8,128)(2,1)S(1)}, bf16[64,1024]{1,0:T(8,128)(2,1)S(1)}, u32[]{:S(2)}, u32[]{:S(2)}) %collective-permute-start.20) | collective-permute-done | bytes 131104 | tf_op jit(solution)/shard_map/ppermute | solution.py:23
  86.3 1.5 collective-permute-done.22.refs_1_
  87.8 3.3 %shard_map.174 = (bf16[128,1408]{1,0:T(8,128)(2,1)S(1)}, bf16[128,1376]{1,0:T(8,128)(2,1)S(1)}, bf16[4,128,1024]{2,1,0:T(8,128)(2,1)S(1)}, f32[4,128,128]{2,1,0:T(8,128)S(1)}, bf16[2752,256]{1,0:T(8,128)(2,1)S(1)}) custom-call(bf16[4,64,1024]{2,1,0:T(8,128)(2,1)S(1)} %shard_map.171.refs_0_.refs_2_, bf16[4,64,1024]{2,1,0:T(8,128)(2,1)S(1)} %collective-permute-done.22.refs_1_, ...), custom_call_target="tpu_custom_call" | custom-call | flops 721420288 | tf_op jit(solution)/shard_map/pallas_call | solution.py:75
  91.1 1.6 collective-permute-start.27
  94.0 3.7 %shard_map.175 = (bf16[128,1408]{1,0:T(8,128)(2,1)S(1)}, bf16[128,1376]{1,0:T(8,128)(2,1)S(1)}, f32[128,1408]{1,0:T(8,128)S(1)}, f32[128,1376]{1,0:T(8,128)S(1)}...) custom-call(bf16[4,128,1024]{2,1,0:T(8,128)(2,1)S(1)} %get-tuple-element.48.scaled, ...), custom_call_target="tpu_custom_call" | custom-call | flops 2164260864 | tf_op jit(solution)/shard_map/pallas_call | solution.py:75
  98.5 5.5 %collective-permute-done.28.value_two = bf16[128,1376]{1,0:T(8,128)(2,1)S(1)} collective-permute-done((bf16[128,1376]{1,0:T(8,128)(2,1)S(1)}, bf16[128,1376]{1,0:T(8,128)(2,1)S(1)}, u32[]{:S(2)}, u32[]{:S(2)}) %collective-permute-start.28) | collective-permute-done | bytes 352288 | tf_op jit(solution)/shard_map/ppermute | solution.py:23
  104.3 3.2 %collective-permute-start.29 = (bf16[128,1408]{1,0:T(8,128)(2,1)S(1)}, bf16[128,1408]{1,0:T(8,128)(2,1)S(1)}, u32[]{:S(2)}, u32[]{:S(2)}) collective-permute-start(bf16[128,1408]{1,0:T(8,128)(2,1)S(1)} %get-tuple-element.57), channel_id=1, source_target_pairs={{0,8},{8,16},{16,24},{24,0},{1,9},{9,17},{17,25},{25,1},{2,10},{10... | collective-permute-start | bytes 1081352 | tf_op jit(solution)/shard_map/ppermute | solution.py:23
  107.6 1.9 %collective-permute-start.31 = (bf16[128,1376]{1,0:T(8,128)(2,1)S(1)}, bf16[128,1376]{1,0:T(8,128)(2,1)S(1)}, u32[]{:S(2)}, u32[]{:S(2)}) collective-permute-start(bf16[128,1376]{1,0:T(8,128)(2,1)S(1)} %get-tuple-element.60), channel_id=1, source_target_pairs={{0,24},{8,0},{16,8},{24,16},{1,25},{9,1},{17,9},{25,17},{2,26},{10... | collective-permute-start | bytes 1056776 | tf_op jit(solution)/shard_map/ppermute | solution.py:23
  109.6 2.2 %collective-permute-start.36 = (bf16[1376,256]{1,0:T(8,128)(2,1)S(1)}, bf16[1376,256]{1,0:T(8,128)(2,1)S(1)}, u32[]{:S(2)}, u32[]{:S(2)}) collective-permute-start(bf16[1376,256]{1,0:T(8,128)(2,1)S(1)} %copy-done.3), channel_id=1, source_target_pairs={{0,224},{1,33},{32,0},{33,65},{64,32},{65,97},{96,64},{97,129},{12... | collective-permute-start | bytes 2113544 | tf_op jit(solution)/shard_map/ppermute | solution.py:40
  111.8 9.2 %collective-permute-done.30.value_near = bf16[128,1376]{1,0:T(8,128)(2,1)S(1)} collective-permute-done((bf16[128,1376]{1,0:T(8,128)(2,1)S(1)}, bf16[128,1376]{1,0:T(8,128)(2,1)S(1)}, u32[]{:S(2)}, u32[]{:S(2)}) %collective-permute-start.30) | collective-permute-done | bytes 352288 | tf_op jit(solution)/shard_map/ppermute | solution.py:23
  121.7 1.7 %shard_map.177.refs_0_ = bf16[128,1376]{1,0:T(8,128)(2,1)S(1)} custom-call(f32[128,1408]{1,0:T(8,128)S(1)} %get-tuple-element.51.gate_own, bf16[128,1408]{1,0:T(8,128)(2,1)S(1)} %collective-permute-done.26.gate_near, bf16[128,1408]{1,0:T(8,128)(2,1)S(1)} %collective-permute-done.29.gate_join, f32[128,1376]{1,0:T(8,128)S(1)} %get-tuple-element.58.value_own, ...), custom_call_target="tpu_custom_call" | custom-call | flops 16777216 | tf_op jit(solution)/shard_map/pallas_call | solution.py:75
  123.5 2.6 %collective-permute-start.32 = (bf16[128,1376]{1,0:T(8,128)(2,1)S(1)}, bf16[128,1376]{1,0:T(8,128)(2,1)S(1)}, u32[]{:S(2)}, u32[]{:S(2)}) collective-permute-start(bf16[128,1376]{1,0:T(8,128)(2,1)S(1)} %shard_map.177.refs_0_), channel_id=1, source_target_pairs={{0,8},{1,25},{8,16},{9,1},{16,24},{17,9},{24,0},{25,17},{2,10},{3,... | collective-permute-start | bytes 1056776 | tf_op jit(solution)/shard_map/ppermute | solution.py:40
  126.1 8.1 %collective-permute-done.32.refs_1_ = bf16[128,1376]{1,0:T(8,128)(2,1)S(1)} collective-permute-done((bf16[128,1376]{1,0:T(8,128)(2,1)S(1)}, bf16[128,1376]{1,0:T(8,128)(2,1)S(1)}, u32[]{:S(2)}, u32[]{:S(2)}) %collective-permute-start.32) | collective-permute-done | bytes 352288 | tf_op jit(solution)/shard_map/ppermute | solution.py:40
  136.1 5.5 %collective-permute-done.34.refs_3_ = bf16[128,1376]{1,0:T(8,128)(2,1)S(1)} collective-permute-done((bf16[128,1376]{1,0:T(8,128)(2,1)S(1)}, bf16[128,1376]{1,0:T(8,128)(2,1)S(1)}, u32[]{:S(2)}, u32[]{:S(2)}) %collective-permute-start.34) | collective-permute-done | bytes 352288 | tf_op jit(solution)/shard_map/ppermute | solution.py:40
  145.9 2.9 %collective-permute-start.40 = (bf16[256,256]{1,0:T(8,128)(2,1)S(1)}, bf16[256,256]{1,0:T(8,128)(2,1)S(1)}, u32[]{:S(2)}, u32[]{:S(2)}) collective-permute-start(bf16[256,256]{1,0:T(8,128)(2,1)S(1)} %get-tuple-element.63), channel_id=1, source_target_pairs={{0,4},{2,6},{4,0},{6,2},{1,5},{3,7},{5,1},{7,3},{8,12},{10,14},{12... | collective-permute-start | bytes 393224 | tf_op jit(solution)/shard_map/ppermute | solution.py:23
  149.1 3.2 %collective-permute-done.39.first = bf16[256,256]{1,0:T(8,128)(2,1)S(1)} collective-permute-done((bf16[256,256]{1,0:T(8,128)(2,1)S(1)}, bf16[256,256]{1,0:T(8,128)(2,1)S(1)}, u32[]{:S(2)}, u32[]{:S(2)}) %collective-permute-start.39) | collective-permute-done | bytes 131104 | tf_op jit(solution)/shard_map/ppermute | solution.py:23
  152.3 2.7 %collective-permute-done.40.second = bf16[256,256]{1,0:T(8,128)(2,1)S(1)} collective-permute-done((bf16[256,256]{1,0:T(8,128)(2,1)S(1)}, bf16[256,256]{1,0:T(8,128)(2,1)S(1)}, u32[]{:S(2)}, u32[]{:S(2)}) %collective-permute-start.40) | collective-permute-done | bytes 131104 | tf_op jit(solution)/shard_map/ppermute | solution.py:23
  155.4 5.1 %collective-permute-start.42 = (bf16[128,256]{1,0:T(8,128)(2,1)S(1)}, bf16[128,256]{1,0:T(8,128)(2,1)S(1)}, u32[]{:S(2)}, u32[]{:S(2)}) collective-permute-start(bf16[128,256]{1,0:T(8,128)(2,1)S(1)} %get-tuple-element.65), channel_id=1, source_target_pairs={{0,0},{1,16},{8,8},{9,24},{16,1},{17,17},{24,9},{25,25},{2,2},{3,1... | collective-permute-start | bytes 196616 | tf_op jit(solution)/shard_map/ppermute | solution.py:67
  160.6 2.1 %collective-permute-done.42.near = bf16[128,256]{1,0:T(8,128)(2,1)S(1)} collective-permute-done((bf16[128,256]{1,0:T(8,128)(2,1)S(1)}, bf16[128,256]{1,0:T(8,128)(2,1)S(1)}, u32[]{:S(2)}, u32[]{:S(2)}) %collective-permute-start.42) | collective-permute-done | bytes 65568 | tf_op jit(solution)/shard_map/ppermute | solution.py:67
  162.7 1.6 collective-permute-done.43.far
  (93 shorter events, 25.8 us)
Async XLA Ops:
  2.5 45.0 %collective-permute-start.23 = (bf16[2752,256]{1,0:T(8,128)(2,1)}, bf16[2752,256]{1,0:T(8,128)(2,1)S(1)}, u32[]{:S(2)}, u32[]{:S(2)}) collective-permute-start(bf16[2752,256]{1,0:T(8,128)(2,1)} %shard_map.172), channel_id=1, source_target_pairs={{0,32},{1,225},{32,64},{33,1},{64,96},{65,33},{96,128},{97,65},{12... | collective-permute-start | bytes 4227080 | tf_op jit(solution)/shard_map/ppermute | solution.py:40
  6.4 33.5 %copy-start = (bf16[784,256]{1,0:T(8,128)(2,1)S(1)}, bf16[784,256]{1,0:T(8,128)(2,1)}, u32[]{:S(2)}) copy-start(bf16[784,256]{1,0:T(8,128)(2,1)} %get-tuple-element.38.refs_2_.refs_4_) | copy-start | bytes 1204228
  6.4 23.1 %collective-permute-start.6 = (bf16[784,256]{1,0:T(8,128)(2,1)}, bf16[784,256]{1,0:T(8,128)(2,1)S(1)}, u32[]{:S(2)}, u32[]{:S(2)}) collective-permute-start(bf16[784,256]{1,0:T(8,128)(2,1)} %get-tuple-element.38.refs_2_.refs_4_), channel_id=1, source_target_pairs={{0,32},{1,225},{32,64},{33,1},{64,96},{65,33},{96,128},{97,65},{12... | collective-permute-start | bytes 1204232 | tf_op jit(solution)/shard_map/ppermute | solution.py:40
  8.4 7.3 %collective-permute-start = (bf16[128,256]{1,0:T(8,128)(2,1)}, bf16[128,256]{1,0:T(8,128)(2,1)S(1)}, u32[]{:S(2)}, u32[]{:S(2)}) collective-permute-start(bf16[128,256]{1,0:T(8,128)(2,1)} %get-tuple-element.36), channel_id=1, source_target_pairs={{0,0},{1,16},{8,8},{9,24},{16,1},{17,17},{24,9},{25,25},{2,2},{3,1... | collective-permute-start | bytes 196616 | tf_op jit(solution)/shard_map/ppermute | solution.py:67
  12.8 4.0 %collective-permute-start.1 = (bf16[128,256]{1,0:T(8,128)(2,1)}, bf16[128,256]{1,0:T(8,128)(2,1)S(1)}, u32[]{:S(2)}, u32[]{:S(2)}) collective-permute-start(bf16[128,256]{1,0:T(8,128)(2,1)} %get-tuple-element.37), channel_id=1, source_target_pairs={{0,8},{1,24},{8,0},{9,16},{16,9},{17,25},{24,1},{25,17},{2,10},{3,... | collective-permute-start | bytes 196616 | tf_op jit(solution)/shard_map/ppermute | solution.py:67
  16.8 7.3 %collective-permute-start.2 = (bf16[256,256]{1,0:T(8,128)(2,1)S(1)}, bf16[256,256]{1,0:T(8,128)(2,1)S(1)}, u32[]{:S(2)}, u32[]{:S(2)}) collective-permute-start(bf16[256,256]{1,0:T(8,128)(2,1)S(1)} %shard_map.164.refs_0_), channel_id=1, source_target_pairs={{0,2},{2,4},{4,6},{6,0},{1,3},{3,5},{5,7},{7,1},{8,10},{10,12},{12... | collective-permute-start | bytes 393224 | tf_op jit(solution)/shard_map/ppermute | solution.py:23
  18.4 8.2 %collective-permute-start.3 = (bf16[256,256]{1,0:T(8,128)(2,1)S(1)}, bf16[256,256]{1,0:T(8,128)(2,1)S(1)}, u32[]{:S(2)}, u32[]{:S(2)}) collective-permute-start(bf16[256,256]{1,0:T(8,128)(2,1)S(1)} %shard_map.164.refs_0_), channel_id=1, source_target_pairs={{0,4},{2,6},{4,0},{6,2},{1,5},{3,7},{5,1},{7,3},{8,12},{10,14},{12... | collective-permute-start | bytes 393224 | tf_op jit(solution)/shard_map/ppermute | solution.py:23
  21.3 5.4 %collective-permute-start.4 = (bf16[256,256]{1,0:T(8,128)(2,1)S(1)}, bf16[256,256]{1,0:T(8,128)(2,1)S(1)}, u32[]{:S(2)}, u32[]{:S(2)}) collective-permute-start(bf16[256,256]{1,0:T(8,128)(2,1)S(1)} %shard_map.164.refs_0_), channel_id=1, source_target_pairs={{0,6},{2,0},{4,2},{6,4},{1,7},{3,1},{5,3},{7,5},{8,14},{10,8},{12,... | collective-permute-start | bytes 393224 | tf_op jit(solution)/shard_map/ppermute | solution.py:23
  26.7 11.7 %collective-permute-start.5 = (bf16[4,256,256]{2,1,0:T(8,128)(2,1)S(1)}, bf16[4,256,256]{2,1,0:T(8,128)(2,1)}, u32[]{:S(2)}, u32[]{:S(2)}) collective-permute-start(bf16[4,256,256]{2,1,0:T(8,128)(2,1)S(1)} %shard_map.165.refs_0_), channel_id=1, source_target_pairs={{0,1},{1,0},{2,3},{3,2},{4,5},{5,4},{6,7},{7,6},{8,9},{9,8},{10,11... | collective-permute-start | bytes 1572872 | tf_op jit(solution)/shard_map/ppermute | solution.py:23
  26.8 11.6 %collective-permute-start.7 = (bf16[784,256]{1,0:T(8,128)(2,1)}, bf16[784,256]{1,0:T(8,128)(2,1)S(1)}, u32[]{:S(2)}, u32[]{:S(2)}) collective-permute-start(bf16[784,256]{1,0:T(8,128)(2,1)} %get-tuple-element.38.refs_2_.refs_4_), channel_id=1, source_target_pairs={{0,224},{1,33},{32,0},{33,65},{64,32},{65,97},{96,64},{97,129},{12... | collective-permute-start | bytes 1204232 | tf_op jit(solution)/shard_map/ppermute | solution.py:40
  29.5 10.4 %collective-permute-start.8 = (bf16[784,256]{1,0:T(8,128)(2,1)S(1)}, bf16[784,256]{1,0:T(8,128)(2,1)S(1)}, u32[]{:S(2)}, u32[]{:S(2)}) collective-permute-start(bf16[784,256]{1,0:T(8,128)(2,1)S(1)} %collective-permute-done.6.refs_3_.refs_5_), channel_id=1, source_target_pairs={{0,32},{1,225},{32,64},{33,1},{64,96},{65,33},{96,128},{97,65},{12... | collective-permute-start | bytes 1204232 | tf_op jit(solution)/shard_map/ppermute | solution.py:40
  29.5 23.8 %copy-start.10 = (f32[2,128]{1,0:T(2,128)S(1)}, f32[2,128]{1,0:T(2,128)}, u32[]{:S(2)}) copy-start(f32[2,128]{1,0:T(2,128)} %refs_6_.1) | copy-start | bytes 3076
  42.7 8.7 %collective-permute-start.10 = (bf16[128,640]{1,0:T(8,128)(2,1)S(1)}, bf16[128,640]{1,0:T(8,128)(2,1)S(1)}, u32[]{:S(2)}, u32[]{:S(2)}) collective-permute-start(bf16[128,640]{1,0:T(8,128)(2,1)S(1)} %get-tuple-element.41), channel_id=1, source_target_pairs={{0,16},{8,24},{16,0},{24,8},{1,17},{9,25},{17,1},{25,9},{2,18},{10... | collective-permute-start | bytes 491528 | tf_op jit(solution)/shard_map/ppermute | solution.py:23
  43.7 9.6 %collective-permute-start.11 = (bf16[128,640]{1,0:T(8,128)(2,1)S(1)}, bf16[128,640]{1,0:T(8,128)(2,1)S(1)}, u32[]{:S(2)}, u32[]{:S(2)}) collective-permute-start(bf16[128,640]{1,0:T(8,128)(2,1)S(1)} %get-tuple-element.42), channel_id=1, source_target_pairs={{0,8},{8,16},{16,24},{24,0},{1,9},{9,17},{17,25},{25,1},{2,10},{10... | collective-permute-start | bytes 491528 | tf_op jit(solution)/shard_map/ppermute | solution.py:23
  45.8 7.6 %collective-permute-start.9 = (bf16[128,640]{1,0:T(8,128)(2,1)S(1)}, bf16[128,640]{1,0:T(8,128)(2,1)S(1)}, u32[]{:S(2)}, u32[]{:S(2)}) collective-permute-start(bf16[128,640]{1,0:T(8,128)(2,1)S(1)} %get-tuple-element.40), channel_id=1, source_target_pairs={{0,24},{8,0},{16,8},{24,16},{1,25},{9,1},{17,9},{25,17},{2,26},{10... | collective-permute-start | bytes 491528 | tf_op jit(solution)/shard_map/ppermute | solution.py:23
  47.1 38.7 %collective-permute-start.24 = (bf16[2752,256]{1,0:T(8,128)(2,1)S(1)}, bf16[2752,256]{1,0:T(8,128)(2,1)S(1)}, u32[]{:S(2)}, u32[]{:S(2)}) collective-permute-start(bf16[2752,256]{1,0:T(8,128)(2,1)S(1)} %copy-done.11), channel_id=1, source_target_pairs={{0,224},{1,33},{32,0},{33,65},{64,32},{65,97},{96,64},{97,129},{12... | collective-permute-start | bytes 4227080 | tf_op jit(solution)/shard_map/ppermute | solution.py:40
  47.5 40.3 %collective-permute-start.25 = (bf16[2752,256]{1,0:T(8,128)(2,1)S(1)}, bf16[2752,256]{1,0:T(8,128)(2,1)S(1)}, u32[]{:S(2)}, u32[]{:S(2)}) collective-permute-start(bf16[2752,256]{1,0:T(8,128)(2,1)S(1)} %collective-permute-done.23.first), channel_id=1, source_target_pairs={{0,32},{1,225},{32,64},{33,1},{64,96},{65,33},{96,128},{97,65},{12... | collective-permute-start | bytes 4227080 | tf_op jit(solution)/shard_map/ppermute | solution.py:40
  53.9 5.0 %collective-permute-start.12 = (bf16[128,256]{1,0:T(8,128)(2,1)S(1)}, bf16[128,256]{1,0:T(8,128)(2,1)S(1)}, u32[]{:S(2)}, u32[]{:S(2)}) collective-permute-start(bf16[128,256]{1,0:T(8,128)(2,1)S(1)} %shard_map.167.refs_0_), channel_id=1, source_target_pairs={{0,8},{8,16},{16,24},{24,0},{1,9},{9,17},{17,25},{25,1},{2,10},{10... | collective-permute-start | bytes 196616 | tf_op jit(solution)/shard_map/ppermute | solution.py:23
  56.8 5.8 %collective-permute-start.13 = (bf16[128,256]{1,0:T(8,128)(2,1)S(1)}, bf16[128,256]{1,0:T(8,128)(2,1)S(1)}, u32[]{:S(2)}, u32[]{:S(2)}) collective-permute-start(bf16[128,256]{1,0:T(8,128)(2,1)S(1)} %shard_map.167.refs_0_), channel_id=1, source_target_pairs={{0,16},{8,24},{16,0},{24,8},{1,17},{9,25},{17,1},{25,9},{2,18},{10... | collective-permute-start | bytes 196616 | tf_op jit(solution)/shard_map/ppermute | solution.py:23
  56.8 5.8 %collective-permute-start.14 = (bf16[128,256]{1,0:T(8,128)(2,1)S(1)}, bf16[128,256]{1,0:T(8,128)(2,1)S(1)}, u32[]{:S(2)}, u32[]{:S(2)}) collective-permute-start(bf16[128,256]{1,0:T(8,128)(2,1)S(1)} %shard_map.167.refs_0_), channel_id=1, source_target_pairs={{0,24},{8,0},{16,8},{24,16},{1,25},{9,1},{17,9},{25,17},{2,26},{10... | collective-permute-start | bytes 196616 | tf_op jit(solution)/shard_map/ppermute | solution.py:23
  62.9 2.0 %collective-permute-start.15 = (bf16[256,1024]{1,0:T(8,128)(2,1)S(1)}, bf16[256,1024]{1,0:T(8,128)(2,1)S(1)}, u32[]{:S(2)}, u32[]{:S(2)}) collective-permute-start(bf16[256,1024]{1,0:T(8,128)(2,1)S(1)} %shard_map.168), channel_id=1, source_target_pairs={{0,1},{1,0},{2,3},{3,2},{4,5},{5,4},{6,7},{7,6},{8,9},{9,8},{10,11... | collective-permute-start | bytes 1572872 | tf_op jit(solution)/shard_map/ppermute | solution.py:23
  65.3 6.9 %collective-permute-start.16 = (bf16[64,1024]{1,0:T(8,128)(2,1)S(1)}, bf16[64,1024]{1,0:T(8,128)(2,1)S(1)}, u32[]{:S(2)}, u32[]{:S(2)}) collective-permute-start(bf16[64,1024]{1,0:T(8,128)(2,1)S(1)} %get-tuple-element.45), channel_id=1, source_target_pairs={{0,2},{2,4},{4,6},{6,0},{1,3},{3,5},{5,7},{7,1},{8,10},{10,12},{12... | collective-permute-start | bytes 393224 | tf_op jit(solution)/shard_map/ppermute | solution.py:23
  66.4 9.3 %collective-permute-start.17 = (bf16[64,1024]{1,0:T(8,128)(2,1)S(1)}, bf16[64,1024]{1,0:T(8,128)(2,1)S(1)}, u32[]{:S(2)}, u32[]{:S(2)}) collective-permute-start(bf16[64,1024]{1,0:T(8,128)(2,1)S(1)} %get-tuple-element.46), channel_id=1, source_target_pairs={{0,4},{2,6},{4,0},{6,2},{1,5},{3,7},{5,1},{7,3},{8,12},{10,14},{12... | collective-permute-start | bytes 393224 | tf_op jit(solution)/shard_map/ppermute | solution.py:23
  69.4 6.3 %collective-permute-start.18 = (bf16[64,1024]{1,0:T(8,128)(2,1)S(1)}, bf16[64,1024]{1,0:T(8,128)(2,1)S(1)}, u32[]{:S(2)}, u32[]{:S(2)}) collective-permute-start(bf16[64,1024]{1,0:T(8,128)(2,1)S(1)} %get-tuple-element.47), channel_id=1, source_target_pairs={{0,6},{2,0},{4,2},{6,4},{1,7},{3,1},{5,3},{7,5},{8,14},{10,8},{12,... | collective-permute-start | bytes 393224 | tf_op jit(solution)/shard_map/ppermute | solution.py:23
  75.8 6.6 %collective-permute-start.19 = (bf16[64,1024]{1,0:T(8,128)(2,1)S(1)}, bf16[64,1024]{1,0:T(8,128)(2,1)S(1)}, u32[]{:S(2)}, u32[]{:S(2)}) collective-permute-start(bf16[64,1024]{1,0:T(8,128)(2,1)S(1)} %shard_map.170.refs_0_), channel_id=1, source_target_pairs={{0,2},{2,4},{4,6},{6,0},{1,3},{3,5},{5,7},{7,1},{8,10},{10,12},{12... | collective-permute-start | bytes 393224 | tf_op jit(solution)/shard_map/ppermute | solution.py:23
  77.3 8.4 %collective-permute-start.20 = (bf16[64,1024]{1,0:T(8,128)(2,1)S(1)}, bf16[64,1024]{1,0:T(8,128)(2,1)S(1)}, u32[]{:S(2)}, u32[]{:S(2)}) collective-permute-start(bf16[64,1024]{1,0:T(8,128)(2,1)S(1)} %shard_map.170.refs_0_), channel_id=1, source_target_pairs={{0,4},{2,6},{4,0},{6,2},{1,5},{3,7},{5,1},{7,3},{8,12},{10,14},{12... | collective-permute-start | bytes 393224 | tf_op jit(solution)/shard_map/ppermute | solution.py:23
  79.8 5.9 %collective-permute-start.21 = (bf16[64,1024]{1,0:T(8,128)(2,1)S(1)}, bf16[64,1024]{1,0:T(8,128)(2,1)S(1)}, u32[]{:S(2)}, u32[]{:S(2)}) collective-permute-start(bf16[64,1024]{1,0:T(8,128)(2,1)S(1)} %shard_map.170.refs_0_), channel_id=1, source_target_pairs={{0,6},{2,0},{4,2},{6,4},{1,7},{3,1},{5,3},{7,5},{8,14},{10,8},{12,... | collective-permute-start | bytes 393224 | tf_op jit(solution)/shard_map/ppermute | solution.py:23
  85.8 2.0 %collective-permute-start.22 = (bf16[4,64,1024]{2,1,0:T(8,128)(2,1)S(1)}, bf16[4,64,1024]{2,1,0:T(8,128)(2,1)S(1)}, u32[]{:S(2)}, u32[]{:S(2)}) collective-permute-start(bf16[4,64,1024]{2,1,0:T(8,128)(2,1)S(1)} %shard_map.171.refs_0_.refs_2_), channel_id=1, source_target_pairs={{0,1},{1,0},{2,3},{3,2},{4,5},{5,4},{6,7},{7,6},{8,9},{9,8},{10,11... | collective-permute-start | bytes 1572872 | tf_op jit(solution)/shard_map/ppermute | solution.py:23
  91.1 12.9 %collective-permute-start.27 = (bf16[128,1408]{1,0:T(8,128)(2,1)S(1)}, bf16[128,1408]{1,0:T(8,128)(2,1)S(1)}, u32[]{:S(2)}, u32[]{:S(2)}) collective-permute-start(bf16[128,1408]{1,0:T(8,128)(2,1)S(1)} %get-tuple-element.53), channel_id=1, source_target_pairs={{0,8},{8,16},{16,24},{24,0},{1,9},{9,17},{17,25},{25,1},{2,10},{10... | collective-permute-start | bytes 1081352 | tf_op jit(solution)/shard_map/ppermute | solution.py:23
  92.7 11.3 %collective-permute-start.28 = (bf16[128,1376]{1,0:T(8,128)(2,1)S(1)}, bf16[128,1376]{1,0:T(8,128)(2,1)S(1)}, u32[]{:S(2)}, u32[]{:S(2)}) collective-permute-start(bf16[128,1376]{1,0:T(8,128)(2,1)S(1)} %get-tuple-element.54), channel_id=1, source_target_pairs={{0,24},{8,0},{16,8},{24,16},{1,25},{9,1},{17,9},{25,17},{2,26},{10... | collective-permute-start | bytes 1056776 | tf_op jit(solution)/shard_map/ppermute | solution.py:23
  93.2 16.3 %collective-permute-start.35 = (bf16[1376,256]{1,0:T(8,128)(2,1)S(1)}, bf16[1376,256]{1,0:T(8,128)(2,1)S(1)}, u32[]{:S(2)}, u32[]{:S(2)}) collective-permute-start(bf16[1376,256]{1,0:T(8,128)(2,1)S(1)} %copy-done.3), channel_id=1, source_target_pairs={{0,32},{1,225},{32,64},{33,1},{64,96},{65,33},{96,128},{97,65},{12... | collective-permute-start | bytes 2113544 | tf_op jit(solution)/shard_map/ppermute | solution.py:40
  97.8 24.0 %copy-start.6 = (f32[3,1376]{1,0:T(4,128)S(1)}, f32[3,1376]{1,0:T(4,128)}, u32[]{:S(2)}) copy-start(f32[3,1376]{1,0:T(4,128)} %gate_kernel.1) | copy-start | bytes 49540
  97.8 24.0 %copy-start.7 = (f32[3,1376]{1,0:T(4,128)S(1)}, f32[3,1376]{1,0:T(4,128)}, u32[]{:S(2)}) copy-start(f32[3,1376]{1,0:T(4,128)} %value_kernel.1) | copy-start | bytes 49540
  97.8 23.9 %collective-permute-start.26 = (bf16[128,1408]{1,0:T(8,128)(2,1)S(1)}, bf16[128,1408]{1,0:T(8,128)(2,1)S(1)}, u32[]{:S(2)}, u32[]{:S(2)}) collective-permute-start(bf16[128,1408]{1,0:T(8,128)(2,1)S(1)} %get-tuple-element.52), channel_id=1, source_target_pairs={{0,24},{8,0},{16,8},{24,16},{1,25},{9,1},{17,9},{25,17},{2,26},{10... | collective-permute-start | bytes 1081352 | tf_op jit(solution)/shard_map/ppermute | solution.py:23
  104.3 17.4 %collective-permute-start.29 = (bf16[128,1408]{1,0:T(8,128)(2,1)S(1)}, bf16[128,1408]{1,0:T(8,128)(2,1)S(1)}, u32[]{:S(2)}, u32[]{:S(2)}) collective-permute-start(bf16[128,1408]{1,0:T(8,128)(2,1)S(1)} %get-tuple-element.57), channel_id=1, source_target_pairs={{0,8},{8,16},{16,24},{24,0},{1,9},{9,17},{17,25},{25,1},{2,10},{10... | collective-permute-start | bytes 1081352 | tf_op jit(solution)/shard_map/ppermute | solution.py:23
  107.5 13.5 %collective-permute-start.30 = (bf16[128,1376]{1,0:T(8,128)(2,1)S(1)}, bf16[128,1376]{1,0:T(8,128)(2,1)S(1)}, u32[]{:S(2)}, u32[]{:S(2)}) collective-permute-start(bf16[128,1376]{1,0:T(8,128)(2,1)S(1)} %get-tuple-element.59), channel_id=1, source_target_pairs={{0,8},{8,16},{16,24},{24,0},{1,9},{9,17},{17,25},{25,1},{2,10},{10... | collective-permute-start | bytes 1056776 | tf_op jit(solution)/shard_map/ppermute | solution.py:23
  107.6 14.1 %collective-permute-start.31 = (bf16[128,1376]{1,0:T(8,128)(2,1)S(1)}, bf16[128,1376]{1,0:T(8,128)(2,1)S(1)}, u32[]{:S(2)}, u32[]{:S(2)}) collective-permute-start(bf16[128,1376]{1,0:T(8,128)(2,1)S(1)} %get-tuple-element.60), channel_id=1, source_target_pairs={{0,24},{8,0},{16,8},{24,16},{1,25},{9,1},{17,9},{25,17},{2,26},{10... | collective-permute-start | bytes 1056776 | tf_op jit(solution)/shard_map/ppermute | solution.py:23
  109.6 25.4 %collective-permute-start.36 = (bf16[1376,256]{1,0:T(8,128)(2,1)S(1)}, bf16[1376,256]{1,0:T(8,128)(2,1)S(1)}, u32[]{:S(2)}, u32[]{:S(2)}) collective-permute-start(bf16[1376,256]{1,0:T(8,128)(2,1)S(1)} %copy-done.3), channel_id=1, source_target_pairs={{0,224},{1,33},{32,0},{33,65},{64,32},{65,97},{96,64},{97,129},{12... | collective-permute-start | bytes 2113544 | tf_op jit(solution)/shard_map/ppermute | solution.py:40
  121.0 14.0 %collective-permute-start.37 = (bf16[1376,256]{1,0:T(8,128)(2,1)S(1)}, bf16[1376,256]{1,0:T(8,128)(2,1)S(1)}, u32[]{:S(2)}, u32[]{:S(2)}) collective-permute-start(bf16[1376,256]{1,0:T(8,128)(2,1)S(1)} %collective-permute-done.35.refs_1_), channel_id=1, source_target_pairs={{0,32},{1,225},{32,64},{33,1},{64,96},{65,33},{96,128},{97,65},{12... | collective-permute-start | bytes 2113544 | tf_op jit(solution)/shard_map/ppermute | solution.py:40
  123.5 10.7 %collective-permute-start.32 = (bf16[128,1376]{1,0:T(8,128)(2,1)S(1)}, bf16[128,1376]{1,0:T(8,128)(2,1)S(1)}, u32[]{:S(2)}, u32[]{:S(2)}) collective-permute-start(bf16[128,1376]{1,0:T(8,128)(2,1)S(1)} %shard_map.177.refs_0_), channel_id=1, source_target_pairs={{0,8},{1,25},{8,16},{9,1},{16,24},{17,9},{24,0},{25,17},{2,10},{3,... | collective-permute-start | bytes 1056776 | tf_op jit(solution)/shard_map/ppermute | solution.py:40
  126.1 10.0 %collective-permute-start.33 = (bf16[128,1376]{1,0:T(8,128)(2,1)S(1)}, bf16[128,1376]{1,0:T(8,128)(2,1)S(1)}, u32[]{:S(2)}, u32[]{:S(2)}) collective-permute-start(bf16[128,1376]{1,0:T(8,128)(2,1)S(1)} %shard_map.177.refs_0_), channel_id=1, source_target_pairs={{0,24},{1,9},{8,0},{9,17},{16,8},{17,25},{24,16},{25,1},{2,26},{3,... | collective-permute-start | bytes 1056776 | tf_op jit(solution)/shard_map/ppermute | solution.py:40
  134.1 7.4 %collective-permute-start.34 = (bf16[128,1376]{1,0:T(8,128)(2,1)S(1)}, bf16[128,1376]{1,0:T(8,128)(2,1)S(1)}, u32[]{:S(2)}, u32[]{:S(2)}) collective-permute-start(bf16[128,1376]{1,0:T(8,128)(2,1)S(1)} %collective-permute-done.32.refs_1_), channel_id=1, source_target_pairs={{0,8},{1,25},{8,16},{9,1},{16,24},{17,9},{24,0},{25,17},{2,10},{3,... | collective-permute-start | bytes 1056776 | tf_op jit(solution)/shard_map/ppermute | solution.py:40
  142.9 2.0 %collective-permute-start.38 = (bf16[4,256,256]{2,1,0:T(8,128)(2,1)S(1)}, bf16[4,256,256]{2,1,0:T(8,128)(2,1)S(1)}, u32[]{:S(2)}, u32[]{:S(2)}) collective-permute-start(bf16[4,256,256]{2,1,0:T(8,128)(2,1)S(1)} %shard_map.180), channel_id=1, source_target_pairs={{0,1},{1,0},{2,3},{3,2},{4,5},{5,4},{6,7},{7,6},{8,9},{9,8},{10,11... | collective-permute-start | bytes 1572872 | tf_op jit(solution)/shard_map/ppermute | solution.py:23
  145.1 7.3 %collective-permute-start.39 = (bf16[256,256]{1,0:T(8,128)(2,1)S(1)}, bf16[256,256]{1,0:T(8,128)(2,1)S(1)}, u32[]{:S(2)}, u32[]{:S(2)}) collective-permute-start(bf16[256,256]{1,0:T(8,128)(2,1)S(1)} %get-tuple-element.62), channel_id=1, source_target_pairs={{0,2},{2,4},{4,6},{6,0},{1,3},{3,5},{5,7},{7,1},{8,10},{10,12},{12... | collective-permute-start | bytes 393224 | tf_op jit(solution)/shard_map/ppermute | solution.py:23
  145.9 9.2 %collective-permute-start.40 = (bf16[256,256]{1,0:T(8,128)(2,1)S(1)}, bf16[256,256]{1,0:T(8,128)(2,1)S(1)}, u32[]{:S(2)}, u32[]{:S(2)}) collective-permute-start(bf16[256,256]{1,0:T(8,128)(2,1)S(1)} %get-tuple-element.63), channel_id=1, source_target_pairs={{0,4},{2,6},{4,0},{6,2},{1,5},{3,7},{5,1},{7,3},{8,12},{10,14},{12... | collective-permute-start | bytes 393224 | tf_op jit(solution)/shard_map/ppermute | solution.py:23
  148.8 6.5 %collective-permute-start.41 = (bf16[256,256]{1,0:T(8,128)(2,1)S(1)}, bf16[256,256]{1,0:T(8,128)(2,1)S(1)}, u32[]{:S(2)}, u32[]{:S(2)}) collective-permute-start(bf16[256,256]{1,0:T(8,128)(2,1)S(1)} %get-tuple-element.64), channel_id=1, source_target_pairs={{0,6},{2,0},{4,2},{6,4},{1,7},{3,1},{5,3},{7,5},{8,14},{10,8},{12,... | collective-permute-start | bytes 393224 | tf_op jit(solution)/shard_map/ppermute | solution.py:23
  155.4 7.3 %collective-permute-start.42 = (bf16[128,256]{1,0:T(8,128)(2,1)S(1)}, bf16[128,256]{1,0:T(8,128)(2,1)S(1)}, u32[]{:S(2)}, u32[]{:S(2)}) collective-permute-start(bf16[128,256]{1,0:T(8,128)(2,1)S(1)} %get-tuple-element.65), channel_id=1, source_target_pairs={{0,0},{1,16},{8,8},{9,24},{16,1},{17,17},{24,9},{25,25},{2,2},{3,1... | collective-permute-start | bytes 196616 | tf_op jit(solution)/shard_map/ppermute | solution.py:67
  160.5 3.8 %collective-permute-start.43 = (bf16[128,256]{1,0:T(8,128)(2,1)S(1)}, bf16[128,256]{1,0:T(8,128)(2,1)S(1)}, u32[]{:S(2)}, u32[]{:S(2)}) collective-permute-start(bf16[128,256]{1,0:T(8,128)(2,1)S(1)} %get-tuple-element.66), channel_id=1, source_target_pairs={{0,8},{1,24},{8,0},{9,16},{16,9},{17,25},{24,1},{25,17},{2,10},{3,... | collective-permute-start | bytes 196616 | tf_op jit(solution)/shard_map/ppermute | solution.py:67
  (10 other events, 128.6 us)

commit v2 on v1

--- a/solution.py
+++ b/solution.py
@@ -193,7 +193,7 @@
         scratch=[pltpu.VMEM((2 * inner, part), BF16), pltpu.SemaphoreType.DMA((2,))],
         hbm_in=range(2),
         hbm_out=range(1),
-        limit=62,
+        limit=61,
     )(gate_up.T, value_up.T)
     ups = gather_z(up)
     downs = gather_z(down_proj)
@@ -307,7 +307,10 @@
     merge_flops = 2 * own_rows * width * span
     merge_scratch = pltpu.VMEM((RING, length, width), BF16)
     (other,) = kernel_call(
-        merge_other_body, [((own_rows, span), BF16)], flops=merge_flops, scratch=[merge_scratch]
+        merge_other_body,
+        [((own_rows, span), BF16)],
+        flops=merge_flops,
+        scratch=[merge_scratch],
     )(*merges, *packs)
     received = swap_core(other)
 
@@ -372,7 +375,10 @@
 
     load_sems = pltpu.SemaphoreType.DMA((RING,))
     (weights,) = kernel_call(
-        load_body, [((2 * inner, 3 * part), BF16)], scratch=[load_sems], hbm_in=range(4)
+        load_body,
+        [((2 * inner, 3 * part), BF16)],
+        scratch=[load_sems],
+        hbm_in=range(4),
     )(gate_up.T, value_up.T, ups[1], ups[2])
 
     def up_far_body(*refs):
@@ -518,7 +524,10 @@
         move(*((refs[i], refs[RING].at[j]) for i, j in enumerate(order)), refs[RING + 1])
 
     (weights,) = kernel_call(
-        down_load_body, [((RING, inner, part), BF16)], scratch=[load_sems], hbm_in=range(4)
+        down_load_body,
+        [((RING, inner, part), BF16)],
+        scratch=[load_sems],
+        hbm_in=range(4),
     )(*downs)
 
 

time: 168 us -> 168 us (level)
  no operation moved by 1% of the time
where the time goes in v2:
time: 168 us; the launch traced here: 165 us
  waiting for transfers between devices  77.4 us (46%)
  starting transfers between devices  61.6 us (37%)
  Pallas kernels  21.8 us (13%)
  local copies, waits for them, and re-layouts  2.23 us (1%)
    ppermute x28, waiting for transfers between devices, shift(): lax.ppermute(value, axes, [(i, (i + by) % size) for i in range(size)])  47.4 us
    ppermute x28, starting transfers between devices, shift(): lax.ppermute(value, axes, [(i, (i + by) % size) for i in range(size)])  37.5 us
    ppermute x12, waiting for transfers between devices, shift_apart(): return lax.ppermute(value, (*axes, CORE), pairs)  22.5 us
    pallas_call x21, Pallas kernels, run(): pl.pallas_call(body, out_shape=[jax.ShapeDtypeStruct(*out) for out in out...  21.8 us
    ppermute x12, starting transfers between devices, shift_apart(): return lax.ppermute(value, (*axes, CORE), pairs)  14.5 us
    ppermute x4, starting transfers between devices, trade(): return lax.ppermute(value, (X, CORE), pairs)  9.65 us
    ppermute x4, waiting for transfers between devices, trade(): return lax.ppermute(value, (X, CORE), pairs)  7.54 us
  transfers between devices with their start and end apart: 44, of which 27 were waited for; matrix products, arithmetic and copies ran while one was open for 2% of the time, Pallas kernels for 8%

profile of v2, /device:TPU:4, one launch (start us, length us, event | category | flops | bytes accessed | tf_op | source)
XLA Modules:
  0.0 165.1 jit_solution(1722848324710456283)
XLA Ops:
  0.0 2.4 %shard_map.172 = bf16[2752,256]{1,0:T(8,128)(2,1)} custom-call(bf16[1376,256]{1,0:T(8,128)(2,1)} %bitcast.5, bf16[1376,256]{1,0:T(8,128)(2,1)} %bitcast.7), custom_call_target="tpu_custom_call" | custom-call | tf_op jit(solution)/shard_map/pallas_call | solution.py:75
  2.5 2.0 %collective-permute-start.23 = (bf16[2752,256]{1,0:T(8,128)(2,1)}, bf16[2752,256]{1,0:T(8,128)(2,1)S(1)}, u32[]{:S(2)}, u32[]{:S(2)}) collective-permute-start(bf16[2752,256]{1,0:T(8,128)(2,1)} %shard_map.172), channel_id=1, source_target_pairs={{0,32},{1,225},{32,64},{33,1},{64,96},{65,33},{96,128},{97,65},{12... | collective-permute-start | bytes 4227080 | tf_op jit(solution)/shard_map/ppermute | solution.py:40
  4.4 2.0 %shard_map.163 = (bf16[128,256]{1,0:T(8,128)(2,1)}, bf16[128,256]{1,0:T(8,128)(2,1)}, bf16[784,256]{1,0:T(8,128)(2,1)}) custom-call(bf16[128,512]{1,0:T(8,128)(2,1)} %tokens.1, bf16[256,256]{1,0:T(8,128)(2,1)} %gate.1, bf16[256,256]{1,0:T(8,128)(2,1)} %value.1, bf16[256,256]{1,0:T(8,128)(2,1)} %merge.1, bf16[16,128]{1,0:T(8,128)(2,1)} %bitcast.11), custom_call_target="tpu_custom_call" | custom-call | tf_op jit(solution)/shard_map/pallas_call | solution.py:75
  6.4 2.0 %collective-permute-start.6 = (bf16[784,256]{1,0:T(8,128)(2,1)}, bf16[784,256]{1,0:T(8,128)(2,1)S(1)}, u32[]{:S(2)}, u32[]{:S(2)}) collective-permute-start(bf16[784,256]{1,0:T(8,128)(2,1)} %get-tuple-element.38.refs_2_.refs_4_), channel_id=1, source_target_pairs={{0,32},{1,225},{32,64},{33,1},{64,96},{65,33},{96,128},{97,65},{12... | collective-permute-start | bytes 1204232 | tf_op jit(solution)/shard_map/ppermute | solution.py:40
  8.4 4.3 %collective-permute-start = (bf16[128,256]{1,0:T(8,128)(2,1)}, bf16[128,256]{1,0:T(8,128)(2,1)S(1)}, u32[]{:S(2)}, u32[]{:S(2)}) collective-permute-start(bf16[128,256]{1,0:T(8,128)(2,1)} %get-tuple-element.36), channel_id=1, source_target_pairs={{0,0},{1,16},{8,8},{9,24},{16,1},{17,17},{24,9},{25,25},{2,2},{3,1... | collective-permute-start | bytes 196616 | tf_op jit(solution)/shard_map/ppermute | solution.py:67
  12.9 2.8 %collective-permute-done.near = bf16[128,256]{1,0:T(8,128)(2,1)S(1)} collective-permute-done((bf16[128,256]{1,0:T(8,128)(2,1)}, bf16[128,256]{1,0:T(8,128)(2,1)S(1)}, u32[]{:S(2)}, u32[]{:S(2)}) %collective-permute-start) | collective-permute-done | bytes 65568 | tf_op jit(solution)/shard_map/ppermute | solution.py:67
  16.8 1.7 %collective-permute-start.2 = (bf16[256,256]{1,0:T(8,128)(2,1)S(1)}, bf16[256,256]{1,0:T(8,128)(2,1)S(1)}, u32[]{:S(2)}, u32[]{:S(2)}) collective-permute-start(bf16[256,256]{1,0:T(8,128)(2,1)S(1)} %shard_map.164.refs_0_), channel_id=1, source_target_pairs={{0,2},{2,4},{4,6},{6,0},{1,3},{3,5},{5,7},{7,1},{8,10},{10,12},{12... | collective-permute-start | bytes 393224 | tf_op jit(solution)/shard_map/ppermute | solution.py:23
  18.4 2.9 %collective-permute-start.3 = (bf16[256,256]{1,0:T(8,128)(2,1)S(1)}, bf16[256,256]{1,0:T(8,128)(2,1)S(1)}, u32[]{:S(2)}, u32[]{:S(2)}) collective-permute-start(bf16[256,256]{1,0:T(8,128)(2,1)S(1)} %shard_map.164.refs_0_), channel_id=1, source_target_pairs={{0,4},{2,6},{4,0},{6,2},{1,5},{3,7},{5,1},{7,3},{8,12},{10,14},{12... | collective-permute-start | bytes 393224 | tf_op jit(solution)/shard_map/ppermute | solution.py:23
  22.7 1.4 collective-permute-done.2.refs_1_
  24.1 2.5 %collective-permute-done.3.refs_2_ = bf16[256,256]{1,0:T(8,128)(2,1)S(1)} collective-permute-done((bf16[256,256]{1,0:T(8,128)(2,1)S(1)}, bf16[256,256]{1,0:T(8,128)(2,1)S(1)}, u32[]{:S(2)}, u32[]{:S(2)}) %collective-permute-start.3) | collective-permute-done | bytes 131104 | tf_op jit(solution)/shard_map/ppermute | solution.py:23
  29.6 1.4 pad_maximum_fusion
  32.4 6.0 %collective-permute-done.7.refs_4_.refs_6_ = bf16[784,256]{1,0:T(8,128)(2,1)S(1)} collective-permute-done((bf16[784,256]{1,0:T(8,128)(2,1)}, bf16[784,256]{1,0:T(8,128)(2,1)S(1)}, u32[]{:S(2)}, u32[]{:S(2)}) %collective-permute-start.7) | collective-permute-done | bytes 401440 | tf_op jit(solution)/shard_map/ppermute | solution.py:40
  38.4 1.5 collective-permute-done.8.refs_5_.refs_7_
  40.7 2.0 %shard_map.166 = (bf16[4,512,256]{2,1,0:T(8,128)(2,1)S(1)}, bf16[128,640]{1,0:T(8,128)(2,1)S(1)}, bf16[128,640]{1,0:T(8,128)(2,1)S(1)}, bf16[128,640]{1,0:T(8,128)(2,1)S(1)}, bf16[128,640]{1,0:T(8,128)(2,1)S(1)}) custom-call(bf16[4,256,256]{2,1,0:T(8,128)(2,1)S(1)} %shard_map.165.refs_0_, bf16[4,256,256]{2,1,0:T(8,128)(2,1)} %collective-permute-done.5.refs_1_, ...), custom_call_target="tpu_custom_call" | custom-call | flops 536870912 | tf_op jit(solution)/shard_map/pallas_call | solution.py:75
  43.7 2.1 %collective-permute-start.11 = (bf16[128,640]{1,0:T(8,128)(2,1)S(1)}, bf16[128,640]{1,0:T(8,128)(2,1)S(1)}, u32[]{:S(2)}, u32[]{:S(2)}) collective-permute-start(bf16[128,640]{1,0:T(8,128)(2,1)S(1)} %get-tuple-element.42), channel_id=1, source_target_pairs={{0,8},{8,16},{16,24},{24,0},{1,9},{9,17},{17,25},{25,1},{2,10},{10... | collective-permute-start | bytes 491528 | tf_op jit(solution)/shard_map/ppermute | solution.py:23
  47.5 1.7 %collective-permute-start.25 = (bf16[2752,256]{1,0:T(8,128)(2,1)S(1)}, bf16[2752,256]{1,0:T(8,128)(2,1)S(1)}, u32[]{:S(2)}, u32[]{:S(2)}) collective-permute-start(bf16[2752,256]{1,0:T(8,128)(2,1)S(1)} %collective-permute-done.23.first), channel_id=1, source_target_pairs={{0,32},{1,225},{32,64},{33,1},{64,96},{65,33},{96,128},{97,65},{12... | collective-permute-start | bytes 4227080 | tf_op jit(solution)/shard_map/ppermute | solution.py:40
  49.2 2.2 %collective-permute-done.10.refs_2_ = bf16[128,640]{1,0:T(8,128)(2,1)S(1)} collective-permute-done((bf16[128,640]{1,0:T(8,128)(2,1)S(1)}, bf16[128,640]{1,0:T(8,128)(2,1)S(1)}, u32[]{:S(2)}, u32[]{:S(2)}) %collective-permute-start.10) | collective-permute-done | bytes 163872 | tf_op jit(solution)/shard_map/ppermute | solution.py:23
  51.3 2.0 %collective-permute-done.11.refs_3_ = bf16[128,640]{1,0:T(8,128)(2,1)S(1)} collective-permute-done((bf16[128,640]{1,0:T(8,128)(2,1)S(1)}, bf16[128,640]{1,0:T(8,128)(2,1)S(1)}, u32[]{:S(2)}, u32[]{:S(2)}) %collective-permute-start.11) | collective-permute-done | bytes 163872 | tf_op jit(solution)/shard_map/ppermute | solution.py:23
  53.9 2.9 %collective-permute-start.12 = (bf16[128,256]{1,0:T(8,128)(2,1)S(1)}, bf16[128,256]{1,0:T(8,128)(2,1)S(1)}, u32[]{:S(2)}, u32[]{:S(2)}) collective-permute-start(bf16[128,256]{1,0:T(8,128)(2,1)S(1)} %shard_map.167.refs_0_), channel_id=1, source_target_pairs={{0,8},{8,16},{16,24},{24,0},{1,9},{9,17},{17,25},{25,1},{2,10},{10... | collective-permute-start | bytes 196616 | tf_op jit(solution)/shard_map/ppermute | solution.py:23
  56.8 2.0 %collective-permute-start.14 = (bf16[128,256]{1,0:T(8,128)(2,1)S(1)}, bf16[128,256]{1,0:T(8,128)(2,1)S(1)}, u32[]{:S(2)}, u32[]{:S(2)}) collective-permute-start(bf16[128,256]{1,0:T(8,128)(2,1)S(1)} %shard_map.167.refs_0_), channel_id=1, source_target_pairs={{0,24},{8,0},{16,8},{24,16},{1,25},{9,1},{17,9},{25,17},{2,26},{10... | collective-permute-start | bytes 196616 | tf_op jit(solution)/shard_map/ppermute | solution.py:23
  58.8 3.7 %collective-permute-done.13.refs_2_ = bf16[128,256]{1,0:T(8,128)(2,1)S(1)} collective-permute-done((bf16[128,256]{1,0:T(8,128)(2,1)S(1)}, bf16[128,256]{1,0:T(8,128)(2,1)S(1)}, u32[]{:S(2)}, u32[]{:S(2)}) %collective-permute-start.13) | collective-permute-done | bytes 65568 | tf_op jit(solution)/shard_map/ppermute | solution.py:23
  63.0 1.9 %collective-permute-done.15.refs_8_ = bf16[256,1024]{1,0:T(8,128)(2,1)S(1)} collective-permute-done((bf16[256,1024]{1,0:T(8,128)(2,1)S(1)}, bf16[256,1024]{1,0:T(8,128)(2,1)S(1)}, u32[]{:S(2)}, u32[]{:S(2)}) %collective-permute-start.15) | collective-permute-done | bytes 524320 | tf_op jit(solution)/shard_map/ppermute | solution.py:23
  66.4 3.0 %collective-permute-start.17 = (bf16[64,1024]{1,0:T(8,128)(2,1)S(1)}, bf16[64,1024]{1,0:T(8,128)(2,1)S(1)}, u32[]{:S(2)}, u32[]{:S(2)}) collective-permute-start(bf16[64,1024]{1,0:T(8,128)(2,1)S(1)} %get-tuple-element.46), channel_id=1, source_target_pairs={{0,4},{2,6},{4,0},{6,2},{1,5},{3,7},{5,1},{7,3},{8,12},{10,14},{12... | collective-permute-start | bytes 393224 | tf_op jit(solution)/shard_map/ppermute | solution.py:23
  70.3 1.9 %collective-permute-done.16.first = bf16[64,1024]{1,0:T(8,128)(2,1)S(1)} collective-permute-done((bf16[64,1024]{1,0:T(8,128)(2,1)S(1)}, bf16[64,1024]{1,0:T(8,128)(2,1)S(1)}, u32[]{:S(2)}, u32[]{:S(2)}) %collective-permute-start.16) | collective-permute-done | bytes 131104 | tf_op jit(solution)/shard_map/ppermute | solution.py:23
  72.2 3.5 %collective-permute-done.17.second = bf16[64,1024]{1,0:T(8,128)(2,1)S(1)} collective-permute-done((bf16[64,1024]{1,0:T(8,128)(2,1)S(1)}, bf16[64,1024]{1,0:T(8,128)(2,1)S(1)}, u32[]{:S(2)}, u32[]{:S(2)}) %collective-permute-start.17) | collective-permute-done | bytes 131104 | tf_op jit(solution)/shard_map/ppermute | solution.py:23
  75.8 1.5 collective-permute-start.19
  77.3 2.5 %collective-permute-start.20 = (bf16[64,1024]{1,0:T(8,128)(2,1)S(1)}, bf16[64,1024]{1,0:T(8,128)(2,1)S(1)}, u32[]{:S(2)}, u32[]{:S(2)}) collective-permute-start(bf16[64,1024]{1,0:T(8,128)(2,1)S(1)} %shard_map.170.refs_0_), channel_id=1, source_target_pairs={{0,4},{2,6},{4,0},{6,2},{1,5},{3,7},{5,1},{7,3},{8,12},{10,14},{12... | collective-permute-start | bytes 393224 | tf_op jit(solution)/shard_map/ppermute | solution.py:23
  80.6 1.9 %collective-permute-done.19.refs_1_ = bf16[64,1024]{1,0:T(8,128)(2,1)S(1)} collective-permute-done((bf16[64,1024]{1,0:T(8,128)(2,1)S(1)}, bf16[64,1024]{1,0:T(8,128)(2,1)S(1)}, u32[]{:S(2)}, u32[]{:S(2)}) %collective-permute-start.19) | collective-permute-done | bytes 131104 | tf_op jit(solution)/shard_map/ppermute | solution.py:23
  82.4 3.3 %collective-permute-done.20.refs_2_ = bf16[64,1024]{1,0:T(8,128)(2,1)S(1)} collective-permute-done((bf16[64,1024]{1,0:T(8,128)(2,1)S(1)}, bf16[64,1024]{1,0:T(8,128)(2,1)S(1)}, u32[]{:S(2)}, u32[]{:S(2)}) %collective-permute-start.20) | collective-permute-done | bytes 131104 | tf_op jit(solution)/shard_map/ppermute | solution.py:23
  86.3 1.5 collective-permute-done.22.refs_1_
  87.8 3.3 %shard_map.174 = (bf16[128,1408]{1,0:T(8,128)(2,1)S(1)}, bf16[128,1376]{1,0:T(8,128)(2,1)S(1)}, bf16[4,128,1024]{2,1,0:T(8,128)(2,1)S(1)}, f32[4,128,128]{2,1,0:T(8,128)S(1)}, bf16[2752,256]{1,0:T(8,128)(2,1)S(1)}) custom-call(bf16[4,64,1024]{2,1,0:T(8,128)(2,1)S(1)} %shard_map.171.refs_0_.refs_2_, bf16[4,64,1024]{2,1,0:T(8,128)(2,1)S(1)} %collective-permute-done.22.refs_1_, ...), custom_call_target="tpu_custom_call" | custom-call | flops 721420288 | tf_op jit(solution)/shard_map/pallas_call | solution.py:75
  91.1 1.6 collective-permute-start.27
  94.0 3.7 %shard_map.175 = (bf16[128,1408]{1,0:T(8,128)(2,1)S(1)}, bf16[128,1376]{1,0:T(8,128)(2,1)S(1)}, f32[128,1408]{1,0:T(8,128)S(1)}, f32[128,1376]{1,0:T(8,128)S(1)}...) custom-call(bf16[4,128,1024]{2,1,0:T(8,128)(2,1)S(1)} %get-tuple-element.48.scaled, ...), custom_call_target="tpu_custom_call" | custom-call | flops 2164260864 | tf_op jit(solution)/shard_map/pallas_call | solution.py:75
  98.5 5.5 %collective-permute-done.28.value_two = bf16[128,1376]{1,0:T(8,128)(2,1)S(1)} collective-permute-done((bf16[128,1376]{1,0:T(8,128)(2,1)S(1)}, bf16[128,1376]{1,0:T(8,128)(2,1)S(1)}, u32[]{:S(2)}, u32[]{:S(2)}) %collective-permute-start.28) | collective-permute-done | bytes 352288 | tf_op jit(solution)/shard_map/ppermute | solution.py:23
  104.3 3.2 %collective-permute-start.29 = (bf16[128,1408]{1,0:T(8,128)(2,1)S(1)}, bf16[128,1408]{1,0:T(8,128)(2,1)S(1)}, u32[]{:S(2)}, u32[]{:S(2)}) collective-permute-start(bf16[128,1408]{1,0:T(8,128)(2,1)S(1)} %get-tuple-element.57), channel_id=1, source_target_pairs={{0,8},{8,16},{16,24},{24,0},{1,9},{9,17},{17,25},{25,1},{2,10},{10... | collective-permute-start | bytes 1081352 | tf_op jit(solution)/shard_map/ppermute | solution.py:23
  107.6 1.9 %collective-permute-start.31 = (bf16[128,1376]{1,0:T(8,128)(2,1)S(1)}, bf16[128,1376]{1,0:T(8,128)(2,1)S(1)}, u32[]{:S(2)}, u32[]{:S(2)}) collective-permute-start(bf16[128,1376]{1,0:T(8,128)(2,1)S(1)} %get-tuple-element.60), channel_id=1, source_target_pairs={{0,24},{8,0},{16,8},{24,16},{1,25},{9,1},{17,9},{25,17},{2,26},{10... | collective-permute-start | bytes 1056776 | tf_op jit(solution)/shard_map/ppermute | solution.py:23
  109.6 2.2 %collective-permute-start.36 = (bf16[1376,256]{1,0:T(8,128)(2,1)S(1)}, bf16[1376,256]{1,0:T(8,128)(2,1)S(1)}, u32[]{:S(2)}, u32[]{:S(2)}) collective-permute-start(bf16[1376,256]{1,0:T(8,128)(2,1)S(1)} %copy-done.3), channel_id=1, source_target_pairs={{0,224},{1,33},{32,0},{33,65},{64,32},{65,97},{96,64},{97,129},{12... | collective-permute-start | bytes 2113544 | tf_op jit(solution)/shard_map/ppermute | solution.py:40
  111.8 9.2 %collective-permute-done.30.value_near = bf16[128,1376]{1,0:T(8,128)(2,1)S(1)} collective-permute-done((bf16[128,1376]{1,0:T(8,128)(2,1)S(1)}, bf16[128,1376]{1,0:T(8,128)(2,1)S(1)}, u32[]{:S(2)}, u32[]{:S(2)}) %collective-permute-start.30) | collective-permute-done | bytes 352288 | tf_op jit(solution)/shard_map/ppermute | solution.py:23
  121.7 1.7 %shard_map.177.refs_0_ = bf16[128,1376]{1,0:T(8,128)(2,1)S(1)} custom-call(f32[128,1408]{1,0:T(8,128)S(1)} %get-tuple-element.51.gate_own, bf16[128,1408]{1,0:T(8,128)(2,1)S(1)} %collective-permute-done.26.gate_near, bf16[128,1408]{1,0:T(8,128)(2,1)S(1)} %collective-permute-done.29.gate_join, f32[128,1376]{1,0:T(8,128)S(1)} %get-tuple-element.58.value_own, ...), custom_call_target="tpu_custom_call" | custom-call | flops 16777216 | tf_op jit(solution)/shard_map/pallas_call | solution.py:75
  123.5 2.6 %collective-permute-start.32 = (bf16[128,1376]{1,0:T(8,128)(2,1)S(1)}, bf16[128,1376]{1,0:T(8,128)(2,1)S(1)}, u32[]{:S(2)}, u32[]{:S(2)}) collective-permute-start(bf16[128,1376]{1,0:T(8,128)(2,1)S(1)} %shard_map.177.refs_0_), channel_id=1, source_target_pairs={{0,8},{1,25},{8,16},{9,1},{16,24},{17,9},{24,0},{25,17},{2,10},{3,... | collective-permute-start | bytes 1056776 | tf_op jit(solution)/shard_map/ppermute | solution.py:40
  126.1 8.1 %collective-permute-done.32.refs_1_ = bf16[128,1376]{1,0:T(8,128)(2,1)S(1)} collective-permute-done((bf16[128,1376]{1,0:T(8,128)(2,1)S(1)}, bf16[128,1376]{1,0:T(8,128)(2,1)S(1)}, u32[]{:S(2)}, u32[]{:S(2)}) %collective-permute-start.32) | collective-permute-done | bytes 352288 | tf_op jit(solution)/shard_map/ppermute | solution.py:40
  136.1 5.5 %collective-permute-done.34.refs_3_ = bf16[128,1376]{1,0:T(8,128)(2,1)S(1)} collective-permute-done((bf16[128,1376]{1,0:T(8,128)(2,1)S(1)}, bf16[128,1376]{1,0:T(8,128)(2,1)S(1)}, u32[]{:S(2)}, u32[]{:S(2)}) %collective-permute-start.34) | collective-permute-done | bytes 352288 | tf_op jit(solution)/shard_map/ppermute | solution.py:40
  145.9 2.9 %collective-permute-start.40 = (bf16[256,256]{1,0:T(8,128)(2,1)S(1)}, bf16[256,256]{1,0:T(8,128)(2,1)S(1)}, u32[]{:S(2)}, u32[]{:S(2)}) collective-permute-start(bf16[256,256]{1,0:T(8,128)(2,1)S(1)} %get-tuple-element.63), channel_id=1, source_target_pairs={{0,4},{2,6},{4,0},{6,2},{1,5},{3,7},{5,1},{7,3},{8,12},{10,14},{12... | collective-permute-start | bytes 393224 | tf_op jit(solution)/shard_map/ppermute | solution.py:23
  149.1 3.2 %collective-permute-done.39.first = bf16[256,256]{1,0:T(8,128)(2,1)S(1)} collective-permute-done((bf16[256,256]{1,0:T(8,128)(2,1)S(1)}, bf16[256,256]{1,0:T(8,128)(2,1)S(1)}, u32[]{:S(2)}, u32[]{:S(2)}) %collective-permute-start.39) | collective-permute-done | bytes 131104 | tf_op jit(solution)/shard_map/ppermute | solution.py:23
  152.3 2.7 %collective-permute-done.40.second = bf16[256,256]{1,0:T(8,128)(2,1)S(1)} collective-permute-done((bf16[256,256]{1,0:T(8,128)(2,1)S(1)}, bf16[256,256]{1,0:T(8,128)(2,1)S(1)}, u32[]{:S(2)}, u32[]{:S(2)}) %collective-permute-start.40) | collective-permute-done | bytes 131104 | tf_op jit(solution)/shard_map/ppermute | solution.py:23
  155.4 5.1 %collective-permute-start.42 = (bf16[128,256]{1,0:T(8,128)(2,1)S(1)}, bf16[128,256]{1,0:T(8,128)(2,1)S(1)}, u32[]{:S(2)}, u32[]{:S(2)}) collective-permute-start(bf16[128,256]{1,0:T(8,128)(2,1)S(1)} %get-tuple-element.65), channel_id=1, source_target_pairs={{0,0},{1,16},{8,8},{9,24},{16,1},{17,17},{24,9},{25,25},{2,2},{3,1... | collective-permute-start | bytes 196616 | tf_op jit(solution)/shard_map/ppermute | solution.py:67
  160.6 2.1 %collective-permute-done.42.near = bf16[128,256]{1,0:T(8,128)(2,1)S(1)} collective-permute-done((bf16[128,256]{1,0:T(8,128)(2,1)S(1)}, bf16[128,256]{1,0:T(8,128)(2,1)S(1)}, u32[]{:S(2)}, u32[]{:S(2)}) %collective-permute-start.42) | collective-permute-done | bytes 65568 | tf_op jit(solution)/shard_map/ppermute | solution.py:67
  162.7 1.6 collective-permute-done.43.far
  (93 shorter events, 25.8 us)
Async XLA Ops:
  2.5 45.0 %collective-permute-start.23 = (bf16[2752,256]{1,0:T(8,128)(2,1)}, bf16[2752,256]{1,0:T(8,128)(2,1)S(1)}, u32[]{:S(2)}, u32[]{:S(2)}) collective-permute-start(bf16[2752,256]{1,0:T(8,128)(2,1)} %shard_map.172), channel_id=1, source_target_pairs={{0,32},{1,225},{32,64},{33,1},{64,96},{65,33},{96,128},{97,65},{12... | collective-permute-start | bytes 4227080 | tf_op jit(solution)/shard_map/ppermute | solution.py:40
  6.4 33.5 %copy-start = (bf16[784,256]{1,0:T(8,128)(2,1)S(1)}, bf16[784,256]{1,0:T(8,128)(2,1)}, u32[]{:S(2)}) copy-start(bf16[784,256]{1,0:T(8,128)(2,1)} %get-tuple-element.38.refs_2_.refs_4_) | copy-start | bytes 1204228
  6.4 23.1 %collective-permute-start.6 = (bf16[784,256]{1,0:T(8,128)(2,1)}, bf16[784,256]{1,0:T(8,128)(2,1)S(1)}, u32[]{:S(2)}, u32[]{:S(2)}) collective-permute-start(bf16[784,256]{1,0:T(8,128)(2,1)} %get-tuple-element.38.refs_2_.refs_4_), channel_id=1, source_target_pairs={{0,32},{1,225},{32,64},{33,1},{64,96},{65,33},{96,128},{97,65},{12... | collective-permute-start | bytes 1204232 | tf_op jit(solution)/shard_map/ppermute | solution.py:40
  8.4 7.3 %collective-permute-start = (bf16[128,256]{1,0:T(8,128)(2,1)}, bf16[128,256]{1,0:T(8,128)(2,1)S(1)}, u32[]{:S(2)}, u32[]{:S(2)}) collective-permute-start(bf16[128,256]{1,0:T(8,128)(2,1)} %get-tuple-element.36), channel_id=1, source_target_pairs={{0,0},{1,16},{8,8},{9,24},{16,1},{17,17},{24,9},{25,25},{2,2},{3,1... | collective-permute-start | bytes 196616 | tf_op jit(solution)/shard_map/ppermute | solution.py:67
  12.8 4.0 %collective-permute-start.1 = (bf16[128,256]{1,0:T(8,128)(2,1)}, bf16[128,256]{1,0:T(8,128)(2,1)S(1)}, u32[]{:S(2)}, u32[]{:S(2)}) collective-permute-start(bf16[128,256]{1,0:T(8,128)(2,1)} %get-tuple-element.37), channel_id=1, source_target_pairs={{0,8},{1,24},{8,0},{9,16},{16,9},{17,25},{24,1},{25,17},{2,10},{3,... | collective-permute-start | bytes 196616 | tf_op jit(solution)/shard_map/ppermute | solution.py:67
  16.8 7.3 %collective-permute-start.2 = (bf16[256,256]{1,0:T(8,128)(2,1)S(1)}, bf16[256,256]{1,0:T(8,128)(2,1)S(1)}, u32[]{:S(2)}, u32[]{:S(2)}) collective-permute-start(bf16[256,256]{1,0:T(8,128)(2,1)S(1)} %shard_map.164.refs_0_), channel_id=1, source_target_pairs={{0,2},{2,4},{4,6},{6,0},{1,3},{3,5},{5,7},{7,1},{8,10},{10,12},{12... | collective-permute-start | bytes 393224 | tf_op jit(solution)/shard_map/ppermute | solution.py:23
  18.4 8.2 %collective-permute-start.3 = (bf16[256,256]{1,0:T(8,128)(2,1)S(1)}, bf16[256,256]{1,0:T(8,128)(2,1)S(1)}, u32[]{:S(2)}, u32[]{:S(2)}) collective-permute-start(bf16[256,256]{1,0:T(8,128)(2,1)S(1)} %shard_map.164.refs_0_), channel_id=1, source_target_pairs={{0,4},{2,6},{4,0},{6,2},{1,5},{3,7},{5,1},{7,3},{8,12},{10,14},{12... | collective-permute-start | bytes 393224 | tf_op jit(solution)/shard_map/ppermute | solution.py:23
  21.3 5.4 %collective-permute-start.4 = (bf16[256,256]{1,0:T(8,128)(2,1)S(1)}, bf16[256,256]{1,0:T(8,128)(2,1)S(1)}, u32[]{:S(2)}, u32[]{:S(2)}) collective-permute-start(bf16[256,256]{1,0:T(8,128)(2,1)S(1)} %shard_map.164.refs_0_), channel_id=1, source_target_pairs={{0,6},{2,0},{4,2},{6,4},{1,7},{3,1},{5,3},{7,5},{8,14},{10,8},{12,... | collective-permute-start | bytes 393224 | tf_op jit(solution)/shard_map/ppermute | solution.py:23
  26.7 11.7 %collective-permute-start.5 = (bf16[4,256,256]{2,1,0:T(8,128)(2,1)S(1)}, bf16[4,256,256]{2,1,0:T(8,128)(2,1)}, u32[]{:S(2)}, u32[]{:S(2)}) collective-permute-start(bf16[4,256,256]{2,1,0:T(8,128)(2,1)S(1)} %shard_map.165.refs_0_), channel_id=1, source_target_pairs={{0,1},{1,0},{2,3},{3,2},{4,5},{5,4},{6,7},{7,6},{8,9},{9,8},{10,11... | collective-permute-start | bytes 1572872 | tf_op jit(solution)/shard_map/ppermute | solution.py:23
  26.8 11.6 %collective-permute-start.7 = (bf16[784,256]{1,0:T(8,128)(2,1)}, bf16[784,256]{1,0:T(8,128)(2,1)S(1)}, u32[]{:S(2)}, u32[]{:S(2)}) collective-permute-start(bf16[784,256]{1,0:T(8,128)(2,1)} %get-tuple-element.38.refs_2_.refs_4_), channel_id=1, source_target_pairs={{0,224},{1,33},{32,0},{33,65},{64,32},{65,97},{96,64},{97,129},{12... | collective-permute-start | bytes 1204232 | tf_op jit(solution)/shard_map/ppermute | solution.py:40
  29.5 10.4 %collective-permute-start.8 = (bf16[784,256]{1,0:T(8,128)(2,1)S(1)}, bf16[784,256]{1,0:T(8,128)(2,1)S(1)}, u32[]{:S(2)}, u32[]{:S(2)}) collective-permute-start(bf16[784,256]{1,0:T(8,128)(2,1)S(1)} %collective-permute-done.6.refs_3_.refs_5_), channel_id=1, source_target_pairs={{0,32},{1,225},{32,64},{33,1},{64,96},{65,33},{96,128},{97,65},{12... | collective-permute-start | bytes 1204232 | tf_op jit(solution)/shard_map/ppermute | solution.py:40
  29.5 23.8 %copy-start.10 = (f32[2,128]{1,0:T(2,128)S(1)}, f32[2,128]{1,0:T(2,128)}, u32[]{:S(2)}) copy-start(f32[2,128]{1,0:T(2,128)} %refs_6_.1) | copy-start | bytes 3076
  42.7 8.7 %collective-permute-start.10 = (bf16[128,640]{1,0:T(8,128)(2,1)S(1)}, bf16[128,640]{1,0:T(8,128)(2,1)S(1)}, u32[]{:S(2)}, u32[]{:S(2)}) collective-permute-start(bf16[128,640]{1,0:T(8,128)(2,1)S(1)} %get-tuple-element.41), channel_id=1, source_target_pairs={{0,16},{8,24},{16,0},{24,8},{1,17},{9,25},{17,1},{25,9},{2,18},{10... | collective-permute-start | bytes 491528 | tf_op jit(solution)/shard_map/ppermute | solution.py:23
  43.7 9.6 %collective-permute-start.11 = (bf16[128,640]{1,0:T(8,128)(2,1)S(1)}, bf16[128,640]{1,0:T(8,128)(2,1)S(1)}, u32[]{:S(2)}, u32[]{:S(2)}) collective-permute-start(bf16[128,640]{1,0:T(8,128)(2,1)S(1)} %get-tuple-element.42), channel_id=1, source_target_pairs={{0,8},{8,16},{16,24},{24,0},{1,9},{9,17},{17,25},{25,1},{2,10},{10... | collective-permute-start | bytes 491528 | tf_op jit(solution)/shard_map/ppermute | solution.py:23
  45.8 7.6 %collective-permute-start.9 = (bf16[128,640]{1,0:T(8,128)(2,1)S(1)}, bf16[128,640]{1,0:T(8,128)(2,1)S(1)}, u32[]{:S(2)}, u32[]{:S(2)}) collective-permute-start(bf16[128,640]{1,0:T(8,128)(2,1)S(1)} %get-tuple-element.40), channel_id=1, source_target_pairs={{0,24},{8,0},{16,8},{24,16},{1,25},{9,1},{17,9},{25,17},{2,26},{10... | collective-permute-start | bytes 491528 | tf_op jit(solution)/shard_map/ppermute | solution.py:23
  47.1 38.7 %collective-permute-start.24 = (bf16[2752,256]{1,0:T(8,128)(2,1)S(1)}, bf16[2752,256]{1,0:T(8,128)(2,1)S(1)}, u32[]{:S(2)}, u32[]{:S(2)}) collective-permute-start(bf16[2752,256]{1,0:T(8,128)(2,1)S(1)} %copy-done.11), channel_id=1, source_target_pairs={{0,224},{1,33},{32,0},{33,65},{64,32},{65,97},{96,64},{97,129},{12... | collective-permute-start | bytes 4227080 | tf_op jit(solution)/shard_map/ppermute | solution.py:40
  47.5 40.3 %collective-permute-start.25 = (bf16[2752,256]{1,0:T(8,128)(2,1)S(1)}, bf16[2752,256]{1,0:T(8,128)(2,1)S(1)}, u32[]{:S(2)}, u32[]{:S(2)}) collective-permute-start(bf16[2752,256]{1,0:T(8,128)(2,1)S(1)} %collective-permute-done.23.first), channel_id=1, source_target_pairs={{0,32},{1,225},{32,64},{33,1},{64,96},{65,33},{96,128},{97,65},{12... | collective-permute-start | bytes 4227080 | tf_op jit(solution)/shard_map/ppermute | solution.py:40
  53.9 5.0 %collective-permute-start.12 = (bf16[128,256]{1,0:T(8,128)(2,1)S(1)}, bf16[128,256]{1,0:T(8,128)(2,1)S(1)}, u32[]{:S(2)}, u32[]{:S(2)}) collective-permute-start(bf16[128,256]{1,0:T(8,128)(2,1)S(1)} %shard_map.167.refs_0_), channel_id=1, source_target_pairs={{0,8},{8,16},{16,24},{24,0},{1,9},{9,17},{17,25},{25,1},{2,10},{10... | collective-permute-start | bytes 196616 | tf_op jit(solution)/shard_map/ppermute | solution.py:23
  56.8 5.8 %collective-permute-start.13 = (bf16[128,256]{1,0:T(8,128)(2,1)S(1)}, bf16[128,256]{1,0:T(8,128)(2,1)S(1)}, u32[]{:S(2)}, u32[]{:S(2)}) collective-permute-start(bf16[128,256]{1,0:T(8,128)(2,1)S(1)} %shard_map.167.refs_0_), channel_id=1, source_target_pairs={{0,16},{8,24},{16,0},{24,8},{1,17},{9,25},{17,1},{25,9},{2,18},{10... | collective-permute-start | bytes 196616 | tf_op jit(solution)/shard_map/ppermute | solution.py:23
  56.8 5.8 %collective-permute-start.14 = (bf16[128,256]{1,0:T(8,128)(2,1)S(1)}, bf16[128,256]{1,0:T(8,128)(2,1)S(1)}, u32[]{:S(2)}, u32[]{:S(2)}) collective-permute-start(bf16[128,256]{1,0:T(8,128)(2,1)S(1)} %shard_map.167.refs_0_), channel_id=1, source_target_pairs={{0,24},{8,0},{16,8},{24,16},{1,25},{9,1},{17,9},{25,17},{2,26},{10... | collective-permute-start | bytes 196616 | tf_op jit(solution)/shard_map/ppermute | solution.py:23
  62.9 2.0 %collective-permute-start.15 = (bf16[256,1024]{1,0:T(8,128)(2,1)S(1)}, bf16[256,1024]{1,0:T(8,128)(2,1)S(1)}, u32[]{:S(2)}, u32[]{:S(2)}) collective-permute-start(bf16[256,1024]{1,0:T(8,128)(2,1)S(1)} %shard_map.168), channel_id=1, source_target_pairs={{0,1},{1,0},{2,3},{3,2},{4,5},{5,4},{6,7},{7,6},{8,9},{9,8},{10,11... | collective-permute-start | bytes 1572872 | tf_op jit(solution)/shard_map/ppermute | solution.py:23
  65.3 6.9 %collective-permute-start.16 = (bf16[64,1024]{1,0:T(8,128)(2,1)S(1)}, bf16[64,1024]{1,0:T(8,128)(2,1)S(1)}, u32[]{:S(2)}, u32[]{:S(2)}) collective-permute-start(bf16[64,1024]{1,0:T(8,128)(2,1)S(1)} %get-tuple-element.45), channel_id=1, source_target_pairs={{0,2},{2,4},{4,6},{6,0},{1,3},{3,5},{5,7},{7,1},{8,10},{10,12},{12... | collective-permute-start | bytes 393224 | tf_op jit(solution)/shard_map/ppermute | solution.py:23
  66.4 9.3 %collective-permute-start.17 = (bf16[64,1024]{1,0:T(8,128)(2,1)S(1)}, bf16[64,1024]{1,0:T(8,128)(2,1)S(1)}, u32[]{:S(2)}, u32[]{:S(2)}) collective-permute-start(bf16[64,1024]{1,0:T(8,128)(2,1)S(1)} %get-tuple-element.46), channel_id=1, source_target_pairs={{0,4},{2,6},{4,0},{6,2},{1,5},{3,7},{5,1},{7,3},{8,12},{10,14},{12... | collective-permute-start | bytes 393224 | tf_op jit(solution)/shard_map/ppermute | solution.py:23
  69.4 6.3 %collective-permute-start.18 = (bf16[64,1024]{1,0:T(8,128)(2,1)S(1)}, bf16[64,1024]{1,0:T(8,128)(2,1)S(1)}, u32[]{:S(2)}, u32[]{:S(2)}) collective-permute-start(bf16[64,1024]{1,0:T(8,128)(2,1)S(1)} %get-tuple-element.47), channel_id=1, source_target_pairs={{0,6},{2,0},{4,2},{6,4},{1,7},{3,1},{5,3},{7,5},{8,14},{10,8},{12,... | collective-permute-start | bytes 393224 | tf_op jit(solution)/shard_map/ppermute | solution.py:23
  75.8 6.6 %collective-permute-start.19 = (bf16[64,1024]{1,0:T(8,128)(2,1)S(1)}, bf16[64,1024]{1,0:T(8,128)(2,1)S(1)}, u32[]{:S(2)}, u32[]{:S(2)}) collective-permute-start(bf16[64,1024]{1,0:T(8,128)(2,1)S(1)} %shard_map.170.refs_0_), channel_id=1, source_target_pairs={{0,2},{2,4},{4,6},{6,0},{1,3},{3,5},{5,7},{7,1},{8,10},{10,12},{12... | collective-permute-start | bytes 393224 | tf_op jit(solution)/shard_map/ppermute | solution.py:23
  77.3 8.4 %collective-permute-start.20 = (bf16[64,1024]{1,0:T(8,128)(2,1)S(1)}, bf16[64,1024]{1,0:T(8,128)(2,1)S(1)}, u32[]{:S(2)}, u32[]{:S(2)}) collective-permute-start(bf16[64,1024]{1,0:T(8,128)(2,1)S(1)} %shard_map.170.refs_0_), channel_id=1, source_target_pairs={{0,4},{2,6},{4,0},{6,2},{1,5},{3,7},{5,1},{7,3},{8,12},{10,14},{12... | collective-permute-start | bytes 393224 | tf_op jit(solution)/shard_map/ppermute | solution.py:23
  79.8 5.9 %collective-permute-start.21 = (bf16[64,1024]{1,0:T(8,128)(2,1)S(1)}, bf16[64,1024]{1,0:T(8,128)(2,1)S(1)}, u32[]{:S(2)}, u32[]{:S(2)}) collective-permute-start(bf16[64,1024]{1,0:T(8,128)(2,1)S(1)} %shard_map.170.refs_0_), channel_id=1, source_target_pairs={{0,6},{2,0},{4,2},{6,4},{1,7},{3,1},{5,3},{7,5},{8,14},{10,8},{12,... | collective-permute-start | bytes 393224 | tf_op jit(solution)/shard_map/ppermute | solution.py:23
  85.8 2.0 %collective-permute-start.22 = (bf16[4,64,1024]{2,1,0:T(8,128)(2,1)S(1)}, bf16[4,64,1024]{2,1,0:T(8,128)(2,1)S(1)}, u32[]{:S(2)}, u32[]{:S(2)}) collective-permute-start(bf16[4,64,1024]{2,1,0:T(8,128)(2,1)S(1)} %shard_map.171.refs_0_.refs_2_), channel_id=1, source_target_pairs={{0,1},{1,0},{2,3},{3,2},{4,5},{5,4},{6,7},{7,6},{8,9},{9,8},{10,11... | collective-permute-start | bytes 1572872 | tf_op jit(solution)/shard_map/ppermute | solution.py:23
  91.1 12.9 %collective-permute-start.27 = (bf16[128,1408]{1,0:T(8,128)(2,1)S(1)}, bf16[128,1408]{1,0:T(8,128)(2,1)S(1)}, u32[]{:S(2)}, u32[]{:S(2)}) collective-permute-start(bf16[128,1408]{1,0:T(8,128)(2,1)S(1)} %get-tuple-element.53), channel_id=1, source_target_pairs={{0,8},{8,16},{16,24},{24,0},{1,9},{9,17},{17,25},{25,1},{2,10},{10... | collective-permute-start | bytes 1081352 | tf_op jit(solution)/shard_map/ppermute | solution.py:23
  92.7 11.3 %collective-permute-start.28 = (bf16[128,1376]{1,0:T(8,128)(2,1)S(1)}, bf16[128,1376]{1,0:T(8,128)(2,1)S(1)}, u32[]{:S(2)}, u32[]{:S(2)}) collective-permute-start(bf16[128,1376]{1,0:T(8,128)(2,1)S(1)} %get-tuple-element.54), channel_id=1, source_target_pairs={{0,24},{8,0},{16,8},{24,16},{1,25},{9,1},{17,9},{25,17},{2,26},{10... | collective-permute-start | bytes 1056776 | tf_op jit(solution)/shard_map/ppermute | solution.py:23
  93.2 16.3 %collective-permute-start.35 = (bf16[1376,256]{1,0:T(8,128)(2,1)S(1)}, bf16[1376,256]{1,0:T(8,128)(2,1)S(1)}, u32[]{:S(2)}, u32[]{:S(2)}) collective-permute-start(bf16[1376,256]{1,0:T(8,128)(2,1)S(1)} %copy-done.3), channel_id=1, source_target_pairs={{0,32},{1,225},{32,64},{33,1},{64,96},{65,33},{96,128},{97,65},{12... | collective-permute-start | bytes 2113544 | tf_op jit(solution)/shard_map/ppermute | solution.py:40
  97.8 24.0 %copy-start.6 = (f32[3,1376]{1,0:T(4,128)S(1)}, f32[3,1376]{1,0:T(4,128)}, u32[]{:S(2)}) copy-start(f32[3,1376]{1,0:T(4,128)} %gate_kernel.1) | copy-start | bytes 49540
  97.8 24.0 %copy-start.7 = (f32[3,1376]{1,0:T(4,128)S(1)}, f32[3,1376]{1,0:T(4,128)}, u32[]{:S(2)}) copy-start(f32[3,1376]{1,0:T(4,128)} %value_kernel.1) | copy-start | bytes 49540
  97.8 23.9 %collective-permute-start.26 = (bf16[128,1408]{1,0:T(8,128)(2,1)S(1)}, bf16[128,1408]{1,0:T(8,128)(2,1)S(1)}, u32[]{:S(2)}, u32[]{:S(2)}) collective-permute-start(bf16[128,1408]{1,0:T(8,128)(2,1)S(1)} %get-tuple-element.52), channel_id=1, source_target_pairs={{0,24},{8,0},{16,8},{24,16},{1,25},{9,1},{17,9},{25,17},{2,26},{10... | collective-permute-start | bytes 1081352 | tf_op jit(solution)/shard_map/ppermute | solution.py:23
  104.3 17.4 %collective-permute-start.29 = (bf16[128,1408]{1,0:T(8,128)(2,1)S(1)}, bf16[128,1408]{1,0:T(8,128)(2,1)S(1)}, u32[]{:S(2)}, u32[]{:S(2)}) collective-permute-start(bf16[128,1408]{1,0:T(8,128)(2,1)S(1)} %get-tuple-element.57), channel_id=1, source_target_pairs={{0,8},{8,16},{16,24},{24,0},{1,9},{9,17},{17,25},{25,1},{2,10},{10... | collective-permute-start | bytes 1081352 | tf_op jit(solution)/shard_map/ppermute | solution.py:23
  107.5 13.5 %collective-permute-start.30 = (bf16[128,1376]{1,0:T(8,128)(2,1)S(1)}, bf16[128,1376]{1,0:T(8,128)(2,1)S(1)}, u32[]{:S(2)}, u32[]{:S(2)}) collective-permute-start(bf16[128,1376]{1,0:T(8,128)(2,1)S(1)} %get-tuple-element.59), channel_id=1, source_target_pairs={{0,8},{8,16},{16,24},{24,0},{1,9},{9,17},{17,25},{25,1},{2,10},{10... | collective-permute-start | bytes 1056776 | tf_op jit(solution)/shard_map/ppermute | solution.py:23
  107.6 14.1 %collective-permute-start.31 = (bf16[128,1376]{1,0:T(8,128)(2,1)S(1)}, bf16[128,1376]{1,0:T(8,128)(2,1)S(1)}, u32[]{:S(2)}, u32[]{:S(2)}) collective-permute-start(bf16[128,1376]{1,0:T(8,128)(2,1)S(1)} %get-tuple-element.60), channel_id=1, source_target_pairs={{0,24},{8,0},{16,8},{24,16},{1,25},{9,1},{17,9},{25,17},{2,26},{10... | collective-permute-start | bytes 1056776 | tf_op jit(solution)/shard_map/ppermute | solution.py:23
  109.6 25.4 %collective-permute-start.36 = (bf16[1376,256]{1,0:T(8,128)(2,1)S(1)}, bf16[1376,256]{1,0:T(8,128)(2,1)S(1)}, u32[]{:S(2)}, u32[]{:S(2)}) collective-permute-start(bf16[1376,256]{1,0:T(8,128)(2,1)S(1)} %copy-done.3), channel_id=1, source_target_pairs={{0,224},{1,33},{32,0},{33,65},{64,32},{65,97},{96,64},{97,129},{12... | collective-permute-start | bytes 2113544 | tf_op jit(solution)/shard_map/ppermute | solution.py:40
  121.0 14.0 %collective-permute-start.37 = (bf16[1376,256]{1,0:T(8,128)(2,1)S(1)}, bf16[1376,256]{1,0:T(8,128)(2,1)S(1)}, u32[]{:S(2)}, u32[]{:S(2)}) collective-permute-start(bf16[1376,256]{1,0:T(8,128)(2,1)S(1)} %collective-permute-done.35.refs_1_), channel_id=1, source_target_pairs={{0,32},{1,225},{32,64},{33,1},{64,96},{65,33},{96,128},{97,65},{12... | collective-permute-start | bytes 2113544 | tf_op jit(solution)/shard_map/ppermute | solution.py:40
  123.5 10.7 %collective-permute-start.32 = (bf16[128,1376]{1,0:T(8,128)(2,1)S(1)}, bf16[128,1376]{1,0:T(8,128)(2,1)S(1)}, u32[]{:S(2)}, u32[]{:S(2)}) collective-permute-start(bf16[128,1376]{1,0:T(8,128)(2,1)S(1)} %shard_map.177.refs_0_), channel_id=1, source_target_pairs={{0,8},{1,25},{8,16},{9,1},{16,24},{17,9},{24,0},{25,17},{2,10},{3,... | collective-permute-start | bytes 1056776 | tf_op jit(solution)/shard_map/ppermute | solution.py:40
  126.1 10.0 %collective-permute-start.33 = (bf16[128,1376]{1,0:T(8,128)(2,1)S(1)}, bf16[128,1376]{1,0:T(8,128)(2,1)S(1)}, u32[]{:S(2)}, u32[]{:S(2)}) collective-permute-start(bf16[128,1376]{1,0:T(8,128)(2,1)S(1)} %shard_map.177.refs_0_), channel_id=1, source_target_pairs={{0,24},{1,9},{8,0},{9,17},{16,8},{17,25},{24,16},{25,1},{2,26},{3,... | collective-permute-start | bytes 1056776 | tf_op jit(solution)/shard_map/ppermute | solution.py:40
  134.1 7.4 %collective-permute-start.34 = (bf16[128,1376]{1,0:T(8,128)(2,1)S(1)}, bf16[128,1376]{1,0:T(8,128)(2,1)S(1)}, u32[]{:S(2)}, u32[]{:S(2)}) collective-permute-start(bf16[128,1376]{1,0:T(8,128)(2,1)S(1)} %collective-permute-done.32.refs_1_), channel_id=1, source_target_pairs={{0,8},{1,25},{8,16},{9,1},{16,24},{17,9},{24,0},{25,17},{2,10},{3,... | collective-permute-start | bytes 1056776 | tf_op jit(solution)/shard_map/ppermute | solution.py:40
  142.9 2.0 %collective-permute-start.38 = (bf16[4,256,256]{2,1,0:T(8,128)(2,1)S(1)}, bf16[4,256,256]{2,1,0:T(8,128)(2,1)S(1)}, u32[]{:S(2)}, u32[]{:S(2)}) collective-permute-start(bf16[4,256,256]{2,1,0:T(8,128)(2,1)S(1)} %shard_map.180), channel_id=1, source_target_pairs={{0,1},{1,0},{2,3},{3,2},{4,5},{5,4},{6,7},{7,6},{8,9},{9,8},{10,11... | collective-permute-start | bytes 1572872 | tf_op jit(solution)/shard_map/ppermute | solution.py:23
  145.1 7.3 %collective-permute-start.39 = (bf16[256,256]{1,0:T(8,128)(2,1)S(1)}, bf16[256,256]{1,0:T(8,128)(2,1)S(1)}, u32[]{:S(2)}, u32[]{:S(2)}) collective-permute-start(bf16[256,256]{1,0:T(8,128)(2,1)S(1)} %get-tuple-element.62), channel_id=1, source_target_pairs={{0,2},{2,4},{4,6},{6,0},{1,3},{3,5},{5,7},{7,1},{8,10},{10,12},{12... | collective-permute-start | bytes 393224 | tf_op jit(solution)/shard_map/ppermute | solution.py:23
  145.9 9.2 %collective-permute-start.40 = (bf16[256,256]{1,0:T(8,128)(2,1)S(1)}, bf16[256,256]{1,0:T(8,128)(2,1)S(1)}, u32[]{:S(2)}, u32[]{:S(2)}) collective-permute-start(bf16[256,256]{1,0:T(8,128)(2,1)S(1)} %get-tuple-element.63), channel_id=1, source_target_pairs={{0,4},{2,6},{4,0},{6,2},{1,5},{3,7},{5,1},{7,3},{8,12},{10,14},{12... | collective-permute-start | bytes 393224 | tf_op jit(solution)/shard_map/ppermute | solution.py:23
  148.8 6.5 %collective-permute-start.41 = (bf16[256,256]{1,0:T(8,128)(2,1)S(1)}, bf16[256,256]{1,0:T(8,128)(2,1)S(1)}, u32[]{:S(2)}, u32[]{:S(2)}) collective-permute-start(bf16[256,256]{1,0:T(8,128)(2,1)S(1)} %get-tuple-element.64), channel_id=1, source_target_pairs={{0,6},{2,0},{4,2},{6,4},{1,7},{3,1},{5,3},{7,5},{8,14},{10,8},{12,... | collective-permute-start | bytes 393224 | tf_op jit(solution)/shard_map/ppermute | solution.py:23
  155.4 7.3 %collective-permute-start.42 = (bf16[128,256]{1,0:T(8,128)(2,1)S(1)}, bf16[128,256]{1,0:T(8,128)(2,1)S(1)}, u32[]{:S(2)}, u32[]{:S(2)}) collective-permute-start(bf16[128,256]{1,0:T(8,128)(2,1)S(1)} %get-tuple-element.65), channel_id=1, source_target_pairs={{0,0},{1,16},{8,8},{9,24},{16,1},{17,17},{24,9},{25,25},{2,2},{3,1... | collective-permute-start | bytes 196616 | tf_op jit(solution)/shard_map/ppermute | solution.py:67
  160.5 3.8 %collective-permute-start.43 = (bf16[128,256]{1,0:T(8,128)(2,1)S(1)}, bf16[128,256]{1,0:T(8,128)(2,1)S(1)}, u32[]{:S(2)}, u32[]{:S(2)}) collective-permute-start(bf16[128,256]{1,0:T(8,128)(2,1)S(1)} %get-tuple-element.66), channel_id=1, source_target_pairs={{0,8},{1,24},{8,0},{9,16},{16,9},{17,25},{24,1},{25,17},{2,10},{3,... | collective-permute-start | bytes 196616 | tf_op jit(solution)/shard_map/ppermute | solution.py:67
  (10 other events, 128.6 us)

commit v3 on v2

--- a/solution.py
+++ b/solution.py
@@ -350,13 +350,13 @@
 
     spare = padded - inner
 
-    def over_tiles(run):
+    def over_tiles(run, unroll=1):
         def step(n, carry):
             start = pl.multiple_of(n * part, part)
             run(pl.ds(start, part), pl.ds(pl.multiple_of(inner + start, 32), part))
             return carry
 
-        lax.fori_loop(0, inner // part, step, 0)
+        lax.fori_loop(0, inner // part, step, 0, unroll=unroll)
         rest = inner // part * part
         run(slice(rest, inner), slice(inner + rest, 2 * inner))
 
@@ -410,7 +410,7 @@
             gate_out[:, at] = up_dot(scaled[0], weights, last, at).astype(BF16)
             value_out[:, at] = up_dot(scaled[0], weights, last, value_at).astype(BF16)
 
-        over_tiles(run)
+        over_tiles(run, 2)
         gate_out[:, inner:] = parts[0, :, :spare].astype(BF16)
 
     up_flops = 2 * length * span * inner
@@ -509,7 +509,7 @@
             run(aligned(n * LANES, LANES), LANES)
             return carry
 
-        lax.fori_loop(0, inner // LANES, step, 0)
+        lax.fori_loop(0, inner // LANES, step, 0, unroll=2)
         rest = inner // LANES * LANES
         run(slice(rest, inner), inner - rest)
 
@@ -542,7 +542,7 @@
                 out[j] = dot(left[...], weights[j]).astype(out.dtype)
                 return carry
 
-            lax.fori_loop(0, RING, step, 0, unroll=2)
+            lax.fori_loop(0, RING, step, 0, unroll=True)
 
         return kernel_call(
             run,

time: 168 us -> 167 us (level)
  no operation moved by 1% of the time
where the time goes in v3:
time: 167 us; the launch traced here: 164 us
  waiting for transfers between devices  77.5 us (46%)
  starting transfers between devices  61.6 us (37%)
  Pallas kernels  20.6 us (12%)
  local copies, waits for them, and re-layouts  2.23 us (1%)
    ppermute x28, waiting for transfers between devices, shift(): lax.ppermute(value, axes, [(i, (i + by) % size) for i in range(size)])  47.5 us
    ppermute x28, starting transfers between devices, shift(): lax.ppermute(value, axes, [(i, (i + by) % size) for i in range(size)])  37.5 us
    ppermute x12, waiting for transfers between devices, shift_apart(): return lax.ppermute(value, (*axes, CORE), pairs)  22.5 us
    pallas_call x21, Pallas kernels, run(): pl.pallas_call(body, out_shape=[jax.ShapeDtypeStruct(*out) for out in out...  20.6 us
    ppermute x12, starting transfers between devices, shift_apart(): return lax.ppermute(value, (*axes, CORE), pairs)  14.5 us
    ppermute x4, starting transfers between devices, trade(): return lax.ppermute(value, (X, CORE), pairs)  9.64 us
    ppermute x4, waiting for transfers between devices, trade(): return lax.ppermute(value, (X, CORE), pairs)  7.54 us
  transfers between devices with their start and end apart: 44, of which 27 were waited for; matrix products, arithmetic and copies ran while one was open for 2% of the time, Pallas kernels for 8%

profile of v3, /device:TPU:4, one launch (start us, length us, event | category | flops | bytes accessed | tf_op | source)
XLA Modules:
  0.0 163.9 jit_solution(6039460348261124874)
XLA Ops:
  0.0 2.4 %shard_map.172 = bf16[2752,256]{1,0:T(8,128)(2,1)} custom-call(bf16[1376,256]{1,0:T(8,128)(2,1)} %bitcast.5, bf16[1376,256]{1,0:T(8,128)(2,1)} %bitcast.7), custom_call_target="tpu_custom_call" | custom-call | tf_op jit(solution)/shard_map/pallas_call | solution.py:75
  2.5 2.0 %collective-permute-start.23 = (bf16[2752,256]{1,0:T(8,128)(2,1)}, bf16[2752,256]{1,0:T(8,128)(2,1)S(1)}, u32[]{:S(2)}, u32[]{:S(2)}) collective-permute-start(bf16[2752,256]{1,0:T(8,128)(2,1)} %shard_map.172), channel_id=1, source_target_pairs={{0,32},{1,225},{32,64},{33,1},{64,96},{65,33},{96,128},{97,65},{12... | collective-permute-start | bytes 4227080 | tf_op jit(solution)/shard_map/ppermute | solution.py:40
  4.4 2.0 %shard_map.163 = (bf16[128,256]{1,0:T(8,128)(2,1)}, bf16[128,256]{1,0:T(8,128)(2,1)}, bf16[784,256]{1,0:T(8,128)(2,1)}) custom-call(bf16[128,512]{1,0:T(8,128)(2,1)} %tokens.1, bf16[256,256]{1,0:T(8,128)(2,1)} %gate.1, bf16[256,256]{1,0:T(8,128)(2,1)} %value.1, bf16[256,256]{1,0:T(8,128)(2,1)} %merge.1, bf16[16,128]{1,0:T(8,128)(2,1)} %bitcast.11), custom_call_target="tpu_custom_call" | custom-call | tf_op jit(solution)/shard_map/pallas_call | solution.py:75
  6.4 2.0 %collective-permute-start.6 = (bf16[784,256]{1,0:T(8,128)(2,1)}, bf16[784,256]{1,0:T(8,128)(2,1)S(1)}, u32[]{:S(2)}, u32[]{:S(2)}) collective-permute-start(bf16[784,256]{1,0:T(8,128)(2,1)} %get-tuple-element.38.refs_2_.refs_4_), channel_id=1, source_target_pairs={{0,32},{1,225},{32,64},{33,1},{64,96},{65,33},{96,128},{97,65},{12... | collective-permute-start | bytes 1204232 | tf_op jit(solution)/shard_map/ppermute | solution.py:40
  8.4 4.3 %collective-permute-start = (bf16[128,256]{1,0:T(8,128)(2,1)}, bf16[128,256]{1,0:T(8,128)(2,1)S(1)}, u32[]{:S(2)}, u32[]{:S(2)}) collective-permute-start(bf16[128,256]{1,0:T(8,128)(2,1)} %get-tuple-element.36), channel_id=1, source_target_pairs={{0,0},{1,16},{8,8},{9,24},{16,1},{17,17},{24,9},{25,25},{2,2},{3,1... | collective-permute-start | bytes 196616 | tf_op jit(solution)/shard_map/ppermute | solution.py:67
  12.9 2.8 %collective-permute-done.near = bf16[128,256]{1,0:T(8,128)(2,1)S(1)} collective-permute-done((bf16[128,256]{1,0:T(8,128)(2,1)}, bf16[128,256]{1,0:T(8,128)(2,1)S(1)}, u32[]{:S(2)}, u32[]{:S(2)}) %collective-permute-start) | collective-permute-done | bytes 65568 | tf_op jit(solution)/shard_map/ppermute | solution.py:67
  16.8 1.7 %collective-permute-start.2 = (bf16[256,256]{1,0:T(8,128)(2,1)S(1)}, bf16[256,256]{1,0:T(8,128)(2,1)S(1)}, u32[]{:S(2)}, u32[]{:S(2)}) collective-permute-start(bf16[256,256]{1,0:T(8,128)(2,1)S(1)} %shard_map.164.refs_0_), channel_id=1, source_target_pairs={{0,2},{2,4},{4,6},{6,0},{1,3},{3,5},{5,7},{7,1},{8,10},{10,12},{12... | collective-permute-start | bytes 393224 | tf_op jit(solution)/shard_map/ppermute | solution.py:23
  18.4 2.9 %collective-permute-start.3 = (bf16[256,256]{1,0:T(8,128)(2,1)S(1)}, bf16[256,256]{1,0:T(8,128)(2,1)S(1)}, u32[]{:S(2)}, u32[]{:S(2)}) collective-permute-start(bf16[256,256]{1,0:T(8,128)(2,1)S(1)} %shard_map.164.refs_0_), channel_id=1, source_target_pairs={{0,4},{2,6},{4,0},{6,2},{1,5},{3,7},{5,1},{7,3},{8,12},{10,14},{12... | collective-permute-start | bytes 393224 | tf_op jit(solution)/shard_map/ppermute | solution.py:23
  22.7 1.4 collective-permute-done.2.refs_1_
  24.1 2.5 %collective-permute-done.3.refs_2_ = bf16[256,256]{1,0:T(8,128)(2,1)S(1)} collective-permute-done((bf16[256,256]{1,0:T(8,128)(2,1)S(1)}, bf16[256,256]{1,0:T(8,128)(2,1)S(1)}, u32[]{:S(2)}, u32[]{:S(2)}) %collective-permute-start.3) | collective-permute-done | bytes 131104 | tf_op jit(solution)/shard_map/ppermute | solution.py:23
  29.6 1.4 pad_maximum_fusion
  32.4 6.0 %collective-permute-done.7.refs_4_.refs_6_ = bf16[784,256]{1,0:T(8,128)(2,1)S(1)} collective-permute-done((bf16[784,256]{1,0:T(8,128)(2,1)}, bf16[784,256]{1,0:T(8,128)(2,1)S(1)}, u32[]{:S(2)}, u32[]{:S(2)}) %collective-permute-start.7) | collective-permute-done | bytes 401440 | tf_op jit(solution)/shard_map/ppermute | solution.py:40
  38.4 1.5 collective-permute-done.8.refs_5_.refs_7_
  40.7 2.0 %shard_map.166 = (bf16[4,512,256]{2,1,0:T(8,128)(2,1)S(1)}, bf16[128,640]{1,0:T(8,128)(2,1)S(1)}, bf16[128,640]{1,0:T(8,128)(2,1)S(1)}, bf16[128,640]{1,0:T(8,128)(2,1)S(1)}, bf16[128,640]{1,0:T(8,128)(2,1)S(1)}) custom-call(bf16[4,256,256]{2,1,0:T(8,128)(2,1)S(1)} %shard_map.165.refs_0_, bf16[4,256,256]{2,1,0:T(8,128)(2,1)} %collective-permute-done.5.refs_1_, ...), custom_call_target="tpu_custom_call" | custom-call | flops 536870912 | tf_op jit(solution)/shard_map/pallas_call | solution.py:75
  43.7 2.1 %collective-permute-start.11 = (bf16[128,640]{1,0:T(8,128)(2,1)S(1)}, bf16[128,640]{1,0:T(8,128)(2,1)S(1)}, u32[]{:S(2)}, u32[]{:S(2)}) collective-permute-start(bf16[128,640]{1,0:T(8,128)(2,1)S(1)} %get-tuple-element.42), channel_id=1, source_target_pairs={{0,8},{8,16},{16,24},{24,0},{1,9},{9,17},{17,25},{25,1},{2,10},{10... | collective-permute-start | bytes 491528 | tf_op jit(solution)/shard_map/ppermute | solution.py:23
  47.5 1.7 %collective-permute-start.25 = (bf16[2752,256]{1,0:T(8,128)(2,1)S(1)}, bf16[2752,256]{1,0:T(8,128)(2,1)S(1)}, u32[]{:S(2)}, u32[]{:S(2)}) collective-permute-start(bf16[2752,256]{1,0:T(8,128)(2,1)S(1)} %collective-permute-done.23.first), channel_id=1, source_target_pairs={{0,32},{1,225},{32,64},{33,1},{64,96},{65,33},{96,128},{97,65},{12... | collective-permute-start | bytes 4227080 | tf_op jit(solution)/shard_map/ppermute | solution.py:40
  49.2 2.2 %collective-permute-done.10.refs_2_ = bf16[128,640]{1,0:T(8,128)(2,1)S(1)} collective-permute-done((bf16[128,640]{1,0:T(8,128)(2,1)S(1)}, bf16[128,640]{1,0:T(8,128)(2,1)S(1)}, u32[]{:S(2)}, u32[]{:S(2)}) %collective-permute-start.10) | collective-permute-done | bytes 163872 | tf_op jit(solution)/shard_map/ppermute | solution.py:23
  51.3 2.0 %collective-permute-done.11.refs_3_ = bf16[128,640]{1,0:T(8,128)(2,1)S(1)} collective-permute-done((bf16[128,640]{1,0:T(8,128)(2,1)S(1)}, bf16[128,640]{1,0:T(8,128)(2,1)S(1)}, u32[]{:S(2)}, u32[]{:S(2)}) %collective-permute-start.11) | collective-permute-done | bytes 163872 | tf_op jit(solution)/shard_map/ppermute | solution.py:23
  53.9 2.9 %collective-permute-start.12 = (bf16[128,256]{1,0:T(8,128)(2,1)S(1)}, bf16[128,256]{1,0:T(8,128)(2,1)S(1)}, u32[]{:S(2)}, u32[]{:S(2)}) collective-permute-start(bf16[128,256]{1,0:T(8,128)(2,1)S(1)} %shard_map.167.refs_0_), channel_id=1, source_target_pairs={{0,8},{8,16},{16,24},{24,0},{1,9},{9,17},{17,25},{25,1},{2,10},{10... | collective-permute-start | bytes 196616 | tf_op jit(solution)/shard_map/ppermute | solution.py:23
  56.8 2.0 %collective-permute-start.14 = (bf16[128,256]{1,0:T(8,128)(2,1)S(1)}, bf16[128,256]{1,0:T(8,128)(2,1)S(1)}, u32[]{:S(2)}, u32[]{:S(2)}) collective-permute-start(bf16[128,256]{1,0:T(8,128)(2,1)S(1)} %shard_map.167.refs_0_), channel_id=1, source_target_pairs={{0,24},{8,0},{16,8},{24,16},{1,25},{9,1},{17,9},{25,17},{2,26},{10... | collective-permute-start | bytes 196616 | tf_op jit(solution)/shard_map/ppermute | solution.py:23
  58.8 3.7 %collective-permute-done.13.refs_2_ = bf16[128,256]{1,0:T(8,128)(2,1)S(1)} collective-permute-done((bf16[128,256]{1,0:T(8,128)(2,1)S(1)}, bf16[128,256]{1,0:T(8,128)(2,1)S(1)}, u32[]{:S(2)}, u32[]{:S(2)}) %collective-permute-start.13) | collective-permute-done | bytes 65568 | tf_op jit(solution)/shard_map/ppermute | solution.py:23
  63.0 1.9 %collective-permute-done.15.refs_8_ = bf16[256,1024]{1,0:T(8,128)(2,1)S(1)} collective-permute-done((bf16[256,1024]{1,0:T(8,128)(2,1)S(1)}, bf16[256,1024]{1,0:T(8,128)(2,1)S(1)}, u32[]{:S(2)}, u32[]{:S(2)}) %collective-permute-start.15) | collective-permute-done | bytes 524320 | tf_op jit(solution)/shard_map/ppermute | solution.py:23
  66.4 3.0 %collective-permute-start.17 = (bf16[64,1024]{1,0:T(8,128)(2,1)S(1)}, bf16[64,1024]{1,0:T(8,128)(2,1)S(1)}, u32[]{:S(2)}, u32[]{:S(2)}) collective-permute-start(bf16[64,1024]{1,0:T(8,128)(2,1)S(1)} %get-tuple-element.46), channel_id=1, source_target_pairs={{0,4},{2,6},{4,0},{6,2},{1,5},{3,7},{5,1},{7,3},{8,12},{10,14},{12... | collective-permute-start | bytes 393224 | tf_op jit(solution)/shard_map/ppermute | solution.py:23
  70.3 1.9 %collective-permute-done.16.first = bf16[64,1024]{1,0:T(8,128)(2,1)S(1)} collective-permute-done((bf16[64,1024]{1,0:T(8,128)(2,1)S(1)}, bf16[64,1024]{1,0:T(8,128)(2,1)S(1)}, u32[]{:S(2)}, u32[]{:S(2)}) %collective-permute-start.16) | collective-permute-done | bytes 131104 | tf_op jit(solution)/shard_map/ppermute | solution.py:23
  72.2 3.5 %collective-permute-done.17.second = bf16[64,1024]{1,0:T(8,128)(2,1)S(1)} collective-permute-done((bf16[64,1024]{1,0:T(8,128)(2,1)S(1)}, bf16[64,1024]{1,0:T(8,128)(2,1)S(1)}, u32[]{:S(2)}, u32[]{:S(2)}) %collective-permute-start.17) | collective-permute-done | bytes 131104 | tf_op jit(solution)/shard_map/ppermute | solution.py:23
  75.8 1.5 collective-permute-start.19
  77.3 2.5 %collective-permute-start.20 = (bf16[64,1024]{1,0:T(8,128)(2,1)S(1)}, bf16[64,1024]{1,0:T(8,128)(2,1)S(1)}, u32[]{:S(2)}, u32[]{:S(2)}) collective-permute-start(bf16[64,1024]{1,0:T(8,128)(2,1)S(1)} %shard_map.170.refs_0_), channel_id=1, source_target_pairs={{0,4},{2,6},{4,0},{6,2},{1,5},{3,7},{5,1},{7,3},{8,12},{10,14},{12... | collective-permute-start | bytes 393224 | tf_op jit(solution)/shard_map/ppermute | solution.py:23
  80.6 1.9 %collective-permute-done.19.refs_1_ = bf16[64,1024]{1,0:T(8,128)(2,1)S(1)} collective-permute-done((bf16[64,1024]{1,0:T(8,128)(2,1)S(1)}, bf16[64,1024]{1,0:T(8,128)(2,1)S(1)}, u32[]{:S(2)}, u32[]{:S(2)}) %collective-permute-start.19) | collective-permute-done | bytes 131104 | tf_op jit(solution)/shard_map/ppermute | solution.py:23
  82.4 3.3 %collective-permute-done.20.refs_2_ = bf16[64,1024]{1,0:T(8,128)(2,1)S(1)} collective-permute-done((bf16[64,1024]{1,0:T(8,128)(2,1)S(1)}, bf16[64,1024]{1,0:T(8,128)(2,1)S(1)}, u32[]{:S(2)}, u32[]{:S(2)}) %collective-permute-start.20) | collective-permute-done | bytes 131104 | tf_op jit(solution)/shard_map/ppermute | solution.py:23
  86.3 1.5 collective-permute-done.22.refs_1_
  87.8 2.9 %shard_map.174 = (bf16[128,1408]{1,0:T(8,128)(2,1)S(1)}, bf16[128,1376]{1,0:T(8,128)(2,1)S(1)}, bf16[4,128,1024]{2,1,0:T(8,128)(2,1)S(1)}, f32[4,128,128]{2,1,0:T(8,128)S(1)}, bf16[2752,256]{1,0:T(8,128)(2,1)S(1)}) custom-call(bf16[4,64,1024]{2,1,0:T(8,128)(2,1)S(1)} %shard_map.171.refs_0_.refs_2_, bf16[4,64,1024]{2,1,0:T(8,128)(2,1)S(1)} %collective-permute-done.22.refs_1_, ...), custom_call_target="tpu_custom_call" | custom-call | flops 721420288 | tf_op jit(solution)/shard_map/pallas_call | solution.py:75
  90.7 1.6 collective-permute-start.27
  93.6 3.7 %shard_map.175 = (bf16[128,1408]{1,0:T(8,128)(2,1)S(1)}, bf16[128,1376]{1,0:T(8,128)(2,1)S(1)}, f32[128,1408]{1,0:T(8,128)S(1)}, f32[128,1376]{1,0:T(8,128)S(1)}...) custom-call(bf16[4,128,1024]{2,1,0:T(8,128)(2,1)S(1)} %get-tuple-element.48.scaled, ...), custom_call_target="tpu_custom_call" | custom-call | flops 2164260864 | tf_op jit(solution)/shard_map/pallas_call | solution.py:75
  98.3 5.3 %collective-permute-done.28.value_two = bf16[128,1376]{1,0:T(8,128)(2,1)S(1)} collective-permute-done((bf16[128,1376]{1,0:T(8,128)(2,1)S(1)}, bf16[128,1376]{1,0:T(8,128)(2,1)S(1)}, u32[]{:S(2)}, u32[]{:S(2)}) %collective-permute-start.28) | collective-permute-done | bytes 352288 | tf_op jit(solution)/shard_map/ppermute | solution.py:23
  103.9 3.0 %collective-permute-start.29 = (bf16[128,1408]{1,0:T(8,128)(2,1)S(1)}, bf16[128,1408]{1,0:T(8,128)(2,1)S(1)}, u32[]{:S(2)}, u32[]{:S(2)}) collective-permute-start(bf16[128,1408]{1,0:T(8,128)(2,1)S(1)} %get-tuple-element.57), channel_id=1, source_target_pairs={{0,8},{8,16},{16,24},{24,0},{1,9},{9,17},{17,25},{25,1},{2,10},{10... | collective-permute-start | bytes 1081352 | tf_op jit(solution)/shard_map/ppermute | solution.py:23
  106.9 1.9 %collective-permute-start.31 = (bf16[128,1376]{1,0:T(8,128)(2,1)S(1)}, bf16[128,1376]{1,0:T(8,128)(2,1)S(1)}, u32[]{:S(2)}, u32[]{:S(2)}) collective-permute-start(bf16[128,1376]{1,0:T(8,128)(2,1)S(1)} %get-tuple-element.60), channel_id=1, source_target_pairs={{0,24},{8,0},{16,8},{24,16},{1,25},{9,1},{17,9},{25,17},{2,26},{10... | collective-permute-start | bytes 1056776 | tf_op jit(solution)/shard_map/ppermute | solution.py:23
  108.9 2.2 %collective-permute-start.36 = (bf16[1376,256]{1,0:T(8,128)(2,1)S(1)}, bf16[1376,256]{1,0:T(8,128)(2,1)S(1)}, u32[]{:S(2)}, u32[]{:S(2)}) collective-permute-start(bf16[1376,256]{1,0:T(8,128)(2,1)S(1)} %copy-done.3), channel_id=1, source_target_pairs={{0,224},{1,33},{32,0},{33,65},{64,32},{65,97},{96,64},{97,129},{12... | collective-permute-start | bytes 2113544 | tf_op jit(solution)/shard_map/ppermute | solution.py:40
  111.1 9.2 %collective-permute-done.30.value_near = bf16[128,1376]{1,0:T(8,128)(2,1)S(1)} collective-permute-done((bf16[128,1376]{1,0:T(8,128)(2,1)S(1)}, bf16[128,1376]{1,0:T(8,128)(2,1)S(1)}, u32[]{:S(2)}, u32[]{:S(2)}) %collective-permute-start.30) | collective-permute-done | bytes 352288 | tf_op jit(solution)/shard_map/ppermute | solution.py:23
  121.1 1.4 shard_map.177.refs_0_
  122.5 2.6 %collective-permute-start.32 = (bf16[128,1376]{1,0:T(8,128)(2,1)S(1)}, bf16[128,1376]{1,0:T(8,128)(2,1)S(1)}, u32[]{:S(2)}, u32[]{:S(2)}) collective-permute-start(bf16[128,1376]{1,0:T(8,128)(2,1)S(1)} %shard_map.177.refs_0_), channel_id=1, source_target_pairs={{0,8},{1,25},{8,16},{9,1},{16,24},{17,9},{24,0},{25,17},{2,10},{3,... | collective-permute-start | bytes 1056776 | tf_op jit(solution)/shard_map/ppermute | solution.py:40
  125.1 8.1 %collective-permute-done.32.refs_1_ = bf16[128,1376]{1,0:T(8,128)(2,1)S(1)} collective-permute-done((bf16[128,1376]{1,0:T(8,128)(2,1)S(1)}, bf16[128,1376]{1,0:T(8,128)(2,1)S(1)}, u32[]{:S(2)}, u32[]{:S(2)}) %collective-permute-start.32) | collective-permute-done | bytes 352288 | tf_op jit(solution)/shard_map/ppermute | solution.py:40
  135.1 5.5 %collective-permute-done.34.refs_3_ = bf16[128,1376]{1,0:T(8,128)(2,1)S(1)} collective-permute-done((bf16[128,1376]{1,0:T(8,128)(2,1)S(1)}, bf16[128,1376]{1,0:T(8,128)(2,1)S(1)}, u32[]{:S(2)}, u32[]{:S(2)}) %collective-permute-start.34) | collective-permute-done | bytes 352288 | tf_op jit(solution)/shard_map/ppermute | solution.py:40
  144.6 2.9 %collective-permute-start.40 = (bf16[256,256]{1,0:T(8,128)(2,1)S(1)}, bf16[256,256]{1,0:T(8,128)(2,1)S(1)}, u32[]{:S(2)}, u32[]{:S(2)}) collective-permute-start(bf16[256,256]{1,0:T(8,128)(2,1)S(1)} %get-tuple-element.63), channel_id=1, source_target_pairs={{0,4},{2,6},{4,0},{6,2},{1,5},{3,7},{5,1},{7,3},{8,12},{10,14},{12... | collective-permute-start | bytes 393224 | tf_op jit(solution)/shard_map/ppermute | solution.py:23
  147.9 3.2 %collective-permute-done.39.first = bf16[256,256]{1,0:T(8,128)(2,1)S(1)} collective-permute-done((bf16[256,256]{1,0:T(8,128)(2,1)S(1)}, bf16[256,256]{1,0:T(8,128)(2,1)S(1)}, u32[]{:S(2)}, u32[]{:S(2)}) %collective-permute-start.39) | collective-permute-done | bytes 131104 | tf_op jit(solution)/shard_map/ppermute | solution.py:23
  151.1 2.7 %collective-permute-done.40.second = bf16[256,256]{1,0:T(8,128)(2,1)S(1)} collective-permute-done((bf16[256,256]{1,0:T(8,128)(2,1)S(1)}, bf16[256,256]{1,0:T(8,128)(2,1)S(1)}, u32[]{:S(2)}, u32[]{:S(2)}) %collective-permute-start.40) | collective-permute-done | bytes 131104 | tf_op jit(solution)/shard_map/ppermute | solution.py:23
  154.1 5.1 %collective-permute-start.42 = (bf16[128,256]{1,0:T(8,128)(2,1)S(1)}, bf16[128,256]{1,0:T(8,128)(2,1)S(1)}, u32[]{:S(2)}, u32[]{:S(2)}) collective-permute-start(bf16[128,256]{1,0:T(8,128)(2,1)S(1)} %get-tuple-element.65), channel_id=1, source_target_pairs={{0,0},{1,16},{8,8},{9,24},{16,1},{17,17},{24,9},{25,25},{2,2},{3,1... | collective-permute-start | bytes 196616 | tf_op jit(solution)/shard_map/ppermute | solution.py:67
  159.3 2.1 %collective-permute-done.42.near = bf16[128,256]{1,0:T(8,128)(2,1)S(1)} collective-permute-done((bf16[128,256]{1,0:T(8,128)(2,1)S(1)}, bf16[128,256]{1,0:T(8,128)(2,1)S(1)}, u32[]{:S(2)}, u32[]{:S(2)}) %collective-permute-start.42) | collective-permute-done | bytes 65568 | tf_op jit(solution)/shard_map/ppermute | solution.py:67
  161.5 1.5 collective-permute-done.43.far
  (93 shorter events, 25.7 us)
Async XLA Ops:
  2.5 45.0 %collective-permute-start.23 = (bf16[2752,256]{1,0:T(8,128)(2,1)}, bf16[2752,256]{1,0:T(8,128)(2,1)S(1)}, u32[]{:S(2)}, u32[]{:S(2)}) collective-permute-start(bf16[2752,256]{1,0:T(8,128)(2,1)} %shard_map.172), channel_id=1, source_target_pairs={{0,32},{1,225},{32,64},{33,1},{64,96},{65,33},{96,128},{97,65},{12... | collective-permute-start | bytes 4227080 | tf_op jit(solution)/shard_map/ppermute | solution.py:40
  6.4 33.5 %copy-start = (bf16[784,256]{1,0:T(8,128)(2,1)S(1)}, bf16[784,256]{1,0:T(8,128)(2,1)}, u32[]{:S(2)}) copy-start(bf16[784,256]{1,0:T(8,128)(2,1)} %get-tuple-element.38.refs_2_.refs_4_) | copy-start | bytes 1204228
  6.4 23.1 %collective-permute-start.6 = (bf16[784,256]{1,0:T(8,128)(2,1)}, bf16[784,256]{1,0:T(8,128)(2,1)S(1)}, u32[]{:S(2)}, u32[]{:S(2)}) collective-permute-start(bf16[784,256]{1,0:T(8,128)(2,1)} %get-tuple-element.38.refs_2_.refs_4_), channel_id=1, source_target_pairs={{0,32},{1,225},{32,64},{33,1},{64,96},{65,33},{96,128},{97,65},{12... | collective-permute-start | bytes 1204232 | tf_op jit(solution)/shard_map/ppermute | solution.py:40
  8.4 7.3 %collective-permute-start = (bf16[128,256]{1,0:T(8,128)(2,1)}, bf16[128,256]{1,0:T(8,128)(2,1)S(1)}, u32[]{:S(2)}, u32[]{:S(2)}) collective-permute-start(bf16[128,256]{1,0:T(8,128)(2,1)} %get-tuple-element.36), channel_id=1, source_target_pairs={{0,0},{1,16},{8,8},{9,24},{16,1},{17,17},{24,9},{25,25},{2,2},{3,1... | collective-permute-start | bytes 196616 | tf_op jit(solution)/shard_map/ppermute | solution.py:67
  12.8 4.0 %collective-permute-start.1 = (bf16[128,256]{1,0:T(8,128)(2,1)}, bf16[128,256]{1,0:T(8,128)(2,1)S(1)}, u32[]{:S(2)}, u32[]{:S(2)}) collective-permute-start(bf16[128,256]{1,0:T(8,128)(2,1)} %get-tuple-element.37), channel_id=1, source_target_pairs={{0,8},{1,24},{8,0},{9,16},{16,9},{17,25},{24,1},{25,17},{2,10},{3,... | collective-permute-start | bytes 196616 | tf_op jit(solution)/shard_map/ppermute | solution.py:67
  16.8 7.3 %collective-permute-start.2 = (bf16[256,256]{1,0:T(8,128)(2,1)S(1)}, bf16[256,256]{1,0:T(8,128)(2,1)S(1)}, u32[]{:S(2)}, u32[]{:S(2)}) collective-permute-start(bf16[256,256]{1,0:T(8,128)(2,1)S(1)} %shard_map.164.refs_0_), channel_id=1, source_target_pairs={{0,2},{2,4},{4,6},{6,0},{1,3},{3,5},{5,7},{7,1},{8,10},{10,12},{12... | collective-permute-start | bytes 393224 | tf_op jit(solution)/shard_map/ppermute | solution.py:23
  18.4 8.2 %collective-permute-start.3 = (bf16[256,256]{1,0:T(8,128)(2,1)S(1)}, bf16[256,256]{1,0:T(8,128)(2,1)S(1)}, u32[]{:S(2)}, u32[]{:S(2)}) collective-permute-start(bf16[256,256]{1,0:T(8,128)(2,1)S(1)} %shard_map.164.refs_0_), channel_id=1, source_target_pairs={{0,4},{2,6},{4,0},{6,2},{1,5},{3,7},{5,1},{7,3},{8,12},{10,14},{12... | collective-permute-start | bytes 393224 | tf_op jit(solution)/shard_map/ppermute | solution.py:23
  21.3 5.4 %collective-permute-start.4 = (bf16[256,256]{1,0:T(8,128)(2,1)S(1)}, bf16[256,256]{1,0:T(8,128)(2,1)S(1)}, u32[]{:S(2)}, u32[]{:S(2)}) collective-permute-start(bf16[256,256]{1,0:T(8,128)(2,1)S(1)} %shard_map.164.refs_0_), channel_id=1, source_target_pairs={{0,6},{2,0},{4,2},{6,4},{1,7},{3,1},{5,3},{7,5},{8,14},{10,8},{12,... | collective-permute-start | bytes 393224 | tf_op jit(solution)/shard_map/ppermute | solution.py:23
  26.7 11.7 %collective-permute-start.5 = (bf16[4,256,256]{2,1,0:T(8,128)(2,1)S(1)}, bf16[4,256,256]{2,1,0:T(8,128)(2,1)}, u32[]{:S(2)}, u32[]{:S(2)}) collective-permute-start(bf16[4,256,256]{2,1,0:T(8,128)(2,1)S(1)} %shard_map.165.refs_0_), channel_id=1, source_target_pairs={{0,1},{1,0},{2,3},{3,2},{4,5},{5,4},{6,7},{7,6},{8,9},{9,8},{10,11... | collective-permute-start | bytes 1572872 | tf_op jit(solution)/shard_map/ppermute | solution.py:23
  26.8 11.6 %collective-permute-start.7 = (bf16[784,256]{1,0:T(8,128)(2,1)}, bf16[784,256]{1,0:T(8,128)(2,1)S(1)}, u32[]{:S(2)}, u32[]{:S(2)}) collective-permute-start(bf16[784,256]{1,0:T(8,128)(2,1)} %get-tuple-element.38.refs_2_.refs_4_), channel_id=1, source_target_pairs={{0,224},{1,33},{32,0},{33,65},{64,32},{65,97},{96,64},{97,129},{12... | collective-permute-start | bytes 1204232 | tf_op jit(solution)/shard_map/ppermute | solution.py:40
  29.5 10.4 %collective-permute-start.8 = (bf16[784,256]{1,0:T(8,128)(2,1)S(1)}, bf16[784,256]{1,0:T(8,128)(2,1)S(1)}, u32[]{:S(2)}, u32[]{:S(2)}) collective-permute-start(bf16[784,256]{1,0:T(8,128)(2,1)S(1)} %collective-permute-done.6.refs_3_.refs_5_), channel_id=1, source_target_pairs={{0,32},{1,225},{32,64},{33,1},{64,96},{65,33},{96,128},{97,65},{12... | collective-permute-start | bytes 1204232 | tf_op jit(solution)/shard_map/ppermute | solution.py:40
  29.5 23.8 %copy-start.8 = (f32[2,128]{1,0:T(2,128)S(1)}, f32[2,128]{1,0:T(2,128)}, u32[]{:S(2)}) copy-start(f32[2,128]{1,0:T(2,128)} %refs_4_.1) | copy-start | bytes 3076
  29.5 23.8 %copy-start.9 = (f32[2,128]{1,0:T(2,128)S(1)}, f32[2,128]{1,0:T(2,128)}, u32[]{:S(2)}) copy-start(f32[2,128]{1,0:T(2,128)} %refs_5_.1) | copy-start | bytes 3076
  29.5 23.8 %copy-start.10 = (f32[2,128]{1,0:T(2,128)S(1)}, f32[2,128]{1,0:T(2,128)}, u32[]{:S(2)}) copy-start(f32[2,128]{1,0:T(2,128)} %refs_6_.1) | copy-start | bytes 3076
  42.7 8.7 %collective-permute-start.10 = (bf16[128,640]{1,0:T(8,128)(2,1)S(1)}, bf16[128,640]{1,0:T(8,128)(2,1)S(1)}, u32[]{:S(2)}, u32[]{:S(2)}) collective-permute-start(bf16[128,640]{1,0:T(8,128)(2,1)S(1)} %get-tuple-element.41), channel_id=1, source_target_pairs={{0,16},{8,24},{16,0},{24,8},{1,17},{9,25},{17,1},{25,9},{2,18},{10... | collective-permute-start | bytes 491528 | tf_op jit(solution)/shard_map/ppermute | solution.py:23
  43.7 9.6 %collective-permute-start.11 = (bf16[128,640]{1,0:T(8,128)(2,1)S(1)}, bf16[128,640]{1,0:T(8,128)(2,1)S(1)}, u32[]{:S(2)}, u32[]{:S(2)}) collective-permute-start(bf16[128,640]{1,0:T(8,128)(2,1)S(1)} %get-tuple-element.42), channel_id=1, source_target_pairs={{0,8},{8,16},{16,24},{24,0},{1,9},{9,17},{17,25},{25,1},{2,10},{10... | collective-permute-start | bytes 491528 | tf_op jit(solution)/shard_map/ppermute | solution.py:23
  45.8 7.6 %collective-permute-start.9 = (bf16[128,640]{1,0:T(8,128)(2,1)S(1)}, bf16[128,640]{1,0:T(8,128)(2,1)S(1)}, u32[]{:S(2)}, u32[]{:S(2)}) collective-permute-start(bf16[128,640]{1,0:T(8,128)(2,1)S(1)} %get-tuple-element.40), channel_id=1, source_target_pairs={{0,24},{8,0},{16,8},{24,16},{1,25},{9,1},{17,9},{25,17},{2,26},{10... | collective-permute-start | bytes 491528 | tf_op jit(solution)/shard_map/ppermute | solution.py:23
  47.1 38.7 %collective-permute-start.24 = (bf16[2752,256]{1,0:T(8,128)(2,1)S(1)}, bf16[2752,256]{1,0:T(8,128)(2,1)S(1)}, u32[]{:S(2)}, u32[]{:S(2)}) collective-permute-start(bf16[2752,256]{1,0:T(8,128)(2,1)S(1)} %copy-done.11), channel_id=1, source_target_pairs={{0,224},{1,33},{32,0},{33,65},{64,32},{65,97},{96,64},{97,129},{12... | collective-permute-start | bytes 4227080 | tf_op jit(solution)/shard_map/ppermute | solution.py:40
  47.5 40.3 %collective-permute-start.25 = (bf16[2752,256]{1,0:T(8,128)(2,1)S(1)}, bf16[2752,256]{1,0:T(8,128)(2,1)S(1)}, u32[]{:S(2)}, u32[]{:S(2)}) collective-permute-start(bf16[2752,256]{1,0:T(8,128)(2,1)S(1)} %collective-permute-done.23.first), channel_id=1, source_target_pairs={{0,32},{1,225},{32,64},{33,1},{64,96},{65,33},{96,128},{97,65},{12... | collective-permute-start | bytes 4227080 | tf_op jit(solution)/shard_map/ppermute | solution.py:40
  53.9 5.0 %collective-permute-start.12 = (bf16[128,256]{1,0:T(8,128)(2,1)S(1)}, bf16[128,256]{1,0:T(8,128)(2,1)S(1)}, u32[]{:S(2)}, u32[]{:S(2)}) collective-permute-start(bf16[128,256]{1,0:T(8,128)(2,1)S(1)} %shard_map.167.refs_0_), channel_id=1, source_target_pairs={{0,8},{8,16},{16,24},{24,0},{1,9},{9,17},{17,25},{25,1},{2,10},{10... | collective-permute-start | bytes 196616 | tf_op jit(solution)/shard_map/ppermute | solution.py:23
  56.8 5.8 %collective-permute-start.13 = (bf16[128,256]{1,0:T(8,128)(2,1)S(1)}, bf16[128,256]{1,0:T(8,128)(2,1)S(1)}, u32[]{:S(2)}, u32[]{:S(2)}) collective-permute-start(bf16[128,256]{1,0:T(8,128)(2,1)S(1)} %shard_map.167.refs_0_), channel_id=1, source_target_pairs={{0,16},{8,24},{16,0},{24,8},{1,17},{9,25},{17,1},{25,9},{2,18},{10... | collective-permute-start | bytes 196616 | tf_op jit(solution)/shard_map/ppermute | solution.py:23
  56.8 5.8 %collective-permute-start.14 = (bf16[128,256]{1,0:T(8,128)(2,1)S(1)}, bf16[128,256]{1,0:T(8,128)(2,1)S(1)}, u32[]{:S(2)}, u32[]{:S(2)}) collective-permute-start(bf16[128,256]{1,0:T(8,128)(2,1)S(1)} %shard_map.167.refs_0_), channel_id=1, source_target_pairs={{0,24},{8,0},{16,8},{24,16},{1,25},{9,1},{17,9},{25,17},{2,26},{10... | collective-permute-start | bytes 196616 | tf_op jit(solution)/shard_map/ppermute | solution.py:23
  62.9 2.0 %collective-permute-start.15 = (bf16[256,1024]{1,0:T(8,128)(2,1)S(1)}, bf16[256,1024]{1,0:T(8,128)(2,1)S(1)}, u32[]{:S(2)}, u32[]{:S(2)}) collective-permute-start(bf16[256,1024]{1,0:T(8,128)(2,1)S(1)} %shard_map.168), channel_id=1, source_target_pairs={{0,1},{1,0},{2,3},{3,2},{4,5},{5,4},{6,7},{7,6},{8,9},{9,8},{10,11... | collective-permute-start | bytes 1572872 | tf_op jit(solution)/shard_map/ppermute | solution.py:23
  65.3 6.9 %collective-permute-start.16 = (bf16[64,1024]{1,0:T(8,128)(2,1)S(1)}, bf16[64,1024]{1,0:T(8,128)(2,1)S(1)}, u32[]{:S(2)}, u32[]{:S(2)}) collective-permute-start(bf16[64,1024]{1,0:T(8,128)(2,1)S(1)} %get-tuple-element.45), channel_id=1, source_target_pairs={{0,2},{2,4},{4,6},{6,0},{1,3},{3,5},{5,7},{7,1},{8,10},{10,12},{12... | collective-permute-start | bytes 393224 | tf_op jit(solution)/shard_map/ppermute | solution.py:23
  66.4 9.3 %collective-permute-start.17 = (bf16[64,1024]{1,0:T(8,128)(2,1)S(1)}, bf16[64,1024]{1,0:T(8,128)(2,1)S(1)}, u32[]{:S(2)}, u32[]{:S(2)}) collective-permute-start(bf16[64,1024]{1,0:T(8,128)(2,1)S(1)} %get-tuple-element.46), channel_id=1, source_target_pairs={{0,4},{2,6},{4,0},{6,2},{1,5},{3,7},{5,1},{7,3},{8,12},{10,14},{12... | collective-permute-start | bytes 393224 | tf_op jit(solution)/shard_map/ppermute | solution.py:23
  69.4 6.3 %collective-permute-start.18 = (bf16[64,1024]{1,0:T(8,128)(2,1)S(1)}, bf16[64,1024]{1,0:T(8,128)(2,1)S(1)}, u32[]{:S(2)}, u32[]{:S(2)}) collective-permute-start(bf16[64,1024]{1,0:T(8,128)(2,1)S(1)} %get-tuple-element.47), channel_id=1, source_target_pairs={{0,6},{2,0},{4,2},{6,4},{1,7},{3,1},{5,3},{7,5},{8,14},{10,8},{12,... | collective-permute-start | bytes 393224 | tf_op jit(solution)/shard_map/ppermute | solution.py:23
  75.8 6.6 %collective-permute-start.19 = (bf16[64,1024]{1,0:T(8,128)(2,1)S(1)}, bf16[64,1024]{1,0:T(8,128)(2,1)S(1)}, u32[]{:S(2)}, u32[]{:S(2)}) collective-permute-start(bf16[64,1024]{1,0:T(8,128)(2,1)S(1)} %shard_map.170.refs_0_), channel_id=1, source_target_pairs={{0,2},{2,4},{4,6},{6,0},{1,3},{3,5},{5,7},{7,1},{8,10},{10,12},{12... | collective-permute-start | bytes 393224 | tf_op jit(solution)/shard_map/ppermute | solution.py:23
  77.3 8.4 %collective-permute-start.20 = (bf16[64,1024]{1,0:T(8,128)(2,1)S(1)}, bf16[64,1024]{1,0:T(8,128)(2,1)S(1)}, u32[]{:S(2)}, u32[]{:S(2)}) collective-permute-start(bf16[64,1024]{1,0:T(8,128)(2,1)S(1)} %shard_map.170.refs_0_), channel_id=1, source_target_pairs={{0,4},{2,6},{4,0},{6,2},{1,5},{3,7},{5,1},{7,3},{8,12},{10,14},{12... | collective-permute-start | bytes 393224 | tf_op jit(solution)/shard_map/ppermute | solution.py:23
  79.8 5.9 %collective-permute-start.21 = (bf16[64,1024]{1,0:T(8,128)(2,1)S(1)}, bf16[64,1024]{1,0:T(8,128)(2,1)S(1)}, u32[]{:S(2)}, u32[]{:S(2)}) collective-permute-start(bf16[64,1024]{1,0:T(8,128)(2,1)S(1)} %shard_map.170.refs_0_), channel_id=1, source_target_pairs={{0,6},{2,0},{4,2},{6,4},{1,7},{3,1},{5,3},{7,5},{8,14},{10,8},{12,... | collective-permute-start | bytes 393224 | tf_op jit(solution)/shard_map/ppermute | solution.py:23
  85.8 2.0 %collective-permute-start.22 = (bf16[4,64,1024]{2,1,0:T(8,128)(2,1)S(1)}, bf16[4,64,1024]{2,1,0:T(8,128)(2,1)S(1)}, u32[]{:S(2)}, u32[]{:S(2)}) collective-permute-start(bf16[4,64,1024]{2,1,0:T(8,128)(2,1)S(1)} %shard_map.171.refs_0_.refs_2_), channel_id=1, source_target_pairs={{0,1},{1,0},{2,3},{3,2},{4,5},{5,4},{6,7},{7,6},{8,9},{9,8},{10,11... | collective-permute-start | bytes 1572872 | tf_op jit(solution)/shard_map/ppermute | solution.py:23
  90.7 12.9 %collective-permute-start.27 = (bf16[128,1408]{1,0:T(8,128)(2,1)S(1)}, bf16[128,1408]{1,0:T(8,128)(2,1)S(1)}, u32[]{:S(2)}, u32[]{:S(2)}) collective-permute-start(bf16[128,1408]{1,0:T(8,128)(2,1)S(1)} %get-tuple-element.53), channel_id=1, source_target_pairs={{0,8},{8,16},{16,24},{24,0},{1,9},{9,17},{17,25},{25,1},{2,10},{10... | collective-permute-start | bytes 1081352 | tf_op jit(solution)/shard_map/ppermute | solution.py:23
  92.3 11.3 %collective-permute-start.28 = (bf16[128,1376]{1,0:T(8,128)(2,1)S(1)}, bf16[128,1376]{1,0:T(8,128)(2,1)S(1)}, u32[]{:S(2)}, u32[]{:S(2)}) collective-permute-start(bf16[128,1376]{1,0:T(8,128)(2,1)S(1)} %get-tuple-element.54), channel_id=1, source_target_pairs={{0,24},{8,0},{16,8},{24,16},{1,25},{9,1},{17,9},{25,17},{2,26},{10... | collective-permute-start | bytes 1056776 | tf_op jit(solution)/shard_map/ppermute | solution.py:23
  92.8 16.1 %collective-permute-start.35 = (bf16[1376,256]{1,0:T(8,128)(2,1)S(1)}, bf16[1376,256]{1,0:T(8,128)(2,1)S(1)}, u32[]{:S(2)}, u32[]{:S(2)}) collective-permute-start(bf16[1376,256]{1,0:T(8,128)(2,1)S(1)} %copy-done.3), channel_id=1, source_target_pairs={{0,32},{1,225},{32,64},{33,1},{64,96},{65,33},{96,128},{97,65},{12... | collective-permute-start | bytes 2113544 | tf_op jit(solution)/shard_map/ppermute | solution.py:40
  97.3 23.7 %collective-permute-start.26 = (bf16[128,1408]{1,0:T(8,128)(2,1)S(1)}, bf16[128,1408]{1,0:T(8,128)(2,1)S(1)}, u32[]{:S(2)}, u32[]{:S(2)}) collective-permute-start(bf16[128,1408]{1,0:T(8,128)(2,1)S(1)} %get-tuple-element.52), channel_id=1, source_target_pairs={{0,24},{8,0},{16,8},{24,16},{1,25},{9,1},{17,9},{25,17},{2,26},{10... | collective-permute-start | bytes 1081352 | tf_op jit(solution)/shard_map/ppermute | solution.py:23
  103.9 17.2 %collective-permute-start.29 = (bf16[128,1408]{1,0:T(8,128)(2,1)S(1)}, bf16[128,1408]{1,0:T(8,128)(2,1)S(1)}, u32[]{:S(2)}, u32[]{:S(2)}) collective-permute-start(bf16[128,1408]{1,0:T(8,128)(2,1)S(1)} %get-tuple-element.57), channel_id=1, source_target_pairs={{0,8},{8,16},{16,24},{24,0},{1,9},{9,17},{17,25},{25,1},{2,10},{10... | collective-permute-start | bytes 1081352 | tf_op jit(solution)/shard_map/ppermute | solution.py:23
  106.8 13.5 %collective-permute-start.30 = (bf16[128,1376]{1,0:T(8,128)(2,1)S(1)}, bf16[128,1376]{1,0:T(8,128)(2,1)S(1)}, u32[]{:S(2)}, u32[]{:S(2)}) collective-permute-start(bf16[128,1376]{1,0:T(8,128)(2,1)S(1)} %get-tuple-element.59), channel_id=1, source_target_pairs={{0,8},{8,16},{16,24},{24,0},{1,9},{9,17},{17,25},{25,1},{2,10},{10... | collective-permute-start | bytes 1056776 | tf_op jit(solution)/shard_map/ppermute | solution.py:23
  106.9 14.1 %collective-permute-start.31 = (bf16[128,1376]{1,0:T(8,128)(2,1)S(1)}, bf16[128,1376]{1,0:T(8,128)(2,1)S(1)}, u32[]{:S(2)}, u32[]{:S(2)}) collective-permute-start(bf16[128,1376]{1,0:T(8,128)(2,1)S(1)} %get-tuple-element.60), channel_id=1, source_target_pairs={{0,24},{8,0},{16,8},{24,16},{1,25},{9,1},{17,9},{25,17},{2,26},{10... | collective-permute-start | bytes 1056776 | tf_op jit(solution)/shard_map/ppermute | solution.py:23
  108.9 25.0 %collective-permute-start.36 = (bf16[1376,256]{1,0:T(8,128)(2,1)S(1)}, bf16[1376,256]{1,0:T(8,128)(2,1)S(1)}, u32[]{:S(2)}, u32[]{:S(2)}) collective-permute-start(bf16[1376,256]{1,0:T(8,128)(2,1)S(1)} %copy-done.3), channel_id=1, source_target_pairs={{0,224},{1,33},{32,0},{33,65},{64,32},{65,97},{96,64},{97,129},{12... | collective-permute-start | bytes 2113544 | tf_op jit(solution)/shard_map/ppermute | solution.py:40
  120.3 13.6 %collective-permute-start.37 = (bf16[1376,256]{1,0:T(8,128)(2,1)S(1)}, bf16[1376,256]{1,0:T(8,128)(2,1)S(1)}, u32[]{:S(2)}, u32[]{:S(2)}) collective-permute-start(bf16[1376,256]{1,0:T(8,128)(2,1)S(1)} %collective-permute-done.35.refs_1_), channel_id=1, source_target_pairs={{0,32},{1,225},{32,64},{33,1},{64,96},{65,33},{96,128},{97,65},{12... | collective-permute-start | bytes 2113544 | tf_op jit(solution)/shard_map/ppermute | solution.py:40
  122.5 10.7 %collective-permute-start.32 = (bf16[128,1376]{1,0:T(8,128)(2,1)S(1)}, bf16[128,1376]{1,0:T(8,128)(2,1)S(1)}, u32[]{:S(2)}, u32[]{:S(2)}) collective-permute-start(bf16[128,1376]{1,0:T(8,128)(2,1)S(1)} %shard_map.177.refs_0_), channel_id=1, source_target_pairs={{0,8},{1,25},{8,16},{9,1},{16,24},{17,9},{24,0},{25,17},{2,10},{3,... | collective-permute-start | bytes 1056776 | tf_op jit(solution)/shard_map/ppermute | solution.py:40
  125.0 10.0 %collective-permute-start.33 = (bf16[128,1376]{1,0:T(8,128)(2,1)S(1)}, bf16[128,1376]{1,0:T(8,128)(2,1)S(1)}, u32[]{:S(2)}, u32[]{:S(2)}) collective-permute-start(bf16[128,1376]{1,0:T(8,128)(2,1)S(1)} %shard_map.177.refs_0_), channel_id=1, source_target_pairs={{0,24},{1,9},{8,0},{9,17},{16,8},{17,25},{24,16},{25,1},{2,26},{3,... | collective-permute-start | bytes 1056776 | tf_op jit(solution)/shard_map/ppermute | solution.py:40
  133.2 7.4 %collective-permute-start.34 = (bf16[128,1376]{1,0:T(8,128)(2,1)S(1)}, bf16[128,1376]{1,0:T(8,128)(2,1)S(1)}, u32[]{:S(2)}, u32[]{:S(2)}) collective-permute-start(bf16[128,1376]{1,0:T(8,128)(2,1)S(1)} %collective-permute-done.32.refs_1_), channel_id=1, source_target_pairs={{0,8},{1,25},{8,16},{9,1},{16,24},{17,9},{24,0},{25,17},{2,10},{3,... | collective-permute-start | bytes 1056776 | tf_op jit(solution)/shard_map/ppermute | solution.py:40
  141.6 2.0 %collective-permute-start.38 = (bf16[4,256,256]{2,1,0:T(8,128)(2,1)S(1)}, bf16[4,256,256]{2,1,0:T(8,128)(2,1)S(1)}, u32[]{:S(2)}, u32[]{:S(2)}) collective-permute-start(bf16[4,256,256]{2,1,0:T(8,128)(2,1)S(1)} %shard_map.180), channel_id=1, source_target_pairs={{0,1},{1,0},{2,3},{3,2},{4,5},{5,4},{6,7},{7,6},{8,9},{9,8},{10,11... | collective-permute-start | bytes 1572872 | tf_op jit(solution)/shard_map/ppermute | solution.py:23
  143.8 7.3 %collective-permute-start.39 = (bf16[256,256]{1,0:T(8,128)(2,1)S(1)}, bf16[256,256]{1,0:T(8,128)(2,1)S(1)}, u32[]{:S(2)}, u32[]{:S(2)}) collective-permute-start(bf16[256,256]{1,0:T(8,128)(2,1)S(1)} %get-tuple-element.62), channel_id=1, source_target_pairs={{0,2},{2,4},{4,6},{6,0},{1,3},{3,5},{5,7},{7,1},{8,10},{10,12},{12... | collective-permute-start | bytes 393224 | tf_op jit(solution)/shard_map/ppermute | solution.py:23
  144.6 9.2 %collective-permute-start.40 = (bf16[256,256]{1,0:T(8,128)(2,1)S(1)}, bf16[256,256]{1,0:T(8,128)(2,1)S(1)}, u32[]{:S(2)}, u32[]{:S(2)}) collective-permute-start(bf16[256,256]{1,0:T(8,128)(2,1)S(1)} %get-tuple-element.63), channel_id=1, source_target_pairs={{0,4},{2,6},{4,0},{6,2},{1,5},{3,7},{5,1},{7,3},{8,12},{10,14},{12... | collective-permute-start | bytes 393224 | tf_op jit(solution)/shard_map/ppermute | solution.py:23
  147.5 6.5 %collective-permute-start.41 = (bf16[256,256]{1,0:T(8,128)(2,1)S(1)}, bf16[256,256]{1,0:T(8,128)(2,1)S(1)}, u32[]{:S(2)}, u32[]{:S(2)}) collective-permute-start(bf16[256,256]{1,0:T(8,128)(2,1)S(1)} %get-tuple-element.64), channel_id=1, source_target_pairs={{0,6},{2,0},{4,2},{6,4},{1,7},{3,1},{5,3},{7,5},{8,14},{10,8},{12,... | collective-permute-start | bytes 393224 | tf_op jit(solution)/shard_map/ppermute | solution.py:23
  154.1 7.4 %collective-permute-start.42 = (bf16[128,256]{1,0:T(8,128)(2,1)S(1)}, bf16[128,256]{1,0:T(8,128)(2,1)S(1)}, u32[]{:S(2)}, u32[]{:S(2)}) collective-permute-start(bf16[128,256]{1,0:T(8,128)(2,1)S(1)} %get-tuple-element.65), channel_id=1, source_target_pairs={{0,0},{1,16},{8,8},{9,24},{16,1},{17,17},{24,9},{25,25},{2,2},{3,1... | collective-permute-start | bytes 196616 | tf_op jit(solution)/shard_map/ppermute | solution.py:67
  159.2 3.8 %collective-permute-start.43 = (bf16[128,256]{1,0:T(8,128)(2,1)S(1)}, bf16[128,256]{1,0:T(8,128)(2,1)S(1)}, u32[]{:S(2)}, u32[]{:S(2)}) collective-permute-start(bf16[128,256]{1,0:T(8,128)(2,1)S(1)} %get-tuple-element.66), channel_id=1, source_target_pairs={{0,8},{1,24},{8,0},{9,16},{16,9},{17,25},{24,1},{25,17},{2,10},{3,... | collective-permute-start | bytes 196616 | tf_op jit(solution)/shard_map/ppermute | solution.py:67
  (10 other events, 127.6 us)
